TPU v7x, 512 devices: a whole 4x8x8 slice. The times are simulated.
512 devices in a mesh: sp: 32 (over z, x), tp: 16 (over y, core).
Axes of the slice: x: 4, y: 8, z: 8, core: 2. Of those that a mesh axis runs over, the one named last changes fastest.
Arguments:
- queries: bfloat16 [8192, 2048], P('sp', 'tp'), may hold values from -6 to 6
- keys: bfloat16 [8192, 1024], P('sp', 'tp'), may hold values from -6 to 6
- values: bfloat16 [8192, 1024], P('sp', 'tp'), may hold values from -6 to 6
- docs: int32 [8192], P('sp'), may hold values from 0 to 2, never falling along the last dimension, each value on 1 to 5120 neighbouring positions
- query_gain: float32 [64], replicated, may hold values from 0.5 to 8
- key_gain: float32 [64], replicated, may hold values from 0.5 to 8
- out_weight: bfloat16 [2048, 2048], P('tp'), may hold values from -0.125 to 0.125
- residual: bfloat16 [8192, 2048], P('sp', 'tp'), may hold values from -12 to 12
- norm_gain: float32 [2048], P('tp'), may hold values from 0.1 to 1.9
- routes: int32 [8192, 2], P('sp'), may hold values from 0 to 31, all different within a row; in each aligned block of 256 rows (0 to 255, 256 to 511, ...) at most 20 rows name the same one
- route_weight: float32 [8192, 2], P('sp'), may hold values from 0.1 to 1
- gate_weight: bfloat16 [32, 2048, 4096], P('sp', None, 'tp'), may hold values from -0.3125 to 0.3125
- up_weight: bfloat16 [32, 2048, 4096], P('sp', None, 'tp'), may hold values from -0.3125 to 0.3125
- down_weight: bfloat16 [32, 4096, 2048], P('sp', 'tp'), may hold values from -0.09375 to 0.09375
Outputs:
- mixed: bfloat16 [8192, 2048], P('sp', 'tp')
Inputs may be any that keep to these rules, and one draw needn't show every extreme that they name: `routes`: in each aligned block of 256 rows no expert is named by more than 20 rows, and 20 is reached in some block; a row names 2 different experts. `docs`: document numbers never fall along the sequence; a document holds at most 5120 positions.
All inputs are finite; a program needn't handle non-finite values.
Results may differ from a plain program's by a relative error of at most 0.028.
The roundings to bfloat16 on the way count: a program that leaves them out, or rounds other values in their place, can miss the bound.
Values may be sent and summed in bfloat16 or wider, within the bound.
No kernel may reach another device: no remote copies, remote signals or barrier semaphores. Data moves between devices by JAX's collectives and lax.ppermute only.
A program may use at most 64 MiB of HBM per device.

v0:
```python
import jax
import jax.numpy as jnp
from jax import lax
from jax.sharding import PartitionSpec as P

GRID_W = 64


EPSILON = 1e-06
NEG_BIG = -1e30
ROTARY_BASE = 10000.0
CLAMP_LIMIT = 7.0
SIGMOID_SCALE = 1.702


def sent_together(arrays, axis, dim, along):
    columns = [a.reshape(*a.shape[:along], -1) for a in arrays]
    both = jnp.concatenate(columns, axis=along)
    out, at, gathered = (lax.all_gather(both, axis, axis=dim, tiled=True), 0, [])
    for a, column in zip(arrays, columns):
        piece = out[..., at : at + column.shape[along]]
        gathered.append(piece.reshape(*piece.shape[:along], *a.shape[along:]))
        at += column.shape[along]
    return tuple(gathered)


def cut_along(value, dim, length):
    before, after = (value.shape[:dim], value.shape[dim + 1 :])
    return jnp.moveaxis(value.reshape(*before, length, -1, *after), dim, 0)


def summed_on_arrival(value, axis, dim):
    length = lax.axis_size(axis)
    tiles = lax.all_to_all(cut_along(value, dim, length), axis, 0, 0, tiled=True)
    return jnp.sum(tiles.astype(jnp.float32), axis=0)


def copy_for_each(value, axis):
    length = lax.axis_size(axis)
    return lax.all_to_all(
        jnp.broadcast_to(value[None], (length, *value.shape)), axis, 0, 0, tiled=True
    )


def of_everyone(value, axis):
    everything = copy_for_each(value, axis)
    return jnp.sum(everything, axis=0)


def rope_tables(positions, head_dim):
    quarter = head_dim // 4
    freqs = ROTARY_BASE ** (-jnp.arange(quarter, dtype=jnp.float32) / quarter)
    row_pos = (positions // GRID_W).astype(jnp.float32)
    col_pos = (positions % GRID_W).astype(jnp.float32)
    angle = jnp.concatenate([row_pos[:, None] * freqs, col_pos[:, None] * freqs], axis=1)
    return (jnp.cos(angle), jnp.sin(angle))


def norm_rotate(heads, gain, cosine_table, sine_table):
    entries = heads.astype(jnp.float32)
    entries = (
        entries * lax.rsqrt(jnp.mean(entries * entries, axis=-1, keepdims=True) + EPSILON) * gain
    )
    pairs = entries.reshape(entries.shape[:-1] + (entries.shape[-1] // 2, 2))
    first = pairs[..., 0]
    second = pairs[..., 1]
    cos_rows = cosine_table[:, None, :]
    sin_rows = sine_table[:, None, :]
    turned = jnp.stack(
        [first * cos_rows - second * sin_rows, first * sin_rows + second * cos_rows], axis=-1
    )
    return turned.reshape(heads.shape).astype(jnp.bfloat16)


def clamped_unit(gate_pre, up_pre):
    bounded = jnp.minimum(gate_pre, CLAMP_LIMIT)
    linear = jnp.clip(up_pre, -CLAMP_LIMIT, CLAMP_LIMIT)
    return (bounded * jax.nn.sigmoid(SIGMOID_SCALE * bounded) * (linear + 1.0)).astype(jnp.bfloat16)


def block_length(length):
    block_size = length
    while block_size > 2048 and block_size % 2 == 0:
        block_size = block_size // 2
    return block_size


def softmax_update(running, inputs, query_rot, own_tags, score_scale):
    row_peak, denominator, carried = running
    key_block, value_block, tag_block = inputs
    scores = (
        jnp.einsum("tkgd,pkd->tkgp", query_rot, key_block, preferred_element_type=jnp.float32)
        * score_scale
    )
    allowed = own_tags[:, None, None, None] == tag_block[None, None, None, :]
    scores = jnp.where(allowed, scores, NEG_BIG)
    new_peak = jnp.maximum(row_peak, jnp.max(scores, axis=-1))
    weights = jnp.where(allowed, jnp.exp(scores - new_peak[..., None]), 0.0)
    factor = jnp.exp(row_peak - new_peak)
    denominator = denominator * factor + jnp.sum(weights, axis=-1)
    carried = carried * factor[..., None] + jnp.einsum(
        "tkgp,pkd->tkgd",
        weights.astype(jnp.bfloat16),
        value_block,
        preferred_element_type=jnp.float32,
    )
    return (new_peak, denominator, carried)


def per_device(
    queries,
    keys,
    values,
    docs,
    query_gain,
    key_gain,
    out_weight,
    residual,
    norm_gain,
    routes,
    route_weight,
    gate_weight,
    up_weight,
    down_weight,
):
    tokens = queries.shape[0]
    head_dim = query_gain.shape[0]
    query_heads = queries.shape[1] // head_dim
    pair_heads = keys.shape[1] // head_dim
    pair_width = keys.shape[1]
    positions = lax.axis_index("sp") * tokens + jnp.arange(tokens, dtype=jnp.int32)
    cosine_table, sine_table = rope_tables(positions, head_dim)
    query_rot = norm_rotate(
        queries.reshape(tokens, query_heads, head_dim), query_gain, cosine_table, sine_table
    )
    query_rot = query_rot.reshape(tokens, pair_heads, 2, head_dim)
    key_rot = norm_rotate(
        keys.reshape(tokens, pair_heads, head_dim), key_gain, cosine_table, sine_table
    )
    stacked = jnp.concatenate([key_rot.reshape(tokens, pair_width), values], axis=1)
    own_tags = docs.astype(jnp.bfloat16)
    score_scale = head_dim ** (-0.5)
    stat_shape = (tokens, pair_heads, 2)
    initial = (
        jnp.full(stat_shape, NEG_BIG, jnp.float32),
        jnp.zeros(stat_shape, jnp.float32),
        jnp.zeros(stat_shape + (head_dim,), jnp.float32),
    )
    pair_rows, tag_rows = sent_together((stacked, own_tags), "sp", 0, 1)
    length = pair_rows.shape[0]
    block_size = block_length(length)
    blocks = length // block_size
    key_part = pair_rows[:, :pair_width].reshape(blocks, block_size, pair_heads, head_dim)
    value_part = pair_rows[:, pair_width:].reshape(blocks, block_size, pair_heads, head_dim)
    tag_part = tag_rows.reshape(blocks, block_size)

    def advance(carry_state, inputs):
        return (softmax_update(carry_state, inputs, query_rot, own_tags, score_scale), None)

    result, _ = lax.scan(advance, initial, (key_part, value_part, tag_part))
    row_peak, denominator, carried = result
    attended = (
        (carried / denominator[..., None])
        .astype(jnp.bfloat16)
        .reshape(tokens, query_heads * head_dim)
    )
    width_local = residual.shape[1]
    projected = summed_on_arrival(
        lax.dot_general(
            out_weight, attended, (((0,), (1,)), ((), ())), preferred_element_type=jnp.float32
        ).astype(jnp.bfloat16),
        "tp",
        0,
    )
    mixed_first = residual.astype(jnp.float32) + projected.T
    squares = of_everyone(jnp.sum(mixed_first * mixed_first, axis=1), "tp")
    full_width = width_local * lax.axis_size("tp")
    normed = (mixed_first * lax.rsqrt(squares / full_width + EPSILON)[:, None] * norm_gain).astype(
        jnp.bfloat16
    )
    experts = lax.axis_size("sp")
    top_count = routes.shape[1]
    capacity = max(2, 5 * tokens * top_count // (4 * experts))
    flat_routes = routes.reshape(-1)
    entries = flat_routes.shape[0]
    expert_ids = jnp.arange(experts, dtype=jnp.int32)
    onehot = (flat_routes[:, None] == expert_ids[None, :]).astype(jnp.int32)
    earlier = jnp.cumsum(onehot, axis=0) - onehot
    slot_index = jnp.sum(earlier * onehot, axis=1)
    slot_ids = jnp.arange(capacity, dtype=jnp.int32)
    matches = (flat_routes[:, None, None] == expert_ids[None, :, None]) & (
        slot_index[:, None, None] == slot_ids[None, None, :]
    )
    entry_ids = jnp.arange(entries, dtype=jnp.int32)
    source_entry = jnp.sum(jnp.where(matches, entry_ids[:, None, None], 0), axis=0)
    occupied = jnp.any(matches, axis=0)
    source_row = source_entry // top_count
    gate_local = gate_weight[0]
    up_local = up_weight[0]
    down_local = down_weight[0]
    model_width = gate_local.shape[0]
    outgoing = jnp.where(occupied[..., None], normed[source_row], jnp.zeros((), jnp.bfloat16))
    arrived = lax.all_to_all(outgoing, "sp", split_axis=0, concat_axis=0, tiled=True)
    sources = arrived.shape[0]
    flat_rows = arrived.reshape(-1, width_local)
    column_piece = lax.all_gather(flat_rows, "tp", axis=1, tiled=True)
    gate_pre = jnp.dot(column_piece, gate_local, preferred_element_type=jnp.float32)
    up_pre = jnp.dot(column_piece, up_local, preferred_element_type=jnp.float32)
    hidden = clamped_unit(gate_pre, up_pre)
    partial_value = jnp.dot(hidden, down_local, preferred_element_type=jnp.float32).reshape(
        sources, capacity, model_width
    )
    expert_out = summed_on_arrival(partial_value.astype(jnp.bfloat16), "tp", 2).astype(jnp.bfloat16)
    returned = lax.all_to_all(expert_out, "sp", split_axis=0, concat_axis=0, tiled=True)
    lookup = flat_routes * capacity + slot_index
    picked = (
        returned.reshape(-1, width_local)[lookup]
        .reshape(tokens, top_count, width_local)
        .astype(jnp.float32)
    )
    routed = jnp.sum(route_weight[:, :, None] * picked, axis=1)
    return (mixed_first + routed).astype(jnp.bfloat16)


def solution(mesh):
    in_specs = (
        P("sp", "tp"),
        P("sp", "tp"),
        P("sp", "tp"),
        P("sp"),
        P(),
        P(),
        P("tp", None),
        P("sp", "tp"),
        P("tp"),
        P("sp", None),
        P("sp", None),
        P("sp", None, "tp"),
        P("sp", None, "tp"),
        P("sp", "tp", None),
    )
    out_specs = P("sp", "tp")
    return jax.shard_map(
        per_device, mesh=mesh, in_specs=in_specs, out_specs=out_specs, check_vma=False
    )
```

profile of v0, /device:TPU:1, one launch (start us, length us, event | category | flops | bytes accessed | tf_op | source)
XLA Modules:
  0.0 352.6 jit_solution(10780892546366876018)
XLA Ops:
  9.4 1.4 pad_maximum_fusion
  13.3 80.9 %all-gather.3.cloned.1.call-done = bf16[8192,129]{0,1:T(8,128)(2,1)} async-done(((bf16[256,129]{0,1:T(8,128)(2,1)}), bf16[8192,129]{0,1:T(8,128)(2,1)}) %all-gather.3.cloned.1.call-update) | async-done | bytes 2113552 | tf_op jit(solution)/shard_map/all_gather | solution.py:19
  94.1 2.7 fusion.54
  96.8 1.8 reshape.581
  98.7 1.6 copy.94
  101.0 1.6 copy.95
  103.6 35.0 %while.15 = (s32[]{:T(128)}, f32[256,1,2]{0,2,1:T(2,128)S(1)}, f32[256,1,2]{0,2,1:T(2,128)S(1)}, f32[256,1,2,64]{0,3,2,1:T(8,128)S(1)}, bf16[256]{0:T(256)(128)(...) while((s32[]{:T(128)}, f32[256,1,2]{0,2,1:T(2,128)S(1)}, ...), condition=%wide.region_5.6_spmd.clone, body=%wide.region_2.5_spmd.clone.sunk | while | flops 282692608 | bytes 32355992 | solution.py:160
  104.1 3.6 %fusion.68 = (f32[256,2]{0,1:T(2,128)S(1)}, f32[2048,256,2]{1,0,2:T(8,128)}) fusion(pred[256,2048]{0,1:T(8,128)(4,1)S(1)} %broadcast_compare_fusion.3, bf16[256,1,2,64]{0,3,2,1:T(8,128)(2,1)S(1)} %get-tuple-element.262, bf16[4,2048,1,64]{1,3,2,0:T(8,128)(2,1)} %get-tuple-element.261, s32[]{:T(128)} %get-tuple-element.244), kind=kOutput, calls=%fused_computation.4.clone.1 | convolution fusion | flops 137362944 | bytes 5048832 | tf_op jit(solution)/shard_map/while/body/eval_jaxpr/tkgd,pkd->tkgp/dot_general | solution.py:92
  107.7 3.5 fusion.71
  112.8 3.6 %fusion.68 = (f32[256,2]{0,1:T(2,128)S(1)}, f32[2048,256,2]{1,0,2:T(8,128)}) fusion(pred[256,2048]{0,1:T(8,128)(4,1)S(1)} %broadcast_compare_fusion.3, bf16[256,1,2,64]{0,3,2,1:T(8,128)(2,1)S(1)} %get-tuple-element.262, bf16[4,2048,1,64]{1,3,2,0:T(8,128)(2,1)} %get-tuple-element.261, s32[]{:T(128)} %get-tuple-element.244), kind=kOutput, calls=%fused_computation.4.clone.1 | convolution fusion | flops 137362944 | bytes 5048832 | tf_op jit(solution)/shard_map/while/body/eval_jaxpr/tkgd,pkd->tkgp/dot_general | solution.py:92
  116.5 3.5 fusion.71
  121.6 3.6 %fusion.68 = (f32[256,2]{0,1:T(2,128)S(1)}, f32[2048,256,2]{1,0,2:T(8,128)}) fusion(pred[256,2048]{0,1:T(8,128)(4,1)S(1)} %broadcast_compare_fusion.3, bf16[256,1,2,64]{0,3,2,1:T(8,128)(2,1)S(1)} %get-tuple-element.262, bf16[4,2048,1,64]{1,3,2,0:T(8,128)(2,1)} %get-tuple-element.261, s32[]{:T(128)} %get-tuple-element.244), kind=kOutput, calls=%fused_computation.4.clone.1 | convolution fusion | flops 137362944 | bytes 5048832 | tf_op jit(solution)/shard_map/while/body/eval_jaxpr/tkgd,pkd->tkgp/dot_general | solution.py:92
  125.2 3.5 fusion.71
  130.3 3.6 %fusion.68 = (f32[256,2]{0,1:T(2,128)S(1)}, f32[2048,256,2]{1,0,2:T(8,128)}) fusion(pred[256,2048]{0,1:T(8,128)(4,1)S(1)} %broadcast_compare_fusion.3, bf16[256,1,2,64]{0,3,2,1:T(8,128)(2,1)S(1)} %get-tuple-element.262, bf16[4,2048,1,64]{1,3,2,0:T(8,128)(2,1)} %get-tuple-element.261, s32[]{:T(128)} %get-tuple-element.244), kind=kOutput, calls=%fused_computation.4.clone.1 | convolution fusion | flops 137362944 | bytes 5048832 | tf_op jit(solution)/shard_map/while/body/eval_jaxpr/tkgd,pkd->tkgp/dot_general | solution.py:92
  134.0 3.5 fusion.71
  139.2 1.3 copy.127
  140.4 10.9 %all-to-all-start = ((bf16[16,128,256]{1,2,0:T(8,128)(2,1)}), bf16[16,128,256]{1,2,0:T(8,128)(2,1)S(1)}, u32[]{:S(2)}, u32[]{:S(2)}) async-start(bf16[16,128,256]{1,2,0:T(8,128)(2,1)} %bitcast.153), calls=%async_computation | async-start | bytes 2097152 | tf_op jit(solution)/shard_map/all_to_all | solution.py:34
  151.8 1.2 reduce-window.6
  154.5 24.9 %all-to-all-done = bf16[16,128,256]{1,2,0:T(8,128)(2,1)S(1)} async-done(((bf16[16,128,256]{1,2,0:T(8,128)(2,1)}), bf16[16,128,256]{1,2,0:T(8,128)(2,1)S(1)}, u32[]{:S(2)}, u32[]{:S(2)}) %all-to-all-start) | async-done | bytes 1048608 | tf_op jit(solution)/shard_map/all_to_all | solution.py:34
  180.2 3.4 all-to-all-start.1
  183.8 7.2 %all-to-all-done.1 = f32[16,1,256]{2,1,0:T(1,128)S(1)} async-done(((f32[16,1,256]{2,1,0:T(1,128)}), f32[16,1,256]{2,1,0:T(1,128)S(1)}, u32[]{:S(2)}, u32[]{:S(2)}) %all-to-all-start.1) | async-done | bytes 16416 | tf_op jit(solution)/shard_map/all_to_all | solution.py:40
  191.1 2.0 gather_fusion
  193.4 17.9 %all_to_all.26 = bf16[32,20,128]{2,1,0:T(8,128)(2,1)S(1)} all-to-all(bf16[32,20,128]{2,1,0:T(8,128)(2,1)S(1)} %broadcast_select_fusion.1), channel_id=1, replica_groups=mesh['sp'=32,'tp'=16] {'sp'}, dimensions={0} | all-to-all | bytes 327680 | tf_op jit(solution)/shard_map/all_to_all | solution.py:203
  212.0 37.1 %all-gather.5.cloned.1.call-done = bf16[640,2048]{1,0:T(8,128)(2,1)} async-done(((bf16[640,128]{1,0:T(8,128)(2,1)}), bf16[640,2048]{1,0:T(8,128)(2,1)}) %all-gather.5.cloned.1.call-update) | async-done | bytes 2621456 | tf_op jit(solution)/shard_map/all_gather | solution.py:206
  249.1 2.7 convolution_minimum_fusion
  253.8 2.2 copy.126
  256.0 5.0 %all-to-all-start.3 = ((bf16[16,32,20,128]{3,1,2,0:T(8,128)(2,1)}), bf16[16,32,20,128]{3,1,2,0:T(8,128)(2,1)}, u32[]{:S(2)}, u32[]{:S(2)}) async-start(bf16[16,32,20,128]{3,1,2,0:T(8,128)(2,1)} %bitcast.176), calls=%async_computation.3 | async-start | bytes 5242880 | tf_op jit(solution)/shard_map/all_to_all | solution.py:34
  261.4 59.2 %all-to-all-done.3 = bf16[16,32,20,128]{3,1,2,0:T(8,128)(2,1)} async-done(((bf16[16,32,20,128]{3,1,2,0:T(8,128)(2,1)}), bf16[16,32,20,128]{3,1,2,0:T(8,128)(2,1)}, u32[]{:S(2)}, u32[]{:S(2)}) %all-to-all-start.3) | async-done | bytes 2621472 | tf_op jit(solution)/shard_map/all_to_all | solution.py:34
  320.7 2.1 reduce_sum.107
  323.5 9.9 %all-to-all-start.4 = ((bf16[32,20,128]{2,1,0:T(8,128)(2,1)}), bf16[32,20,128]{2,1,0:T(8,128)(2,1)S(1)}, u32[]{:S(2)}, u32[]{:S(2)}) async-start(bf16[32,20,128]{2,1,0:T(8,128)(2,1)} %copy.107), calls=%async_computation.4 | async-start | bytes 393216 | tf_op jit(solution)/shard_map/all_to_all | solution.py:214
  333.4 9.8 %all-to-all-done.4 = bf16[32,20,128]{2,1,0:T(8,128)(2,1)S(1)} async-done(((bf16[32,20,128]{2,1,0:T(8,128)(2,1)}), bf16[32,20,128]{2,1,0:T(8,128)(2,1)S(1)}, u32[]{:S(2)}, u32[]{:S(2)}) %all-to-all-start.4) | async-done | bytes 163872 | tf_op jit(solution)/shard_map/all_to_all | solution.py:214
  343.3 1.3 gather_fusion.1
  (125 shorter events, 22.0 us)
Async XLA Ops:
  6.5 246.3 %copy-start = (bf16[1,256,2048]{2,1,0:T(8,128)(2,1)S(1)}, bf16[1,256,2048]{2,1,0:T(8,128)(2,1)}, u32[]{:S(2)}) copy-start(bf16[1,256,2048]{2,1,0:T(8,128)(2,1)} %param.29) | copy-start | bytes 3145732
  6.5 87.6 %all-gather.3.cloned.1.call-start = ((), (), s32[]{:S(2)}) async-start(), calls=%async_computation.5 | async-start | bytes 2297856 | tf_op jit(solution)/shard_map/all_gather | solution.py:19
  103.6 35.1 %copy-start.3 = (bf16[128,2048]{1,0:T(8,128)(2,1)S(1)}, bf16[128,2048]{1,0:T(8,128)(2,1)}, u32[]{:S(2)}) copy-start(bf16[128,2048]{1,0:T(8,128)(2,1)} %param.22) | copy-start | bytes 1572868
  107.7 3.5 %copy-start.1 = (f32[2048,256,2]{1,0,2:T(8,128)S(1)}, f32[2048,256,2]{1,0,2:T(8,128)}, u32[]{:S(2)}) copy-start(f32[2048,256,2]{1,0,2:T(8,128)} %get-tuple-element.231) | copy-start | bytes 12582916 | tf_op jit(solution)/shard_map/while
  116.5 3.5 %copy-start.1 = (f32[2048,256,2]{1,0,2:T(8,128)S(1)}, f32[2048,256,2]{1,0,2:T(8,128)}, u32[]{:S(2)}) copy-start(f32[2048,256,2]{1,0,2:T(8,128)} %get-tuple-element.231) | copy-start | bytes 12582916 | tf_op jit(solution)/shard_map/while
  125.2 3.5 %copy-start.1 = (f32[2048,256,2]{1,0,2:T(8,128)S(1)}, f32[2048,256,2]{1,0,2:T(8,128)}, u32[]{:S(2)}) copy-start(f32[2048,256,2]{1,0,2:T(8,128)} %get-tuple-element.231) | copy-start | bytes 12582916 | tf_op jit(solution)/shard_map/while
  134.0 3.5 %copy-start.1 = (f32[2048,256,2]{1,0,2:T(8,128)S(1)}, f32[2048,256,2]{1,0,2:T(8,128)}, u32[]{:S(2)}) copy-start(f32[2048,256,2]{1,0,2:T(8,128)} %get-tuple-element.231) | copy-start | bytes 12582916 | tf_op jit(solution)/shard_map/while
  138.6 12.7 %copy-start.4 = (s32[256,2]{0,1:T(2,128)S(1)}, s32[256,2]{0,1:T(2,128)}, u32[]{:S(2)}) copy-start(s32[256,2]{0,1:T(2,128)} %param.25) | copy-start | bytes 6148
  138.6 40.8 %copy-start.2 = (bf16[256,128]{1,0:T(8,128)(2,1)S(1)}, bf16[256,128]{1,0:T(8,128)(2,1)}, u32[]{:S(2)}) copy-start(bf16[256,128]{1,0:T(8,128)(2,1)} %param.23) | copy-start | bytes 196612
  138.7 52.4 %copy-start.6 = (f32[128]{0:T(128)S(1)}, f32[128]{0:T(128)}, u32[]{:S(2)}) copy-start(f32[128]{0:T(128)} %param.24) | copy-start | bytes 1540
  140.4 108.7 %copy-start.8 = (bf16[1,2048,256]{2,1,0:T(8,128)(2,1)S(1)}, bf16[1,2048,256]{2,1,0:T(8,128)(2,1)}, u32[]{:S(2)}) copy-start(bf16[1,2048,256]{2,1,0:T(8,128)(2,1)} %param.27) | copy-start | bytes 3145732
  140.4 38.9 %all-to-all-start = ((bf16[16,128,256]{1,2,0:T(8,128)(2,1)}), bf16[16,128,256]{1,2,0:T(8,128)(2,1)S(1)}, u32[]{:S(2)}, u32[]{:S(2)}) async-start(bf16[16,128,256]{1,2,0:T(8,128)(2,1)} %bitcast.153), calls=%async_computation | async-start | bytes 2097152 | tf_op jit(solution)/shard_map/all_to_all | solution.py:34
  180.2 10.8 %all-to-all-start.1 = ((f32[16,1,256]{2,1,0:T(1,128)}), f32[16,1,256]{2,1,0:T(1,128)S(1)}, u32[]{:S(2)}, u32[]{:S(2)}) async-start(f32[16,1,256]{2,1,0:T(1,128)} %broadcast_in_dim.54), calls=%async_computation.1 | async-start | bytes 32768 | tf_op jit(solution)/shard_map/all_to_all | solution.py:40
  183.7 65.5 %all-gather.5.cloned.1.call-start = ((), (), s32[]{:S(2)}) async-start(), calls=%async_computation.6 | async-start | bytes 2785280 | tf_op jit(solution)/shard_map/all_gather | solution.py:206
  249.1 2.8 copy-start.7
  249.1 2.8 copy-start.9
  253.7 7.5 %copy-start.5 = (f32[256,2]{0,1:T(2,128)S(1)}, f32[256,2]{0,1:T(2,128)}, u32[]{:S(2)}) copy-start(f32[256,2]{0,1:T(2,128)} %param.26) | copy-start | bytes 6148
  256.0 64.7 %all-to-all-start.3 = ((bf16[16,32,20,128]{3,1,2,0:T(8,128)(2,1)}), bf16[16,32,20,128]{3,1,2,0:T(8,128)(2,1)}, u32[]{:S(2)}, u32[]{:S(2)}) async-start(bf16[16,32,20,128]{3,1,2,0:T(8,128)(2,1)} %bitcast.176), calls=%async_computation.3 | async-start | bytes 5242880 | tf_op jit(solution)/shard_map/all_to_all | solution.py:34
  323.5 19.8 %all-to-all-start.4 = ((bf16[32,20,128]{2,1,0:T(8,128)(2,1)}), bf16[32,20,128]{2,1,0:T(8,128)(2,1)S(1)}, u32[]{:S(2)}, u32[]{:S(2)}) async-start(bf16[32,20,128]{2,1,0:T(8,128)(2,1)} %copy.107), calls=%async_computation.4 | async-start | bytes 393216 | tf_op jit(solution)/shard_map/all_to_all | solution.py:214
Sparse Core Ops, SparseCore 0:
  10.9 83.1 all-gather.2
  212.1 36.9 all-gather.4
where the time goes:
time: 355 us; the launch traced here: 353 us
  waiting for transfers between devices  219 us (62%)
  matrix products  33.4 us (9%)
  starting transfers between devices  29.3 us (8%)
  local copies, waits for them, and re-layouts  22.1 us (6%)
  blocking collectives  17.9 us (5%)
  other arithmetic  16.7 us (5%)
  between operations  13.9 us (4%)
    all_to_all x2, waiting for transfers between devices, summed_on_arrival(): lax.all_to_all(cut_along(value, dim, length), axis, 0, 0, tiled=True)  84.1 us
    all_gather x1, waiting for transfers between devices, sent_together(): lax.all_gather(both, axis, axis=dim, tiled=True)  80.9 us
    all_gather x1, waiting for transfers between devices, per_device(): column_piece = lax.all_gather(flat_rows, 'tp', axis=1, tiled=True)  37.1 us
    all_to_all x1, blocking collectives, per_device(): lax.all_to_all(outgoing, 'sp', split_axis=0, concat_axis=0, tiled=True)  17.9 us
    all_to_all x2, starting transfers between devices, summed_on_arrival(): lax.all_to_all(cut_along(value, dim, length), axis, 0, 0, tiled=True)  15.9 us
    dot_general x4, matrix products, softmax_update(): jnp.einsum('tkgd,pkd->tkgp', query_rot, key_block, preferred_element_type...  14.5 us
    dot_general x4, matrix products, softmax_update(): jnp.einsum('tkgp,pkd->tkgd', weights.astype(jnp.bfloat16), value_block, p...  13.9 us
    all_to_all x1, starting transfers between devices, per_device(): lax.all_to_all(expert_out, 'sp', split_axis=0, concat_axis=0, tiled=True)  9.9 us
  transfers between devices with their start and end apart: 6, of which 6 were waited for; matrix products, arithmetic and copies ran while one was open for 2% of the time, Pallas kernels for 0%

commit v1 on v0

v1 whole, which is shorter than its diff:
```python
import functools

import jax
import jax.numpy as jnp
import numpy as np
from jax import lax
from jax.experimental import pallas as pl
from jax.experimental.pallas import tpu as pltpu
from jax.sharding import Mesh, PartitionSpec as P

GRID_W = 64
EPSILON = 1e-06
ROTARY_BASE = 10000.0
CLAMP_LIMIT = 7.0
SIGMOID_SCALE = 1.702
N_Z, N_X, N_Y, N_C = 8, 4, 8, 2
N_SP, N_TP = N_Z * N_X, N_Y * N_C
TOK = 256
HALF = TOK // 2
HD = 64
LANES = 128
D = 2048
EXPERTS = 32
CAP = 20
CAP_PAD = 24
ROWS = N_SP * CAP // 2
HID = 256
NOTE = 16
MASK_BIG = 16384.0

F32 = jnp.float32
BF16 = jnp.bfloat16


def tables():
    quarter = HD // 4
    freqs = (ROTARY_BASE ** (-np.arange(quarter, dtype=np.float32) / quarter)).astype(np.float32)
    lane = np.arange(LANES)
    pair = (lane % HD) // 2
    is_row = pair < quarter
    freq = freqs[np.where(is_row, pair, pair - quarter)]
    sign = np.where(lane % 2 == 0, -1.0, 1.0)
    cols = (np.arange(GRID_W, dtype=np.float32)[:, None] * freq).astype(np.float32)
    rows = (np.arange(N_SP * TOK // GRID_W, dtype=np.float32)[:, None] * freq).astype(np.float32)
    cols, rows = cols.astype(np.float64), rows.astype(np.float64)
    keep = lambda a, m: np.where(m, a, 0.0).astype(np.float32)
    per = TOK // GRID_W
    row_c = keep(np.cos(rows), is_row).reshape(N_SP, per, LANES)
    row_s = keep(np.sin(rows) * sign, is_row).reshape(N_SP, per, LANES)
    row_tab = np.concatenate([row_c, row_s], axis=1)
    col_tab = np.stack([keep(np.cos(cols), ~is_row), keep(np.sin(cols) * sign, ~is_row)])
    return row_tab, col_tab


def compaction():
    out = np.zeros((ROWS, 16 * CAP_PAD), np.float32)
    r = np.arange(ROWS)
    out[r, (r // CAP) * CAP_PAD + r % CAP] = 1.0
    return out


def dot(a, b, ca=1, cb=0):
    return lax.dot_general(a, b, (((ca,), (cb,)), ((), ())), preferred_element_type=F32)


def iota(shape, dim):
    return lax.broadcasted_iota(jnp.int32, shape, dim)


def prep_body(blk, q_ref, k_ref, v_ref, docs_ref, qg_ref, kg_ref, row_ref, col_ref, qs_ref, kvs_ref):
    lane = iota((TOK, LANES), 1)
    low = lane < HD
    even = (lane & 1) == 0
    rows = row_ref[blk[0]]
    per = TOK // GRID_W
    cos_t = jnp.concatenate([col_ref[0] + rows[j : j + 1] for j in range(per)], axis=0)
    sin_t = jnp.concatenate([col_ref[1] + rows[per + j : per + j + 1] for j in range(per)], axis=0)

    def turn(n):
        swapped = jnp.where(even, pltpu.roll(n, LANES - 1, 1), pltpu.roll(n, 1, 1))
        return n * cos_t + swapped * sin_t

    x = q_ref[...].astype(F32)
    sq = x * x
    s0 = jnp.sum(jnp.where(low, sq, 0.0), axis=1, keepdims=True)
    s1 = jnp.sum(jnp.where(low, 0.0, sq), axis=1, keepdims=True)
    r0 = lax.rsqrt(s0 * (1.0 / HD) + EPSILON)
    r1 = lax.rsqrt(s1 * (1.0 / HD) + EPSILON)
    gain = jnp.concatenate([qg_ref[...], qg_ref[...]], axis=1)
    q_out = turn(x * jnp.where(low, r0, r1) * gain).astype(BF16)

    kv = jnp.concatenate([k_ref[...], v_ref[...]], axis=0).astype(F32).T
    sk = jnp.sum(jnp.where(low, kv * kv, 0.0), axis=1, keepdims=True)
    rk = lax.rsqrt(sk * (1.0 / HD) + EPSILON)
    gain_k = jnp.concatenate([kg_ref[...], kg_ref[...]], axis=1)
    kv_out = jnp.where(low, turn(kv * rk * gain_k), kv).astype(BF16)

    docs = docs_ref[...]
    n0 = jnp.sum((docs < 1).astype(F32))
    n1 = jnp.sum((docs < 2).astype(F32))
    row = iota((NOTE, LANES), 0)
    note = jnp.where(row == 0, n0, jnp.where(row == 1, n1, 0.0)).astype(BF16)
    for i in range(N_X):
        qs_ref[i, :TOK, :] = q_out
        qs_ref[i, TOK:, :] = note
    for i in range(N_Z):
        kvs_ref[i, :TOK, :] = kv_out
        kvs_ref[i, TOK:, :] = note


def split3(x):
    hi = x.astype(BF16).astype(F32)
    mid = (x - hi).astype(BF16).astype(F32)
    return hi, mid, x - hi - mid


def attend_body(q_ref, kv_ref, out_ref, kp_ref, vp_ref):
    lane = iota((TOK, LANES), 1)
    low = lane < HD
    idx = iota((TOK, LANES), 0).astype(F32)

    def doc_of(note):
        n0 = note[0:1, :].astype(F32)
        n1 = note[1:2, :].astype(F32)
        return jnp.where(idx < n0, HD, jnp.where(idx < n1, HD + 1, HD + 2))

    for j in range(N_Z):
        kv = kv_ref[j, :TOK, :]
        mark = (doc_of(kv_ref[j, TOK:, :]) == lane).astype(F32)
        kvf = kv.astype(F32)
        kp_ref[j * TOK : (j + 1) * TOK, :] = jnp.where(low, kvf, mark).astype(BF16)
        vp_ref[j * TOK : (j + 1) * TOK, :] = jnp.where(low, 1.0, kvf).astype(BF16)
    eye = (iota((HALF, LANES), 0) == iota((HALF, LANES), 1)).astype(BF16)
    lane_h = iota((HALF, LANES), 1)

    def block(b, carry):
        qf = q_ref[b, :TOK, :].astype(F32) * (HD**-0.5)
        doc = doc_of(q_ref[b, TOK:, :])
        other = jnp.where((doc == lane) | (lane > HD + 2), 0.0, -MASK_BIG)
        heads = []
        for h in range(2):
            qh = qf if h == 0 else pltpu.roll(qf, HD, 1)
            qp = jnp.where(low, qh, other).astype(BF16)
            s = dot(qp, kp_ref[...], 1, 1)
            peak = jnp.max(s, axis=1, keepdims=True)
            p = jnp.exp(s - peak).astype(BF16)
            acc = dot(p, vp_ref[...])
            total = acc[:, 0:1]
            o = acc / total
            heads.append((pltpu.roll(o, HD, 1) if h == 0 else o, peak + jnp.log(total)))
        o = jnp.where(low, heads[0][0], heads[1][0]).astype(BF16)
        parts = split3(heads[0][1]) + split3(heads[1][1])
        for half in range(2):
            rows = slice(half * HALF, (half + 1) * HALF)
            stat = jnp.zeros((HALF, LANES), F32)
            for i, part in enumerate(parts):
                stat = jnp.where(lane_h == i, part[rows], stat)
            stat_t = dot(stat.astype(BF16), eye, 0, 0)
            out_ref[b * 2 + half, :HALF, :] = o[rows]
            out_ref[b * 2 + half, HALF:, :] = stat_t[:NOTE].astype(BF16)
        return carry

    lax.fori_loop(0, N_X, block, 0)


def project_body(core, in_ref, w_own_ref, w_other_ref, out_ref):
    row = iota((NOTE, LANES), 0)
    lane = iota((NOTE, LANES), 1)
    pick = (((row < 3) & (lane < HD)) | ((row >= 3) & (row < 6) & (lane >= HD))).astype(BF16)

    def attended(c):
        lse = [dot(in_ref[x * 2 + c, HALF:, :], pick, 0, 0) for x in range(N_X)]
        top = functools.reduce(jnp.maximum, lse)
        total = jnp.zeros((HALF, LANES), F32)
        mixed = jnp.zeros((HALF, LANES), F32)
        for x in range(N_X):
            w = jnp.exp(lse[x] - top)
            total = total + w
            mixed = mixed + w * in_ref[x * 2 + c, :HALF, :].astype(F32)
        return (mixed / total).astype(BF16)

    own = attended(core[0])
    other = attended(1 - core[0])
    for g in range(N_TP):
        cols = slice(g * LANES, (g + 1) * LANES)
        part = dot(own, w_own_ref[:, cols]) + dot(other, w_other_ref[:, cols])
        out_ref[g] = part.astype(BF16)


def route_body(routes_ref, weight_ref, place_ref, mix_ref):
    expert = iota((EXPERTS, TOK), 0)
    r0, r1 = routes_ref[0:1, :], routes_ref[1:2, :]
    named = ((expert == r0) | (expert == r1)).astype(F32)
    before = (iota((TOK, TOK), 0) < iota((TOK, TOK), 1)).astype(BF16)
    slot = dot(named.astype(BF16), before)
    weight = jnp.where(expert == r0, weight_ref[0:1, :], jnp.where(expert == r1, weight_ref[1:2, :], 0.0))
    slot = jnp.where(named > 0.0, slot, -1.0)
    w3 = split3(weight)
    slots = iota((CAP_PAD, TOK), 0).astype(F32)
    for e in range(EXPERTS):
        rows = slice(e * CAP_PAD, (e + 1) * CAP_PAD)
        hit = slots == slot[e : e + 1, :]
        place_ref[rows, :] = hit.astype(F32)
        for i in range(3):
            mix_ref[i, rows, :] = jnp.where(hit, w3[i][e : e + 1, :], 0.0)


def dispatch_body(in_ref, residual_ref, place_ref, mixed_ref, out_ref):
    halves = []
    for c in range(2):
        total = in_ref[c].astype(F32)
        for y in range(1, N_Y):
            total = total + in_ref[y * 2 + c].astype(F32)
        halves.append(total)
    mixed = residual_ref[...].astype(F32) + jnp.concatenate(halves, axis=0)
    mixed_ref[...] = mixed
    out_ref[...] = dot(place_ref[...].astype(BF16), mixed.astype(BF16)).astype(BF16)


def spread_body(in_ref, drop_ref, out_ref):
    for c in range(2):
        rows = in_ref[c * 16 * CAP_PAD : (c + 1) * 16 * CAP_PAD, :]
        kept = dot(drop_ref[...], rows).astype(BF16)
        for y in range(N_Y):
            out_ref[y * 2 + c] = kept


def expert_body(in_ref, gain_ref, g0_ref, g1_ref, u0_ref, u1_ref, d0_ref, d1_ref, out_ref, x_ref):
    total = jnp.zeros((ROWS, LANES), F32)
    for g in range(N_TP):
        x = in_ref[g].astype(F32)
        total = total + x * x
    scale = lax.rsqrt(jnp.sum(total, axis=1, keepdims=True) * (1.0 / D) + EPSILON)
    for g in range(N_TP):
        x = in_ref[g].astype(F32) * scale * gain_ref[g, 0:1, :]
        x_ref[:, g * LANES : (g + 1) * LANES] = x.astype(BF16)
    hidden = []
    for g_ref, u_ref in ((g0_ref, u0_ref), (g1_ref, u1_ref)):
        gate = jnp.minimum(dot(x_ref[...], g_ref[...]), CLAMP_LIMIT)
        up = jnp.clip(dot(x_ref[...], u_ref[...]), -CLAMP_LIMIT, CLAMP_LIMIT)
        unit = gate * (1.0 / (1.0 + jnp.exp(-SIGMOID_SCALE * gate))) * (up + 1.0)
        hidden.append(unit.astype(BF16))
    for g in range(0, N_TP, 2):
        cols = slice(g * LANES, (g + 2) * LANES)
        part = dot(hidden[0], d0_ref[:, cols]) + dot(hidden[1], d1_ref[:, cols])
        part = part.astype(BF16)
        out_ref[g] = part[:, :LANES]
        out_ref[g + 1] = part[:, LANES:]


def gather_body(in_ref, widen_ref, out_ref):
    for c in range(2):
        total = in_ref[c].astype(F32)
        for y in range(1, N_Y):
            total = total + in_ref[y * 2 + c].astype(F32)
        rows = dot(widen_ref[...], total.astype(BF16)).astype(BF16)
        out_ref[c * 16 * CAP_PAD : (c + 1) * 16 * CAP_PAD, :] = rows


def finish_body(in_ref, mix_ref, mixed_ref, out_ref):
    total = mixed_ref[...]
    rows = in_ref[...]
    for i in range(3):
        total = total + dot(mix_ref[i].astype(BF16), rows, 0, 0)
    out_ref[...] = total.astype(BF16)


def shaped(shape, dtype=BF16):
    return jax.ShapeDtypeStruct(shape, dtype)


VMEM = pl.BlockSpec(memory_space=pltpu.VMEM)
SMEM = pl.BlockSpec(memory_space=pltpu.SMEM)


def call(body, outs, *args, scratch=(), name=None):
    specs = [SMEM if a.shape == (1,) else VMEM for a in args]
    many = isinstance(outs, (list, tuple))
    return pl.pallas_call(
        body,
        out_shape=outs,
        in_specs=specs,
        out_specs=[VMEM] * len(outs) if many else VMEM,
        scratch_shapes=list(scratch),
        name=name,
        compiler_params=pltpu.CompilerParams(vmem_limit_bytes=48 * 1024 * 1024),
    )(*args)


def exchange(x, axes):
    return lax.all_to_all(x, axes, 0, 0, tiled=True)


def partner(x):
    return lax.ppermute(x, "c", [(0, 1), (1, 0)])


def per_device(
    queries,
    keys,
    values,
    docs,
    query_gain,
    key_gain,
    out_weight,
    residual,
    norm_gain,
    routes,
    route_weight,
    gate_weight,
    up_weight,
    down_weight,
):
    row_tab, col_tab = tables()
    drop = compaction()
    block = (lax.axis_index("z") * N_X + lax.axis_index("x")).reshape(1).astype(jnp.int32)
    core = lax.axis_index("c").reshape(1).astype(jnp.int32)
    qs, kvs = call(
        prep_body,
        [shaped((N_X, TOK + NOTE, LANES)), shaped((N_Z, TOK + NOTE, LANES))],
        block,
        queries,
        keys.T,
        values.T,
        docs.reshape(2, LANES),
        query_gain.reshape(1, HD),
        key_gain.reshape(1, HD),
        jnp.asarray(row_tab),
        jnp.asarray(col_tab),
        name="prep",
    )
    kv_all = exchange(kvs, "z")
    q_all = exchange(qs, "x")
    gain_all = exchange(jnp.broadcast_to(norm_gain[None, None, :], (N_TP, 8, LANES)), ("y", "c"))
    gate, up, down = gate_weight[0], up_weight[0], down_weight[0]
    out_other = partner(out_weight)
    gate_o, up_o, down_o = partner(gate), partner(up), partner(down)
    place, mix = call(
        route_body,
        [shaped((EXPERTS * CAP_PAD, TOK), F32), shaped((3, EXPERTS * CAP_PAD, TOK), F32)],
        routes.T,
        route_weight.T,
        name="route",
    )
    partial = call(
        attend_body,
        shaped((N_X * 2, HALF + NOTE, LANES)),
        q_all,
        kv_all,
        scratch=[pltpu.VMEM((N_Z * TOK, LANES), BF16), pltpu.VMEM((N_Z * TOK, LANES), BF16)],
        name="attend",
    )
    partial = exchange(partial, ("x", "c"))
    projected = call(
        project_body,
        shaped((N_TP, HALF, LANES)),
        core,
        partial,
        out_weight,
        out_other,
        name="project",
    )
    projected = exchange(projected, ("y", "c"))
    mixed, outgoing = call(
        dispatch_body,
        [shaped((TOK, LANES), F32), shaped((EXPERTS * CAP_PAD, LANES))],
        projected,
        residual,
        place,
        name="dispatch",
    )
    arrived = exchange(outgoing.reshape(N_SP, CAP_PAD, LANES), ("z", "x"))
    spread = call(
        spread_body,
        shaped((N_TP, ROWS, LANES)),
        arrived.reshape(N_SP * CAP_PAD, LANES),
        jnp.asarray(drop, BF16),
        name="spread",
    )
    columns = exchange(spread, ("y", "c"))
    parts = call(
        expert_body,
        shaped((N_TP, ROWS, LANES)),
        columns,
        gain_all,
        gate,
        gate_o,
        up,
        up_o,
        down,
        down_o,
        scratch=[pltpu.VMEM((ROWS, D), BF16)],
        name="expert",
    )
    parts = exchange(parts, ("y", "c"))
    expert_out = call(
        gather_body,
        shaped((N_SP * CAP_PAD, LANES)),
        parts,
        jnp.asarray(drop.T, BF16),
        name="gather",
    )
    returned = exchange(expert_out.reshape(N_SP, CAP_PAD, LANES), ("z", "x"))
    return call(
        finish_body,
        shaped((TOK, LANES)),
        returned.reshape(N_SP * CAP_PAD, LANES),
        mix,
        mixed,
        name="finish",
    )


def solution(mesh):
    grid = Mesh(mesh.devices.reshape(N_Z, N_X, N_Y, N_C), ("z", "x", "y", "c"))
    sp, tp = ("z", "x"), ("y", "c")
    in_specs = (
        P(sp, tp),
        P(sp, tp),
        P(sp, tp),
        P(sp),
        P(),
        P(),
        P(tp, None),
        P(sp, tp),
        P(tp),
        P(sp, None),
        P(sp, None),
        P(sp, None, tp),
        P(sp, None, tp),
        P(sp, tp, None),
    )
    return jax.shard_map(
        per_device, mesh=grid, in_specs=in_specs, out_specs=P(sp, tp), check_vma=False
    )
```

time: 355 us -> 224 us (0.63)
  waiting for transfers between devices: 219 us -> 65.8 us
  blocking collectives: 17.9 us -> 76.7 us
  matrix products: 33.4 us -> 0 us
  Pallas kernels: 0 us -> 20.6 us
  other arithmetic: 16.7 us -> 0 us
  starting transfers between devices: 29.3 us -> 43.8 us
  between operations: 13.9 us -> 0.15 us
  local copies, waits for them, and re-layouts: 22.1 us -> 15.7 us
    all_gather x2 -> x0, waiting for transfers between devices: 118 us -> none  [the longest x1 80.9 us: sent_together(): lax.all_gather(both, axis, axis=dim, tiled=True)]
    all_to_all x1 -> x4, blocking collectives: 17.9 us -> 76.7 us  [exchange(): return lax.all_to_all(x, axes, 0, 0, tiled=True)]
    all_to_all x4 -> x5, waiting for transfers between devices: 101 us -> 65 us  [exchange(): return lax.all_to_all(x, axes, 0, 0, tiled=True)]
    dot_general x12 -> x0, matrix products: 33.4 us -> none  [the longest x4 14.5 us: softmax_update(): jnp.einsum('tkgd,pkd->tkgp', query_rot, key_block, preferred_element_type...]
    pallas_call x0 -> x9, Pallas kernels: none -> 20.6 us  [call(): pl.pallas_call(body, out_shape=outs, in_specs=specs, out_specs=[VMEM] * l...]
    ppermute x0 -> x4, starting transfers between devices: none -> 10.7 us  [partner(): return lax.ppermute(x, 'c', [(0, 1), (1, 0)])]
    unnamed x23 -> x52, local copies, waits for them, and re-layouts: 4.44 us -> 15.1 us
    reduce_sum x13 -> x0, other arithmetic: 8.69 us -> none  [the longest x4 4.44 us: softmax_update(): denominator = denominator * factor + jnp.sum(weights, axis=-1)]
  transfers between devices with their start and end apart: 6 -> 9, of which waited for: 6 -> 6; matrix products, arithmetic and copies ran while one was open for 2% -> 0% of each run, Pallas kernels for 0% -> 5%
where the time goes in v1:
time: 224 us; the launch traced here: 223 us
  blocking collectives  76.7 us (34%)
  waiting for transfers between devices  65.8 us (29%)
  starting transfers between devices  43.8 us (20%)
  Pallas kernels  20.6 us (9%)
  local copies, waits for them, and re-layouts  15.7 us (7%)
    all_to_all x4, blocking collectives, exchange(): return lax.all_to_all(x, axes, 0, 0, tiled=True)  76.7 us
    all_to_all x5, waiting for transfers between devices, exchange(): return lax.all_to_all(x, axes, 0, 0, tiled=True)  65 us
    all_to_all x5, starting transfers between devices, exchange(): return lax.all_to_all(x, axes, 0, 0, tiled=True)  33.1 us
    pallas_call x9, Pallas kernels, call(): pl.pallas_call(body, out_shape=outs, in_specs=specs, out_specs=[VMEM] * l...  20.6 us
    unnamed x52, local copies, waits for them, and re-layouts  15.1 us
    ppermute x4, starting transfers between devices, partner(): return lax.ppermute(x, 'c', [(0, 1), (1, 0)])  10.7 us
  transfers between devices with their start and end apart: 9, of which 6 were waited for; matrix products, arithmetic and copies ran while one was open for 0% of the time, Pallas kernels for 5%

profile of v1, /device:TPU:1, one launch (start us, length us, event | category | flops | bytes accessed | tf_op | source)
XLA Modules:
  0.0 222.8 jit_solution(6278711829876623596)
XLA Ops:
  0.0 1.0 copy-done.12
  6.2 1.3 prep.1
  7.5 10.2 %all_to_all.45.q_ref = bf16[4,272,128]{2,1,0:T(8,128)(2,1)S(1)} all-to-all(bf16[4,272,128]{2,1,0:T(8,128)(2,1)S(1)} %get-tuple-element.11), channel_id=1, replica_groups=mesh['z'=8,'x'=4,'y'=8,'c'=2] {'x'}, dimensions={0} | all-to-all | bytes 557056 | tf_op jit(solution)/shard_map/all_to_all | solution.py:291
  17.7 10.1 %all-to-all-start.1 = ((bf16[8,272,128]{2,1,0:T(8,128)(2,1)}), bf16[8,272,128]{2,1,0:T(8,128)(2,1)S(1)}, u32[]{:S(2)}, u32[]{:S(2)}) async-start(bf16[8,272,128]{2,1,0:T(8,128)(2,1)} %get-tuple-element.12), calls=%async_computation.1 | async-start | bytes 1114112 | tf_op jit(solution)/shard_map/all_to_all | solution.py:291
  27.8 4.3 %collective-permute-start = (bf16[128,2048]{1,0:T(8,128)(2,1)S(1)}, bf16[128,2048]{1,0:T(8,128)(2,1)S(1)}, u32[]{:S(2)}, u32[]{:S(2)}) collective-permute-start(bf16[128,2048]{1,0:T(8,128)(2,1)S(1)} %copy-done.9), channel_id=1, source_target_pairs={{0,1},{1,0},{2,3},{3,2},{4,5},{5,4},{6,7},{7,6},{8,9},{9,8},{10,11... | collective-permute-start | bytes 1572872 | tf_op jit(solution)/shard_map/ppermute | solution.py:295
  32.1 11.9 %all-to-all-done.1.kv_ref = bf16[8,272,128]{2,1,0:T(8,128)(2,1)S(1)} async-done(((bf16[8,272,128]{2,1,0:T(8,128)(2,1)}), bf16[8,272,128]{2,1,0:T(8,128)(2,1)S(1)}, u32[]{:S(2)}, u32[]{:S(2)}) %all-to-all-start.1) | async-done | bytes 557088 | tf_op jit(solution)/shard_map/all_to_all | solution.py:291
  44.0 8.8 %attend.1 = bf16[8,144,128]{2,1,0:T(8,128)(2,1)} custom-call(bf16[4,272,128]{2,1,0:T(8,128)(2,1)S(1)} %all_to_all.45.q_ref, bf16[8,272,128]{2,1,0:T(8,128)(2,1)S(1)} %all-to-all-done.1.kv_ref), custom_call_target="tpu_custom_call" | custom-call | tf_op jit(solution)/shard_map/attend/pallas_call | solution.py:279
  52.8 6.3 %all-to-all-start.2 = ((bf16[8,144,128]{2,1,0:T(8,128)(2,1)}), bf16[8,144,128]{2,1,0:T(8,128)(2,1)S(1)}, u32[]{:S(2)}, u32[]{:S(2)}) async-start(bf16[8,144,128]{2,1,0:T(8,128)(2,1)} %attend.1), calls=%async_computation.2 | async-start | bytes 589824 | tf_op jit(solution)/shard_map/all_to_all | solution.py:291
  59.1 6.8 %all-to-all-done.2.in_ref = bf16[8,144,128]{2,1,0:T(8,128)(2,1)S(1)} async-done(((bf16[8,144,128]{2,1,0:T(8,128)(2,1)}), bf16[8,144,128]{2,1,0:T(8,128)(2,1)S(1)}, u32[]{:S(2)}, u32[]{:S(2)}) %all-to-all-start.2) | async-done | bytes 294944 | tf_op jit(solution)/shard_map/all_to_all | solution.py:291
  65.9 1.6 project.1
  67.5 8.3 %all-to-all-start.3 = ((bf16[16,128,128]{2,1,0:T(8,128)(2,1)}), bf16[16,128,128]{2,1,0:T(8,128)(2,1)S(1)}, u32[]{:S(2)}, u32[]{:S(2)}) async-start(bf16[16,128,128]{2,1,0:T(8,128)(2,1)} %project.1), calls=%async_computation.3 | async-start | bytes 1048576 | tf_op jit(solution)/shard_map/all_to_all | solution.py:291
  77.1 15.9 %all-to-all-done.3.in_ref = bf16[16,128,128]{2,1,0:T(8,128)(2,1)S(1)} async-done(((bf16[16,128,128]{2,1,0:T(8,128)(2,1)}), bf16[16,128,128]{2,1,0:T(8,128)(2,1)S(1)}, u32[]{:S(2)}, u32[]{:S(2)}) %all-to-all-start.3) | async-done | bytes 524320 | tf_op jit(solution)/shard_map/all_to_all | solution.py:291
  93.0 1.1 copy-done.8
  94.5 14.2 %all_to_all.46 = bf16[32,24,128]{2,1,0:T(8,128)(2,1)S(1)} all-to-all(bf16[32,24,128]{2,1,0:T(8,128)(2,1)S(1)} %bitcast.25), channel_id=1, replica_groups=mesh['z'=8,'x'=4,'y'=8,'c'=2] {'z','x'}, dimensions={0} | all-to-all | bytes 393216 | tf_op jit(solution)/shard_map/all_to_all | solution.py:291
  109.4 4.1 %all-to-all-start.6 = ((f32[16,8,128]{2,1,0:T(8,128)}), f32[16,8,128]{2,1,0:T(8,128)S(1)}, u32[]{:S(2)}, u32[]{:S(2)}) async-start(f32[16,8,128]{2,1,0:T(8,128)} %broadcast_in_dim.2), calls=%async_computation.6 | async-start | bytes 131072 | tf_op jit(solution)/shard_map/all_to_all | solution.py:291
  113.4 1.4 spread.1
  114.8 6.4 %all-to-all-done.6.gain_ref = f32[16,8,128]{2,1,0:T(8,128)S(1)} async-done(((f32[16,8,128]{2,1,0:T(8,128)}), f32[16,8,128]{2,1,0:T(8,128)S(1)}, u32[]{:S(2)}, u32[]{:S(2)}) %all-to-all-start.6) | async-done | bytes 65568 | tf_op jit(solution)/shard_map/all_to_all | solution.py:291
  121.2 4.3 %all-to-all-start.5 = ((bf16[16,320,128]{2,1,0:T(8,128)(2,1)}), bf16[16,320,128]{2,1,0:T(8,128)(2,1)}, u32[]{:S(2)}, u32[]{:S(2)}) async-start(bf16[16,320,128]{2,1,0:T(8,128)(2,1)} %spread.1), calls=%async_computation.5 | async-start | bytes 2621440 | tf_op jit(solution)/shard_map/all_to_all | solution.py:291
  125.5 2.1 collective-permute-start.1
  127.6 2.2 collective-permute-start.2
  129.8 2.1 collective-permute-start.3
  132.0 0.9 copy-done.3
  133.0 1.0 copy-done.5
  134.7 24.1 %all-to-all-done.5.in_ref = bf16[16,320,128]{2,1,0:T(8,128)(2,1)} async-done(((bf16[16,320,128]{2,1,0:T(8,128)(2,1)}), bf16[16,320,128]{2,1,0:T(8,128)(2,1)}, u32[]{:S(2)}, u32[]{:S(2)}) %all-to-all-start.5) | async-done | bytes 1310752 | tf_op jit(solution)/shard_map/all_to_all | solution.py:291
  158.8 1.2 copy-done.1
  160.1 1.2 copy-done.2
  161.3 1.2 copy-done.4
  162.5 1.2 copy-done.6
  163.7 5.3 %expert.1 = bf16[16,320,128]{2,1,0:T(8,128)(2,1)} custom-call(bf16[16,320,128]{2,1,0:T(8,128)(2,1)} %all-to-all-done.5.in_ref, f32[16,8,128]{2,1,0:T(8,128)S(1)} %all-to-all-done.6.gain_ref, bf16[2048,256]{1,0:T(8,128)(2,1)S(1)} %bitcast.17, bf16[2048,256]{1,0:T(8,128)(2,1)S(1)} %copy-done.4, bf16[2048,256]{1,0:T(8,128)(2,1)S(1)} %bitcast.19, ...), custom_call_target="tpu_custom_call" | custom-call | tf_op jit(solution)/shard_map/expert/pallas_call | solution.py:279
  169.0 38.0 %all_to_all.47.in_ref = bf16[16,320,128]{2,1,0:T(8,128)(2,1)S(1)} all-to-all(bf16[16,320,128]{2,1,0:T(8,128)(2,1)} %expert.1), channel_id=1, replica_groups=mesh['z'=8,'x'=4,'y'=8,'c'=2] {'y','c'}, dimensions={0} | all-to-all | bytes 2621440 | tf_op jit(solution)/shard_map/all_to_all | solution.py:291
  207.4 14.2 %all_to_all.48 = bf16[32,24,128]{2,1,0:T(8,128)(2,1)S(1)} all-to-all(bf16[32,24,128]{2,1,0:T(8,128)(2,1)S(1)} %bitcast.22), channel_id=1, replica_groups=mesh['z'=8,'x'=4,'y'=8,'c'=2] {'z','x'}, dimensions={0} | all-to-all | bytes 393216 | tf_op jit(solution)/shard_map/all_to_all | solution.py:291
  221.6 1.1 finish.1
  (52 shorter events, 8.7 us)
Async XLA Ops:
  0.0 27.8 %copy-start.9 = (bf16[128,2048]{1,0:T(8,128)(2,1)S(1)}, bf16[128,2048]{1,0:T(8,128)(2,1)}, u32[]{:S(2)}) copy-start(bf16[128,2048]{1,0:T(8,128)(2,1)} %w_own_ref.1) | copy-start | bytes 1572868
  0.0 1.0 copy-start.12
  1.0 0.8 copy-start.15
  1.8 0.8 copy-start.16
  2.6 0.8 copy-start.18
  3.4 0.8 copy-start.19
  17.7 26.3 %all-to-all-start.1 = ((bf16[8,272,128]{2,1,0:T(8,128)(2,1)}), bf16[8,272,128]{2,1,0:T(8,128)(2,1)S(1)}, u32[]{:S(2)}, u32[]{:S(2)}) async-start(bf16[8,272,128]{2,1,0:T(8,128)(2,1)} %get-tuple-element.12), calls=%async_computation.1 | async-start | bytes 1114112 | tf_op jit(solution)/shard_map/all_to_all | solution.py:291
  27.8 31.3 %collective-permute-start = (bf16[128,2048]{1,0:T(8,128)(2,1)S(1)}, bf16[128,2048]{1,0:T(8,128)(2,1)S(1)}, u32[]{:S(2)}, u32[]{:S(2)}) collective-permute-start(bf16[128,2048]{1,0:T(8,128)(2,1)S(1)} %copy-done.9), channel_id=1, source_target_pairs={{0,1},{1,0},{2,3},{3,2},{4,5},{5,4},{6,7},{7,6},{8,9},{9,8},{10,11... | collective-permute-start | bytes 1572872 | tf_op jit(solution)/shard_map/ppermute | solution.py:295
  52.8 13.1 %all-to-all-start.2 = ((bf16[8,144,128]{2,1,0:T(8,128)(2,1)}), bf16[8,144,128]{2,1,0:T(8,128)(2,1)S(1)}, u32[]{:S(2)}, u32[]{:S(2)}) async-start(bf16[8,144,128]{2,1,0:T(8,128)(2,1)} %attend.1), calls=%async_computation.2 | async-start | bytes 589824 | tf_op jit(solution)/shard_map/all_to_all | solution.py:291
  65.9 9.9 %copy-start.20 = (s32[256,2]{0,1:T(2,128)S(1)}, s32[256,2]{0,1:T(2,128)}, u32[]{:S(2)}) copy-start(s32[256,2]{0,1:T(2,128)} %param.27) | copy-start | bytes 6148
  65.9 9.9 %copy-start.21 = (f32[256,2]{0,1:T(2,128)S(1)}, f32[256,2]{0,1:T(2,128)}, u32[]{:S(2)}) copy-start(f32[256,2]{0,1:T(2,128)} %param.28) | copy-start | bytes 6148
  65.9 27.1 %copy-start.17 = (bf16[256,128]{1,0:T(8,128)(2,1)S(1)}, bf16[256,128]{1,0:T(8,128)(2,1)}, u32[]{:S(2)}) copy-start(bf16[256,128]{1,0:T(8,128)(2,1)} %residual_ref.1) | copy-start | bytes 196612
  67.5 41.2 %copy-start.25 = (f32[128]{0:T(128)S(1)}, f32[128]{0:T(128)}, u32[]{:S(2)}) copy-start(f32[128]{0:T(128)} %param.26) | copy-start | bytes 1540
  67.5 45.9 %copy-start.11 = (bf16[320,384]{1,0:T(8,128)(2,1)S(1)}, bf16[320,384]{1,0:T(8,128)(2,1)}, u32[]{:S(2)}) copy-start(bf16[320,384]{1,0:T(8,128)(2,1)} %constant.28.clone.drop_ref) | copy-start | bytes 737284
  67.5 25.5 %all-to-all-start.3 = ((bf16[16,128,128]{2,1,0:T(8,128)(2,1)}), bf16[16,128,128]{2,1,0:T(8,128)(2,1)S(1)}, u32[]{:S(2)}, u32[]{:S(2)}) async-start(bf16[16,128,128]{2,1,0:T(8,128)(2,1)} %project.1), calls=%async_computation.3 | async-start | bytes 1048576 | tf_op jit(solution)/shard_map/all_to_all | solution.py:291
  76.2 0.9 copy-start.7
  93.0 1.1 copy-start.8
  94.5 14.2 %copy-start.13 = (f32[256,128]{1,0:T(8,128)}, f32[256,128]{1,0:T(8,128)S(1)}, u32[]{:S(2)}) copy-start(f32[256,128]{1,0:T(8,128)S(1)} %get-tuple-element.16.mixed_ref) | copy-start | bytes 393220
  109.4 11.8 %all-to-all-start.6 = ((f32[16,8,128]{2,1,0:T(8,128)}), f32[16,8,128]{2,1,0:T(8,128)S(1)}, u32[]{:S(2)}, u32[]{:S(2)}) async-start(f32[16,8,128]{2,1,0:T(8,128)} %broadcast_in_dim.2), calls=%async_computation.6 | async-start | bytes 131072 | tf_op jit(solution)/shard_map/all_to_all | solution.py:291
  114.8 10.7 %copy-start = (bf16[1,2048,256]{2,1,0:T(8,128)(2,1)S(1)}, bf16[1,2048,256]{2,1,0:T(8,128)(2,1)}, u32[]{:S(2)}) copy-start(bf16[1,2048,256]{2,1,0:T(8,128)(2,1)} %param.29) | copy-start | bytes 3145732
  121.2 37.6 %all-to-all-start.5 = ((bf16[16,320,128]{2,1,0:T(8,128)(2,1)}), bf16[16,320,128]{2,1,0:T(8,128)(2,1)}, u32[]{:S(2)}, u32[]{:S(2)}) async-start(bf16[16,320,128]{2,1,0:T(8,128)(2,1)} %spread.1), calls=%async_computation.5 | async-start | bytes 2621440 | tf_op jit(solution)/shard_map/all_to_all | solution.py:291
  125.5 6.5 %collective-permute-start.1 = (bf16[2048,256]{1,0:T(8,128)(2,1)S(1)}, bf16[2048,256]{1,0:T(8,128)(2,1)S(1)}, u32[]{:S(2)}, u32[]{:S(2)}) collective-permute-start(bf16[2048,256]{1,0:T(8,128)(2,1)S(1)} %bitcast.16), channel_id=1, source_target_pairs={{0,1},{1,0},{2,3},{3,2},{4,5},{5,4},{6,7},{7,6},{8,9},{9,8},{10,11... | collective-permute-start | bytes 3145736 | tf_op jit(solution)/shard_map/ppermute | solution.py:295
  127.6 5.3 %collective-permute-start.2 = (bf16[2048,256]{1,0:T(8,128)(2,1)}, bf16[2048,256]{1,0:T(8,128)(2,1)S(1)}, u32[]{:S(2)}, u32[]{:S(2)}) collective-permute-start(bf16[2048,256]{1,0:T(8,128)(2,1)} %bitcast.18), channel_id=1, source_target_pairs={{0,1},{1,0},{2,3},{3,2},{4,5},{5,4},{6,7},{7,6},{8,9},{9,8},{10,11... | collective-permute-start | bytes 3145736 | tf_op jit(solution)/shard_map/ppermute | solution.py:295
  129.8 4.9 %collective-permute-start.3 = (bf16[256,2048]{1,0:T(8,128)(2,1)}, bf16[256,2048]{1,0:T(8,128)(2,1)}, u32[]{:S(2)}, u32[]{:S(2)}) collective-permute-start(bf16[256,2048]{1,0:T(8,128)(2,1)} %bitcast.20), channel_id=1, source_target_pairs={{0,1},{1,0},{2,3},{3,2},{4,5},{5,4},{6,7},{7,6},{8,9},{9,8},{10,11... | collective-permute-start | bytes 3145736 | tf_op jit(solution)/shard_map/ppermute | solution.py:295
  132.0 1.0 copy-start.3
  133.0 1.0 copy-start.5
  158.8 1.2 copy-start.1
  160.1 1.2 copy-start.2
  161.3 1.2 copy-start.4
  162.5 1.2 copy-start.6
  169.0 38.0 %copy-start.10 = (bf16[384,320]{1,0:T(8,128)(2,1)S(1)}, bf16[384,320]{1,0:T(8,128)(2,1)}, u32[]{:S(2)}) copy-start(bf16[384,320]{1,0:T(8,128)(2,1)} %constant.29.clone.widen_ref) | copy-start | bytes 737284
  207.0 14.6 %copy-start.14 = (f32[256,128]{1,0:T(8,128)S(1)}, f32[256,128]{1,0:T(8,128)}, u32[]{:S(2)}) copy-start(f32[256,128]{1,0:T(8,128)} %copy-done.13) | copy-start | bytes 393220
  (3 other events, 2.0 us)

commit v2 on v1

--- a/solution.py
+++ b/solution.py
@@ -7,6 +7,7 @@
 from jax.experimental import pallas as pl
 from jax.experimental.pallas import tpu as pltpu
 from jax.sharding import Mesh, PartitionSpec as P
+
 
 GRID_W = 64
 EPSILON = 1e-06
@@ -23,8 +24,9 @@
 EXPERTS = 32
 CAP = 20
 CAP_PAD = 24
-ROWS = N_SP * CAP // 2
-HID = 256
+PIECES = 1
+ROWS = N_SP * CAP // (2 * PIECES)
+BLOCKS = N_SP // (2 * PIECES)
 NOTE = 16
 MASK_BIG = 16384.0
 
@@ -53,7 +55,7 @@
 
 
 def compaction():
-    out = np.zeros((ROWS, 16 * CAP_PAD), np.float32)
+    out = np.zeros((ROWS, BLOCKS * CAP_PAD), np.float32)
     r = np.arange(ROWS)
     out[r, (r // CAP) * CAP_PAD + r % CAP] = 1.0
     return out
@@ -67,11 +69,21 @@
     return lax.broadcasted_iota(jnp.int32, shape, dim)
 
 
-def prep_body(blk, q_ref, k_ref, v_ref, docs_ref, qg_ref, kg_ref, row_ref, col_ref, qs_ref, kvs_ref):
+def prep_body(blk, *refs):
+    sources, (qs_ref, kvs_ref), kept, sems = refs[:8], refs[8:10], refs[10:18], refs[18]
+    copies = []
+    for i, (src, dst) in enumerate(zip(sources, kept)):
+        src = src.at[blk[0]] if i == 6 else src
+        copies.append(pltpu.make_async_copy(src, dst, sems.at[i]))
+    for copy in copies:
+        copy.start()
+    for copy in copies:
+        copy.wait()
+    q_ref, k_ref, v_ref, docs_ref, qg_ref, kg_ref, row_ref, col_ref = kept
     lane = iota((TOK, LANES), 1)
     low = lane < HD
     even = (lane & 1) == 0
-    rows = row_ref[blk[0]]
+    rows = row_ref[...]
     per = TOK // GRID_W
     cos_t = jnp.concatenate([col_ref[0] + rows[j : j + 1] for j in range(per)], axis=0)
     sin_t = jnp.concatenate([col_ref[1] + rows[per + j : per + j + 1] for j in range(per)], axis=0)
@@ -100,9 +112,8 @@
     n1 = jnp.sum((docs < 2).astype(F32))
     row = iota((NOTE, LANES), 0)
     note = jnp.where(row == 0, n0, jnp.where(row == 1, n1, 0.0)).astype(BF16)
-    for i in range(N_X):
-        qs_ref[i, :TOK, :] = q_out
-        qs_ref[i, TOK:, :] = note
+    qs_ref[:TOK, :] = q_out
+    qs_ref[TOK:, :] = note
     for i in range(N_Z):
         kvs_ref[i, :TOK, :] = kv_out
         kvs_ref[i, TOK:, :] = note
@@ -114,7 +125,10 @@
     return hi, mid, x - hi - mid
 
 
-def attend_body(q_ref, kv_ref, out_ref, kp_ref, vp_ref):
+def attend_body(spot, *refs):
+    q_refs, (kv_ref, out_ref, q_ref, kp_ref, vp_ref) = refs[:N_X], refs[N_X:]
+    for i in range(N_X):
+        q_ref[i] = q_refs[i][...]
     lane = iota((TOK, LANES), 1)
     low = lane < HD
     idx = iota((TOK, LANES), 0).astype(F32)
@@ -156,14 +170,16 @@
             for i, part in enumerate(parts):
                 stat = jnp.where(lane_h == i, part[rows], stat)
             stat_t = dot(stat.astype(BF16), eye, 0, 0)
-            out_ref[b * 2 + half, :HALF, :] = o[rows]
-            out_ref[b * 2 + half, HALF:, :] = stat_t[:NOTE].astype(BF16)
+            to = lax.rem(spot[0] + N_X - b, N_X) * 2 + half
+            out_ref[to, :HALF, :] = o[rows]
+            out_ref[to, HALF:, :] = stat_t[:NOTE].astype(BF16)
         return carry
 
     lax.fori_loop(0, N_X, block, 0)
 
 
-def project_body(core, in_ref, w_own_ref, w_other_ref, out_ref):
+def project_body(core, in_ref, w_own_ref, w_other_ref, gain_ref, out_ref):
+    gain = split3(gain_ref[...])
     row = iota((NOTE, LANES), 0)
     lane = iota((NOTE, LANES), 1)
     pick = (((row < 3) & (lane < HD)) | ((row >= 3) & (row < 6) & (lane >= HD))).astype(BF16)
@@ -179,53 +195,83 @@
             mixed = mixed + w * in_ref[x * 2 + c, :HALF, :].astype(F32)
         return (mixed / total).astype(BF16)
 
+    note = jnp.where(row == 0, gain[0], jnp.where(row == 1, gain[1], jnp.where(row == 2, gain[2], 0.0)))
     own = attended(core[0])
     other = attended(1 - core[0])
     for g in range(N_TP):
         cols = slice(g * LANES, (g + 1) * LANES)
         part = dot(own, w_own_ref[:, cols]) + dot(other, w_other_ref[:, cols])
-        out_ref[g] = part.astype(BF16)
-
-
-def route_body(routes_ref, weight_ref, place_ref, mix_ref):
+        out_ref[g, :HALF, :] = part.astype(BF16)
+        out_ref[g, HALF:, :] = note.astype(BF16)
+
+
+def slots_of(routes_ref):
     expert = iota((EXPERTS, TOK), 0)
     r0, r1 = routes_ref[0:1, :], routes_ref[1:2, :]
     named = ((expert == r0) | (expert == r1)).astype(F32)
     before = (iota((TOK, TOK), 0) < iota((TOK, TOK), 1)).astype(BF16)
     slot = dot(named.astype(BF16), before)
-    weight = jnp.where(expert == r0, weight_ref[0:1, :], jnp.where(expert == r1, weight_ref[1:2, :], 0.0))
-    slot = jnp.where(named > 0.0, slot, -1.0)
-    w3 = split3(weight)
+    return expert == r0, expert == r1, jnp.where(named > 0.0, slot, -1.0)
+
+
+def laid_out(slot, value, write):
     slots = iota((CAP_PAD, TOK), 0).astype(F32)
-    for e in range(EXPERTS):
-        rows = slice(e * CAP_PAD, (e + 1) * CAP_PAD)
-        hit = slots == slot[e : e + 1, :]
-        place_ref[rows, :] = hit.astype(F32)
-        for i in range(3):
-            mix_ref[i, rows, :] = jnp.where(hit, w3[i][e : e + 1, :], 0.0)
-
-
-def dispatch_body(in_ref, residual_ref, place_ref, mixed_ref, out_ref):
+    for e in range(0, EXPERTS, 2):
+        both = [jnp.where(slots == slot[i : i + 1, :], value(i), 0.0) for i in (e, e + 1)]
+        write(slice(e * CAP_PAD, (e + 2) * CAP_PAD), jnp.concatenate(both, axis=0).astype(BF16))
+
+
+def route_body(routes_ref, place_ref):
+    _, _, slot = slots_of(routes_ref)
+
+    def write(rows, value):
+        place_ref[rows, :] = value
+
+    laid_out(slot, lambda e: 1.0, write)
+
+
+def mix_body(term, routes_ref, weight_ref, mix_ref):
+    first, second, slot = slots_of(routes_ref)
+    weight = jnp.where(first, weight_ref[0:1, :], jnp.where(second, weight_ref[1:2, :], 0.0))
+    part = split3(weight)[term]
+
+    def write(rows, value):
+        mix_ref[rows, :] = value
+
+    laid_out(slot, lambda e: part[e : e + 1, :], write)
+
+
+def dispatch_body(in_ref, residual_ref, place_ref, mixed_ref, gain_ref, out_ref):
     halves = []
     for c in range(2):
-        total = in_ref[c].astype(F32)
+        total = in_ref[c, :HALF, :].astype(F32)
         for y in range(1, N_Y):
-            total = total + in_ref[y * 2 + c].astype(F32)
+            total = total + in_ref[y * 2 + c, :HALF, :].astype(F32)
         halves.append(total)
+    for g in range(N_TP):
+        note = in_ref[g, HALF:, :].astype(F32)
+        gain = note[0:1] + note[1:2] + note[2:3]
+        gain_ref[g] = jnp.broadcast_to(gain, (8, LANES))
     mixed = residual_ref[...].astype(F32) + jnp.concatenate(halves, axis=0)
     mixed_ref[...] = mixed
-    out_ref[...] = dot(place_ref[...].astype(BF16), mixed.astype(BF16)).astype(BF16)
-
-
-def spread_body(in_ref, drop_ref, out_ref):
+    out_ref[...] = dot(place_ref[...], mixed.astype(BF16)).astype(BF16)
+
+
+def spread_body(in_ref, drop_ref, *out_refs):
+    span = BLOCKS * CAP_PAD
     for c in range(2):
-        rows = in_ref[c * 16 * CAP_PAD : (c + 1) * 16 * CAP_PAD, :]
-        kept = dot(drop_ref[...], rows).astype(BF16)
-        for y in range(N_Y):
-            out_ref[y * 2 + c] = kept
-
-
-def expert_body(in_ref, gain_ref, g0_ref, g1_ref, u0_ref, u1_ref, d0_ref, d1_ref, out_ref, x_ref):
+        for i, out_ref in enumerate(out_refs):
+            at = (c * PIECES + i) * span
+            kept = dot(drop_ref[...], in_ref[at : at + span, :]).astype(BF16)
+            for y in range(N_Y):
+                out_ref[y * 2 + c] = kept
+
+
+def expert_body(in_ref, gain_ref, *refs):
+    far, (out_ref, x_ref), weights, sems = refs[:6], refs[6:8], refs[8:14], refs[14]
+    copies = [pltpu.make_async_copy(far[i], weights[i], sems.at[i]) for i in range(6)]
+    for copy in copies:
+        copy.start()
     total = jnp.zeros((ROWS, LANES), F32)
     for g in range(N_TP):
         x = in_ref[g].astype(F32)
@@ -235,33 +281,41 @@
         x = in_ref[g].astype(F32) * scale * gain_ref[g, 0:1, :]
         x_ref[:, g * LANES : (g + 1) * LANES] = x.astype(BF16)
     hidden = []
-    for g_ref, u_ref in ((g0_ref, u0_ref), (g1_ref, u1_ref)):
-        gate = jnp.minimum(dot(x_ref[...], g_ref[...]), CLAMP_LIMIT)
-        up = jnp.clip(dot(x_ref[...], u_ref[...]), -CLAMP_LIMIT, CLAMP_LIMIT)
+    for i in range(2):
+        copies[2 * i].wait()
+        gate = jnp.minimum(dot(x_ref[...], weights[2 * i][...]), CLAMP_LIMIT)
+        copies[2 * i + 1].wait()
+        up = jnp.clip(dot(x_ref[...], weights[2 * i + 1][...]), -CLAMP_LIMIT, CLAMP_LIMIT)
         unit = gate * (1.0 / (1.0 + jnp.exp(-SIGMOID_SCALE * gate))) * (up + 1.0)
         hidden.append(unit.astype(BF16))
+    copies[4].wait()
+    copies[5].wait()
     for g in range(0, N_TP, 2):
         cols = slice(g * LANES, (g + 2) * LANES)
-        part = dot(hidden[0], d0_ref[:, cols]) + dot(hidden[1], d1_ref[:, cols])
+        part = dot(hidden[0], weights[4][:, cols]) + dot(hidden[1], weights[5][:, cols])
         part = part.astype(BF16)
         out_ref[g] = part[:, :LANES]
         out_ref[g + 1] = part[:, LANES:]
 
 
-def gather_body(in_ref, widen_ref, out_ref):
+def gather_body(*refs):
+    in_refs, widen_ref, out_ref = refs[:PIECES], refs[PIECES], refs[PIECES + 1]
+    span = BLOCKS * CAP_PAD
     for c in range(2):
-        total = in_ref[c].astype(F32)
-        for y in range(1, N_Y):
-            total = total + in_ref[y * 2 + c].astype(F32)
-        rows = dot(widen_ref[...], total.astype(BF16)).astype(BF16)
-        out_ref[c * 16 * CAP_PAD : (c + 1) * 16 * CAP_PAD, :] = rows
-
-
-def finish_body(in_ref, mix_ref, mixed_ref, out_ref):
+        for i, in_ref in enumerate(in_refs):
+            total = in_ref[c].astype(F32)
+            for y in range(1, N_Y):
+                total = total + in_ref[y * 2 + c].astype(F32)
+            rows = dot(widen_ref[...], total.astype(BF16)).astype(BF16)
+            at = (c * PIECES + i) * span
+            out_ref[at : at + span, :] = rows
+
+
+def finish_body(in_ref, mix0_ref, mix1_ref, mix2_ref, mixed_ref, out_ref):
     total = mixed_ref[...]
     rows = in_ref[...]
-    for i in range(3):
-        total = total + dot(mix_ref[i].astype(BF16), rows, 0, 0)
+    for mix_ref in (mix0_ref, mix1_ref, mix2_ref):
+        total = total + dot(mix_ref[...], rows, 0, 0)
     out_ref[...] = total.astype(BF16)
 
 
@@ -271,10 +325,13 @@
 
 VMEM = pl.BlockSpec(memory_space=pltpu.VMEM)
 SMEM = pl.BlockSpec(memory_space=pltpu.SMEM)
-
-
-def call(body, outs, *args, scratch=(), name=None):
-    specs = [SMEM if a.shape == (1,) else VMEM for a in args]
+HBM = pl.BlockSpec(memory_space=pltpu.HBM)
+
+
+def call(body, outs, *args, scratch=(), mib=8, far=0):
+    near = len(args) - far
+    specs = [SMEM if a.shape == (1,) else VMEM for a in args[:near]] + [HBM] * far
+    args = args[:near] + tuple(pltpu.with_memory_space_constraint(a, pltpu.HBM) for a in args[near:])
     many = isinstance(outs, (list, tuple))
     return pl.pallas_call(
         body,
@@ -282,13 +339,16 @@
         in_specs=specs,
         out_specs=[VMEM] * len(outs) if many else VMEM,
         scratch_shapes=list(scratch),
-        name=name,
-        compiler_params=pltpu.CompilerParams(vmem_limit_bytes=48 * 1024 * 1024),
+        compiler_params=pltpu.CompilerParams(vmem_limit_bytes=mib * 1024 * 1024),
     )(*args)
 
 
 def exchange(x, axes):
     return lax.all_to_all(x, axes, 0, 0, tiled=True)
+
+
+def shifted(x, axis, size, by):
+    return lax.ppermute(x, axis, [(i, (i + by) % size) for i in range(size)])
 
 
 def partner(x):
@@ -311,103 +371,140 @@
     up_weight,
     down_weight,
 ):
-    row_tab, col_tab = tables()
-    drop = compaction()
-    block = (lax.axis_index("z") * N_X + lax.axis_index("x")).reshape(1).astype(jnp.int32)
-    core = lax.axis_index("c").reshape(1).astype(jnp.int32)
-    qs, kvs = call(
-        prep_body,
-        [shaped((N_X, TOK + NOTE, LANES)), shaped((N_Z, TOK + NOTE, LANES))],
-        block,
+    return step(
         queries,
         keys.T,
         values.T,
         docs.reshape(2, LANES),
         query_gain.reshape(1, HD),
         key_gain.reshape(1, HD),
+        out_weight,
+        residual,
+        norm_gain,
+        routes.T,
+        route_weight.T,
+        gate_weight[0],
+        up_weight[0],
+        down_weight[0],
+    )
+
+
+def step(
+    queries,
+    keys,
+    values,
+    docs,
+    query_gain,
+    key_gain,
+    out_weight,
+    residual,
+    norm_gain,
+    routes,
+    route_weight,
+    gate,
+    up,
+    down,
+):
+    row_tab, col_tab = tables()
+    drop = compaction()
+    block = (lax.axis_index("z") * N_X + lax.axis_index("x")).reshape(1).astype(jnp.int32)
+    spot = lax.axis_index("x").reshape(1).astype(jnp.int32)
+    core = lax.axis_index("c").reshape(1).astype(jnp.int32)
+    sources = (
+        queries,
+        keys,
+        values,
+        docs,
+        query_gain,
+        key_gain,
         jnp.asarray(row_tab),
         jnp.asarray(col_tab),
-        name="prep",
+    )
+    kept = [pltpu.VMEM(a.shape[1:] if i == 6 else a.shape, a.dtype) for i, a in enumerate(sources)]
+    qs, kvs = call(
+        prep_body,
+        [shaped((TOK + NOTE, LANES)), shaped((N_Z, TOK + NOTE, LANES))],
+        block,
+        *sources,
+        scratch=kept + [pltpu.SemaphoreType.DMA((len(sources),))],
+        far=len(sources),
     )
     kv_all = exchange(kvs, "z")
-    q_all = exchange(qs, "x")
-    gain_all = exchange(jnp.broadcast_to(norm_gain[None, None, :], (N_TP, 8, LANES)), ("y", "c"))
-    gate, up, down = gate_weight[0], up_weight[0], down_weight[0]
+    q_all = [qs] + [shifted(qs, "x", N_X, i) for i in range(1, N_X)]
     out_other = partner(out_weight)
-    gate_o, up_o, down_o = partner(gate), partner(up), partner(down)
-    place, mix = call(
-        route_body,
-        [shaped((EXPERTS * CAP_PAD, TOK), F32), shaped((3, EXPERTS * CAP_PAD, TOK), F32)],
-        routes.T,
-        route_weight.T,
-        name="route",
-    )
+    gate_o, up_o = partner(gate), partner(up)
+    down_o = partner(down)
+    slot_table = shaped((EXPERTS * CAP_PAD, TOK))
+    place = call(route_body, slot_table, routes)
+    mixes = [
+        call(functools.partial(mix_body, i), slot_table, routes, route_weight)
+        for i in range(3)
+    ]
     partial = call(
         attend_body,
         shaped((N_X * 2, HALF + NOTE, LANES)),
-        q_all,
+        spot,
+        *q_all,
         kv_all,
-        scratch=[pltpu.VMEM((N_Z * TOK, LANES), BF16), pltpu.VMEM((N_Z * TOK, LANES), BF16)],
-        name="attend",
+        scratch=[
+            pltpu.VMEM((N_X, TOK + NOTE, LANES), BF16),
+            pltpu.VMEM((N_Z * TOK, LANES), BF16),
+            pltpu.VMEM((N_Z * TOK, LANES), BF16),
+        ],
+        mib=24,
     )
     partial = exchange(partial, ("x", "c"))
     projected = call(
         project_body,
-        shaped((N_TP, HALF, LANES)),
+        shaped((N_TP, HALF + NOTE, LANES)),
         core,
         partial,
         out_weight,
         out_other,
-        name="project",
+        norm_gain.reshape(1, LANES),
     )
     projected = exchange(projected, ("y", "c"))
-    mixed, outgoing = call(
+    mixed, gain_all, outgoing = call(
         dispatch_body,
-        [shaped((TOK, LANES), F32), shaped((EXPERTS * CAP_PAD, LANES))],
+        [
+            shaped((TOK, LANES), F32),
+            shaped((N_TP, 8, LANES), F32),
+            shaped((EXPERTS * CAP_PAD, LANES)),
+        ],
         projected,
         residual,
         place,
-        name="dispatch",
     )
     arrived = exchange(outgoing.reshape(N_SP, CAP_PAD, LANES), ("z", "x"))
-    spread = call(
+    pieces = call(
         spread_body,
-        shaped((N_TP, ROWS, LANES)),
+        [shaped((N_TP, ROWS, LANES))] * PIECES,
         arrived.reshape(N_SP * CAP_PAD, LANES),
         jnp.asarray(drop, BF16),
-        name="spread",
-    )
-    columns = exchange(spread, ("y", "c"))
-    parts = call(
-        expert_body,
-        shaped((N_TP, ROWS, LANES)),
-        columns,
-        gain_all,
-        gate,
-        gate_o,
-        up,
-        up_o,
-        down,
-        down_o,
-        scratch=[pltpu.VMEM((ROWS, D), BF16)],
-        name="expert",
-    )
-    parts = exchange(parts, ("y", "c"))
+    )
+    pieces = [exchange(p, ("y", "c")) for p in pieces]
+    weights = (gate, up, gate_o, up_o, down, down_o)
+    parts = []
+    for columns in pieces:
+        part = call(
+            expert_body,
+            shaped((N_TP, ROWS, LANES)),
+            columns,
+            gain_all,
+            *weights,
+            scratch=[pltpu.VMEM((ROWS, D), BF16)]
+            + [pltpu.VMEM(w.shape, BF16) for w in weights]
+            + [pltpu.SemaphoreType.DMA((len(weights),))],
+            mib=24,
+            far=len(weights),
+        )
+        parts.append(exchange(part, ("y", "c")))
     expert_out = call(
-        gather_body,
-        shaped((N_SP * CAP_PAD, LANES)),
-        parts,
-        jnp.asarray(drop.T, BF16),
-        name="gather",
+        gather_body, shaped((N_SP * CAP_PAD, LANES)), *parts, jnp.asarray(drop.T, BF16)
     )
     returned = exchange(expert_out.reshape(N_SP, CAP_PAD, LANES), ("z", "x"))
     return call(
-        finish_body,
-        shaped((TOK, LANES)),
-        returned.reshape(N_SP * CAP_PAD, LANES),
-        mix,
-        mixed,
-        name="finish",
+        finish_body, shaped((TOK, LANES)), returned.reshape(N_SP * CAP_PAD, LANES), *mixes, mixed
     )
 
 

time: 224 us -> 198 us (0.88)
  blocking collectives: 76.7 us -> 54.6 us
  local copies, waits for them, and re-layouts: 15.7 us -> 1.56 us
  starting transfers between devices: 43.8 us -> 51.5 us
  Pallas kernels: 20.6 us -> 23.2 us
    all_to_all x4 -> x2, blocking collectives: 76.7 us -> 54.6 us  [exchange(): return lax.all_to_all(x, axes, 0, 0, tiled=True)]
    unnamed x52 -> x20, local copies, waits for them, and re-layouts: 15.1 us -> 1.56 us
    ppermute x0 -> x3, starting transfers between devices: none -> 10.5 us  [shifted(): return lax.ppermute(x, axis, [(i, (i + by) % size) for i in range(size)])]
    pallas_call x9 -> x12, Pallas kernels: 20.6 us -> 23.2 us  [call(): pl.pallas_call(body, out_shape=outs, in_specs=specs, out_specs=[VMEM] * l...]
  transfers between devices with their start and end apart: 9 -> 12, of which waited for: 6 -> 8; matrix products, arithmetic and copies ran while one was open for 0% -> 0% of each run, Pallas kernels for 5% -> 5%
where the time goes in v2:
time: 198 us; the launch traced here: 197 us
  waiting for transfers between devices  66.5 us (34%)
  blocking collectives  54.6 us (28%)
  starting transfers between devices  51.5 us (26%)
  Pallas kernels  23.2 us (12%)
    all_to_all x5, waiting for transfers between devices, exchange(): return lax.all_to_all(x, axes, 0, 0, tiled=True)  63.2 us
    all_to_all x2, blocking collectives, exchange(): return lax.all_to_all(x, axes, 0, 0, tiled=True)  54.6 us
    all_to_all x5, starting transfers between devices, exchange(): return lax.all_to_all(x, axes, 0, 0, tiled=True)  31.7 us
    pallas_call x12, Pallas kernels, call(): pl.pallas_call(body, out_shape=outs, in_specs=specs, out_specs=[VMEM] * l...  23.2 us
    ppermute x3, starting transfers between devices, shifted(): return lax.ppermute(x, axis, [(i, (i + by) % size) for i in range(size)])  10.5 us
    ppermute x4, starting transfers between devices, partner(): return lax.ppermute(x, 'c', [(0, 1), (1, 0)])  9.21 us
  transfers between devices with their start and end apart: 12, of which 8 were waited for; matrix products, arithmetic and copies ran while one was open for 0% of the time, Pallas kernels for 5%

profile of v2, /device:TPU:1, one launch (start us, length us, event | category | flops | bytes accessed | tf_op | source)
XLA Modules:
  0.0 197.5 jit_solution(7967271465164504616)
XLA Ops:
  0.0 2.4 %shard_map.172 = (bf16[272,128]{1,0:T(8,128)(2,1)S(1)}, bf16[8,272,128]{2,1,0:T(8,128)(2,1)}) custom-call(s32[1]{0:T(128)} %bitcast.2.blk, bf16[256,128]{1,0:T(8,128)(2,1)} %refs_0_.1, bf16[64,256]{1,0:T(8,128)(2,1)} %bitcast.35, bf16[64,256]{1,0:T(8,128)(2,1)} %bitcast.36, s32[2,128]{1,0:T(2,128)} %bitcast.37, f32[1,64]{1,0:T(1,128)} %bitcast.38, ...), custom_call_target="tpu_custom_call" | custom-call | tf_op jit(solution)/shard_map/pallas_call | solution.py:336
  2.5 10.9 %all-to-all-start = ((bf16[8,272,128]{2,1,0:T(8,128)(2,1)}), bf16[8,272,128]{2,1,0:T(8,128)(2,1)S(1)}, u32[]{:S(2)}, u32[]{:S(2)}) async-start(bf16[8,272,128]{2,1,0:T(8,128)(2,1)} %get-tuple-element.11), calls=%async_computation | async-start | bytes 1114112 | tf_op jit(solution)/shard_map/all_to_all | solution.py:347
  13.3 2.9 %collective-permute-start.3 = (bf16[128,2048]{1,0:T(8,128)(2,1)S(1)}, bf16[128,2048]{1,0:T(8,128)(2,1)S(1)}, u32[]{:S(2)}, u32[]{:S(2)}) collective-permute-start(bf16[128,2048]{1,0:T(8,128)(2,1)S(1)} %copy-done), channel_id=1, source_target_pairs={{0,1},{1,0},{2,3},{3,2},{4,5},{5,4},{6,7},{7,6},{8,9},{9,8},{10,11... | collective-permute-start | bytes 1572872 | tf_op jit(solution)/shard_map/ppermute | solution.py:355
  16.2 3.1 %collective-permute-start = (bf16[272,128]{1,0:T(8,128)(2,1)S(1)}, bf16[272,128]{1,0:T(8,128)(2,1)S(1)}, u32[]{:S(2)}, u32[]{:S(2)}) collective-permute-start(bf16[272,128]{1,0:T(8,128)(2,1)S(1)} %get-tuple-element.10.refs_0_), channel_id=1, source_target_pairs={{0,16},{16,32},{32,48},{48,0},{1,17},{17,33},{33,49},{49,1},{2,18}... | collective-permute-start | bytes 208904 | tf_op jit(solution)/shard_map/ppermute | solution.py:351
  19.3 4.4 %collective-permute-start.1 = (bf16[272,128]{1,0:T(8,128)(2,1)S(1)}, bf16[272,128]{1,0:T(8,128)(2,1)S(1)}, u32[]{:S(2)}, u32[]{:S(2)}) collective-permute-start(bf16[272,128]{1,0:T(8,128)(2,1)S(1)} %get-tuple-element.10.refs_0_), channel_id=1, source_target_pairs={{0,32},{16,48},{32,0},{48,16},{1,33},{17,49},{33,1},{49,17},{2,34}... | collective-permute-start | bytes 208904 | tf_op jit(solution)/shard_map/ppermute | solution.py:351
  23.7 3.1 %collective-permute-start.2 = (bf16[272,128]{1,0:T(8,128)(2,1)S(1)}, bf16[272,128]{1,0:T(8,128)(2,1)S(1)}, u32[]{:S(2)}, u32[]{:S(2)}) collective-permute-start(bf16[272,128]{1,0:T(8,128)(2,1)S(1)} %get-tuple-element.10.refs_0_), channel_id=1, source_target_pairs={{0,48},{16,0},{32,16},{48,32},{1,49},{17,1},{33,17},{49,33},{2,50}... | collective-permute-start | bytes 208904 | tf_op jit(solution)/shard_map/ppermute | solution.py:351
  26.8 2.0 collective-permute-done.2.refs_3_
  28.7 3.2 %all-to-all-done.refs_4_ = bf16[8,272,128]{2,1,0:T(8,128)(2,1)S(1)} async-done(((bf16[8,272,128]{2,1,0:T(8,128)(2,1)}), bf16[8,272,128]{2,1,0:T(8,128)(2,1)S(1)}, u32[]{:S(2)}, u32[]{:S(2)}) %all-to-all-start) | async-done | bytes 557088 | tf_op jit(solution)/shard_map/all_to_all | solution.py:347
  32.0 8.9 %shard_map.173 = bf16[8,144,128]{2,1,0:T(8,128)(2,1)} custom-call(s32[1]{0:T(128)} %bitcast.1.spot, bf16[272,128]{1,0:T(8,128)(2,1)S(1)} %get-tuple-element.10.refs_0_, bf16[272,128]{1,0:T(8,128)(2,1)S(1)} %collective-permute-done.refs_1_, bf16[272,128]{1,0:T(8,128)(2,1)S(1)} %collective-permute-done.1.refs_2_, ...), custom_call_target="tpu_custom_call" | custom-call | tf_op jit(solution)/shard_map/pallas_call | solution.py:336
  40.8 4.8 %all-to-all-start.1 = ((bf16[8,144,128]{2,1,0:T(8,128)(2,1)}), bf16[8,144,128]{2,1,0:T(8,128)(2,1)S(1)}, u32[]{:S(2)}, u32[]{:S(2)}) async-start(bf16[8,144,128]{2,1,0:T(8,128)(2,1)} %shard_map.173), calls=%async_computation.1 | async-start | bytes 589824 | tf_op jit(solution)/shard_map/all_to_all | solution.py:347
  45.6 6.8 %all-to-all-done.1.in_ref = bf16[8,144,128]{2,1,0:T(8,128)(2,1)S(1)} async-done(((bf16[8,144,128]{2,1,0:T(8,128)(2,1)}), bf16[8,144,128]{2,1,0:T(8,128)(2,1)S(1)}, u32[]{:S(2)}, u32[]{:S(2)}) %all-to-all-start.1) | async-done | bytes 294944 | tf_op jit(solution)/shard_map/all_to_all | solution.py:347
  52.4 1.6 shard_map.174
  54.0 8.3 %all-to-all-start.2 = ((bf16[16,144,128]{2,1,0:T(8,128)(2,1)}), bf16[16,144,128]{2,1,0:T(8,128)(2,1)S(1)}, u32[]{:S(2)}, u32[]{:S(2)}) async-start(bf16[16,144,128]{2,1,0:T(8,128)(2,1)} %shard_map.174), calls=%async_computation.2 | async-start | bytes 1179648 | tf_op jit(solution)/shard_map/all_to_all | solution.py:347
  62.6 18.3 %all-to-all-done.2.in_ref = bf16[16,144,128]{2,1,0:T(8,128)(2,1)S(1)} async-done(((bf16[16,144,128]{2,1,0:T(8,128)(2,1)}), bf16[16,144,128]{2,1,0:T(8,128)(2,1)S(1)}, u32[]{:S(2)}, u32[]{:S(2)}) %all-to-all-start.2) | async-done | bytes 589856 | tf_op jit(solution)/shard_map/all_to_all | solution.py:347
  80.9 0.3 shard_map.176
  81.2 16.8 %all_to_all.35 = bf16[32,24,128]{2,1,0:T(8,128)(2,1)S(1)} all-to-all(bf16[32,24,128]{2,1,0:T(8,128)(2,1)S(1)} %bitcast.20), channel_id=1, replica_groups=mesh['z'=8,'x'=4,'y'=8,'c'=2] {'z','x'}, dimensions={0} | all-to-all | bytes 393216 | tf_op jit(solution)/shard_map/all_to_all | solution.py:347
  98.0 1.4 shard_map.177
  99.4 3.9 %all-to-all-start.4 = ((bf16[16,320,128]{2,1,0:T(8,128)(2,1)}), bf16[16,320,128]{2,1,0:T(8,128)(2,1)S(1)}, u32[]{:S(2)}, u32[]{:S(2)}) async-start(bf16[16,320,128]{2,1,0:T(8,128)(2,1)} %shard_map.177), calls=%async_computation.4 | async-start | bytes 2621440 | tf_op jit(solution)/shard_map/all_to_all | solution.py:347
  103.3 2.0 %collective-permute-start.4 = (bf16[2048,256]{1,0:T(8,128)(2,1)S(1)}, bf16[2048,256]{1,0:T(8,128)(2,1)S(1)}, u32[]{:S(2)}, u32[]{:S(2)}) collective-permute-start(bf16[2048,256]{1,0:T(8,128)(2,1)S(1)} %bitcast.30), channel_id=1, source_target_pairs={{0,1},{1,0},{2,3},{3,2},{4,5},{5,4},{6,7},{7,6},{8,9},{9,8},{10,11... | collective-permute-start | bytes 3145736 | tf_op jit(solution)/shard_map/ppermute | solution.py:355
  105.3 2.3 %collective-permute-start.5 = (bf16[2048,256]{1,0:T(8,128)(2,1)}, bf16[2048,256]{1,0:T(8,128)(2,1)S(1)}, u32[]{:S(2)}, u32[]{:S(2)}) collective-permute-start(bf16[2048,256]{1,0:T(8,128)(2,1)} %bitcast.31), channel_id=1, source_target_pairs={{0,1},{1,0},{2,3},{3,2},{4,5},{5,4},{6,7},{7,6},{8,9},{9,8},{10,11... | collective-permute-start | bytes 3145736 | tf_op jit(solution)/shard_map/ppermute | solution.py:355
  107.6 2.0 %collective-permute-start.6 = (bf16[256,2048]{1,0:T(8,128)(2,1)}, bf16[256,2048]{1,0:T(8,128)(2,1)}, u32[]{:S(2)}, u32[]{:S(2)}) collective-permute-start(bf16[256,2048]{1,0:T(8,128)(2,1)} %bitcast.33), channel_id=1, source_target_pairs={{0,1},{1,0},{2,3},{3,2},{4,5},{5,4},{6,7},{7,6},{8,9},{9,8},{10,11... | collective-permute-start | bytes 3145736 | tf_op jit(solution)/shard_map/ppermute | solution.py:355
  109.7 0.4 collective-permute-done.5.refs_3_
  110.1 0.5 copy-done.8
  110.6 1.0 copy-done.9
  111.6 0.9 collective-permute-done.6.refs_5_
  112.5 24.0 %all-to-all-done.4.in_ref = bf16[16,320,128]{2,1,0:T(8,128)(2,1)S(1)} async-done(((bf16[16,320,128]{2,1,0:T(8,128)(2,1)}), bf16[16,320,128]{2,1,0:T(8,128)(2,1)S(1)}, u32[]{:S(2)}, u32[]{:S(2)}) %all-to-all-start.4) | async-done | bytes 1310752 | tf_op jit(solution)/shard_map/all_to_all | solution.py:347
  136.5 5.4 %shard_map.178 = bf16[16,320,128]{2,1,0:T(8,128)(2,1)S(1)} custom-call(bf16[16,320,128]{2,1,0:T(8,128)(2,1)S(1)} %all-to-all-done.4.in_ref, f32[16,8,128]{2,1,0:T(8,128)S(1)} %get-tuple-element.13.gain_ref, bf16[2048,256]{1,0:T(8,128)(2,1)} %bitcast.29, bf16[2048,256]{1,0:T(8,128)(2,1)} %bitcast.32, bf16[2048,256]{1,0:T(8,128)(2,1)} %copy-done.8, ...), custom_call_target="tpu_custom_call" | custom-call | tf_op jit(solution)/shard_map/pallas_call | solution.py:336
  142.0 37.8 %all_to_all.36.refs_0_ = bf16[16,320,128]{2,1,0:T(8,128)(2,1)S(1)} all-to-all(bf16[16,320,128]{2,1,0:T(8,128)(2,1)S(1)} %shard_map.178), channel_id=1, replica_groups=mesh['z'=8,'x'=4,'y'=8,'c'=2] {'y','c'}, dimensions={0} | all-to-all | bytes 2621440 | tf_op jit(solution)/shard_map/all_to_all | solution.py:347
  179.8 1.1 shard_map.179
  180.9 3.9 %all-to-all-start.6 = ((bf16[32,24,128]{2,1,0:T(8,128)(2,1)}), bf16[32,24,128]{2,1,0:T(8,128)(2,1)S(1)}, u32[]{:S(2)}, u32[]{:S(2)}) async-start(bf16[32,24,128]{2,1,0:T(8,128)(2,1)} %bitcast.15), calls=%async_computation.6 | async-start | bytes 393216 | tf_op jit(solution)/shard_map/all_to_all | solution.py:347
  185.4 10.9 %all-to-all-done.6 = bf16[32,24,128]{2,1,0:T(8,128)(2,1)S(1)} async-done(((bf16[32,24,128]{2,1,0:T(8,128)(2,1)}), bf16[32,24,128]{2,1,0:T(8,128)(2,1)S(1)}, u32[]{:S(2)}, u32[]{:S(2)}) %all-to-all-start.6) | async-done | bytes 196640 | tf_op jit(solution)/shard_map/all_to_all | solution.py:347
  196.3 1.1 shard_map.183
  (26 shorter events, 1.0 us)
Async XLA Ops:
  0.0 13.3 %copy-start = (bf16[128,2048]{1,0:T(8,128)(2,1)S(1)}, bf16[128,2048]{1,0:T(8,128)(2,1)}, u32[]{:S(2)}) copy-start(bf16[128,2048]{1,0:T(8,128)(2,1)} %w_own_ref.1) | copy-start | bytes 1572868
  2.4 50.0 %copy-start.6 = (f32[128]{0:T(128)S(1)}, f32[128]{0:T(128)}, u32[]{:S(2)}) copy-start(f32[128]{0:T(128)} %param.26) | copy-start | bytes 1540
  2.5 29.5 %all-to-all-start = ((bf16[8,272,128]{2,1,0:T(8,128)(2,1)}), bf16[8,272,128]{2,1,0:T(8,128)(2,1)S(1)}, u32[]{:S(2)}, u32[]{:S(2)}) async-start(bf16[8,272,128]{2,1,0:T(8,128)(2,1)} %get-tuple-element.11), calls=%async_computation | async-start | bytes 1114112 | tf_op jit(solution)/shard_map/all_to_all | solution.py:347
  13.3 32.3 %collective-permute-start.3 = (bf16[128,2048]{1,0:T(8,128)(2,1)S(1)}, bf16[128,2048]{1,0:T(8,128)(2,1)S(1)}, u32[]{:S(2)}, u32[]{:S(2)}) collective-permute-start(bf16[128,2048]{1,0:T(8,128)(2,1)S(1)} %copy-done), channel_id=1, source_target_pairs={{0,1},{1,0},{2,3},{3,2},{4,5},{5,4},{6,7},{7,6},{8,9},{9,8},{10,11... | collective-permute-start | bytes 1572872 | tf_op jit(solution)/shard_map/ppermute | solution.py:355
  16.2 10.6 %collective-permute-start = (bf16[272,128]{1,0:T(8,128)(2,1)S(1)}, bf16[272,128]{1,0:T(8,128)(2,1)S(1)}, u32[]{:S(2)}, u32[]{:S(2)}) collective-permute-start(bf16[272,128]{1,0:T(8,128)(2,1)S(1)} %get-tuple-element.10.refs_0_), channel_id=1, source_target_pairs={{0,16},{16,32},{32,48},{48,0},{1,17},{17,33},{33,49},{49,1},{2,18}... | collective-permute-start | bytes 208904 | tf_op jit(solution)/shard_map/ppermute | solution.py:351
  19.3 7.4 %collective-permute-start.1 = (bf16[272,128]{1,0:T(8,128)(2,1)S(1)}, bf16[272,128]{1,0:T(8,128)(2,1)S(1)}, u32[]{:S(2)}, u32[]{:S(2)}) collective-permute-start(bf16[272,128]{1,0:T(8,128)(2,1)S(1)} %get-tuple-element.10.refs_0_), channel_id=1, source_target_pairs={{0,32},{16,48},{32,0},{48,16},{1,33},{17,49},{33,1},{49,17},{2,34}... | collective-permute-start | bytes 208904 | tf_op jit(solution)/shard_map/ppermute | solution.py:351
  23.7 5.1 %collective-permute-start.2 = (bf16[272,128]{1,0:T(8,128)(2,1)S(1)}, bf16[272,128]{1,0:T(8,128)(2,1)S(1)}, u32[]{:S(2)}, u32[]{:S(2)}) collective-permute-start(bf16[272,128]{1,0:T(8,128)(2,1)S(1)} %get-tuple-element.10.refs_0_), channel_id=1, source_target_pairs={{0,48},{16,0},{32,16},{48,32},{1,49},{17,1},{33,17},{49,33},{2,50}... | collective-permute-start | bytes 208904 | tf_op jit(solution)/shard_map/ppermute | solution.py:351
  40.8 11.6 %all-to-all-start.1 = ((bf16[8,144,128]{2,1,0:T(8,128)(2,1)}), bf16[8,144,128]{2,1,0:T(8,128)(2,1)S(1)}, u32[]{:S(2)}, u32[]{:S(2)}) async-start(bf16[8,144,128]{2,1,0:T(8,128)(2,1)} %shard_map.173), calls=%async_computation.1 | async-start | bytes 589824 | tf_op jit(solution)/shard_map/all_to_all | solution.py:347
  52.4 9.9 %copy-start.4 = (s32[256,2]{0,1:T(2,128)S(1)}, s32[256,2]{0,1:T(2,128)}, u32[]{:S(2)}) copy-start(s32[256,2]{0,1:T(2,128)} %param.27) | copy-start | bytes 6148
  52.4 28.5 %copy-start.3 = (bf16[256,128]{1,0:T(8,128)(2,1)S(1)}, bf16[256,128]{1,0:T(8,128)(2,1)}, u32[]{:S(2)}) copy-start(bf16[256,128]{1,0:T(8,128)(2,1)} %residual_ref.1) | copy-start | bytes 196612
  54.0 44.0 %copy-start.2 = (bf16[320,384]{1,0:T(8,128)(2,1)S(1)}, bf16[320,384]{1,0:T(8,128)(2,1)}, u32[]{:S(2)}) copy-start(bf16[320,384]{1,0:T(8,128)(2,1)} %constant.28.clone.drop_ref) | copy-start | bytes 737284
  54.0 26.9 %all-to-all-start.2 = ((bf16[16,144,128]{2,1,0:T(8,128)(2,1)}), bf16[16,144,128]{2,1,0:T(8,128)(2,1)S(1)}, u32[]{:S(2)}, u32[]{:S(2)}) async-start(bf16[16,144,128]{2,1,0:T(8,128)(2,1)} %shard_map.174), calls=%async_computation.2 | async-start | bytes 1179648 | tf_op jit(solution)/shard_map/all_to_all | solution.py:347
  99.4 3.9 %copy-start.7 = (bf16[1,2048,256]{2,1,0:T(8,128)(2,1)S(1)}, bf16[1,2048,256]{2,1,0:T(8,128)(2,1)}, u32[]{:S(2)}) copy-start(bf16[1,2048,256]{2,1,0:T(8,128)(2,1)} %param.29) | copy-start | bytes 3145732
  99.4 37.1 %all-to-all-start.4 = ((bf16[16,320,128]{2,1,0:T(8,128)(2,1)}), bf16[16,320,128]{2,1,0:T(8,128)(2,1)S(1)}, u32[]{:S(2)}, u32[]{:S(2)}) async-start(bf16[16,320,128]{2,1,0:T(8,128)(2,1)} %shard_map.177), calls=%async_computation.4 | async-start | bytes 2621440 | tf_op jit(solution)/shard_map/all_to_all | solution.py:347
  103.3 6.4 %collective-permute-start.4 = (bf16[2048,256]{1,0:T(8,128)(2,1)S(1)}, bf16[2048,256]{1,0:T(8,128)(2,1)S(1)}, u32[]{:S(2)}, u32[]{:S(2)}) collective-permute-start(bf16[2048,256]{1,0:T(8,128)(2,1)S(1)} %bitcast.30), channel_id=1, source_target_pairs={{0,1},{1,0},{2,3},{3,2},{4,5},{5,4},{6,7},{7,6},{8,9},{9,8},{10,11... | collective-permute-start | bytes 3145736 | tf_op jit(solution)/shard_map/ppermute | solution.py:355
  105.3 4.8 %collective-permute-start.5 = (bf16[2048,256]{1,0:T(8,128)(2,1)}, bf16[2048,256]{1,0:T(8,128)(2,1)S(1)}, u32[]{:S(2)}, u32[]{:S(2)}) collective-permute-start(bf16[2048,256]{1,0:T(8,128)(2,1)} %bitcast.31), channel_id=1, source_target_pairs={{0,1},{1,0},{2,3},{3,2},{4,5},{5,4},{6,7},{7,6},{8,9},{9,8},{10,11... | collective-permute-start | bytes 3145736 | tf_op jit(solution)/shard_map/ppermute | solution.py:355
  107.6 4.9 %collective-permute-start.6 = (bf16[256,2048]{1,0:T(8,128)(2,1)}, bf16[256,2048]{1,0:T(8,128)(2,1)}, u32[]{:S(2)}, u32[]{:S(2)}) collective-permute-start(bf16[256,2048]{1,0:T(8,128)(2,1)} %bitcast.33), channel_id=1, source_target_pairs={{0,1},{1,0},{2,3},{3,2},{4,5},{5,4},{6,7},{7,6},{8,9},{9,8},{10,11... | collective-permute-start | bytes 3145736 | tf_op jit(solution)/shard_map/ppermute | solution.py:355
  109.6 1.0 copy-start.8
  110.6 1.0 copy-start.9
  142.0 37.8 %copy-start.1 = (bf16[384,320]{1,0:T(8,128)(2,1)S(1)}, bf16[384,320]{1,0:T(8,128)(2,1)}, u32[]{:S(2)}) copy-start(bf16[384,320]{1,0:T(8,128)(2,1)} %constant.29.clone.refs_1_) | copy-start | bytes 737284
  179.8 5.0 %copy-start.5 = (f32[256,2]{0,1:T(2,128)S(1)}, f32[256,2]{0,1:T(2,128)}, u32[]{:S(2)}) copy-start(f32[256,2]{0,1:T(2,128)} %param.28) | copy-start | bytes 6148
  180.9 15.5 %all-to-all-start.6 = ((bf16[32,24,128]{2,1,0:T(8,128)(2,1)}), bf16[32,24,128]{2,1,0:T(8,128)(2,1)S(1)}, u32[]{:S(2)}, u32[]{:S(2)}) async-start(bf16[32,24,128]{2,1,0:T(8,128)(2,1)} %bitcast.15), calls=%async_computation.6 | async-start | bytes 393216 | tf_op jit(solution)/shard_map/all_to_all | solution.py:347

commit v3 on v2

--- a/solution.py
+++ b/solution.py
@@ -24,9 +24,9 @@
 EXPERTS = 32
 CAP = 20
 CAP_PAD = 24
-PIECES = 1
-ROWS = N_SP * CAP // (2 * PIECES)
-BLOCKS = N_SP // (2 * PIECES)
+GROUPS = 4
+ROWS = N_SP * CAP // GROUPS
+BLOCKS = N_SP // GROUPS
 NOTE = 16
 MASK_BIG = 16384.0
 
@@ -257,19 +257,18 @@
     out_ref[...] = dot(place_ref[...], mixed.astype(BF16)).astype(BF16)
 
 
-def spread_body(in_ref, drop_ref, *out_refs):
+def spread_body(in_ref, drop_ref, out_ref):
     span = BLOCKS * CAP_PAD
-    for c in range(2):
-        for i, out_ref in enumerate(out_refs):
-            at = (c * PIECES + i) * span
-            kept = dot(drop_ref[...], in_ref[at : at + span, :]).astype(BF16)
-            for y in range(N_Y):
-                out_ref[y * 2 + c] = kept
+    for r in range(GROUPS):
+        kept = dot(drop_ref[...], in_ref[r * span : (r + 1) * span, :]).astype(BF16)
+        for g in range(r, N_TP, GROUPS):
+            out_ref[g] = kept
 
 
 def expert_body(in_ref, gain_ref, *refs):
-    far, (out_ref, x_ref), weights, sems = refs[:6], refs[6:8], refs[8:14], refs[14]
-    copies = [pltpu.make_async_copy(far[i], weights[i], sems.at[i]) for i in range(6)]
+    many = 3 * GROUPS
+    far, (out_ref, x_ref), weights, sems = refs[:many], refs[many : many + 2], refs[many + 2 : -1], refs[-1]
+    copies = [pltpu.make_async_copy(far[i], weights[i], sems.at[i]) for i in range(many)]
     for copy in copies:
         copy.start()
     total = jnp.zeros((ROWS, LANES), F32)
@@ -281,34 +280,34 @@
         x = in_ref[g].astype(F32) * scale * gain_ref[g, 0:1, :]
         x_ref[:, g * LANES : (g + 1) * LANES] = x.astype(BF16)
     hidden = []
-    for i in range(2):
+    for i in range(GROUPS):
         copies[2 * i].wait()
         gate = jnp.minimum(dot(x_ref[...], weights[2 * i][...]), CLAMP_LIMIT)
         copies[2 * i + 1].wait()
         up = jnp.clip(dot(x_ref[...], weights[2 * i + 1][...]), -CLAMP_LIMIT, CLAMP_LIMIT)
         unit = gate * (1.0 / (1.0 + jnp.exp(-SIGMOID_SCALE * gate))) * (up + 1.0)
         hidden.append(unit.astype(BF16))
-    copies[4].wait()
-    copies[5].wait()
+    for copy in copies[2 * GROUPS :]:
+        copy.wait()
+    downs = weights[2 * GROUPS :]
     for g in range(0, N_TP, 2):
         cols = slice(g * LANES, (g + 2) * LANES)
-        part = dot(hidden[0], weights[4][:, cols]) + dot(hidden[1], weights[5][:, cols])
+        part = dot(hidden[0], downs[0][:, cols])
+        for h, w in zip(hidden[1:], downs[1:]):
+            part = part + dot(h, w[:, cols])
         part = part.astype(BF16)
         out_ref[g] = part[:, :LANES]
         out_ref[g + 1] = part[:, LANES:]
 
 
-def gather_body(*refs):
-    in_refs, widen_ref, out_ref = refs[:PIECES], refs[PIECES], refs[PIECES + 1]
+def gather_body(in_ref, widen_ref, out_ref):
     span = BLOCKS * CAP_PAD
-    for c in range(2):
-        for i, in_ref in enumerate(in_refs):
-            total = in_ref[c].astype(F32)
-            for y in range(1, N_Y):
-                total = total + in_ref[y * 2 + c].astype(F32)
-            rows = dot(widen_ref[...], total.astype(BF16)).astype(BF16)
-            at = (c * PIECES + i) * span
-            out_ref[at : at + span, :] = rows
+    for r in range(GROUPS):
+        total = in_ref[r].astype(F32)
+        for g in range(r + GROUPS, N_TP, GROUPS):
+            total = total + in_ref[g].astype(F32)
+        rows = dot(widen_ref[...], total.astype(BF16)).astype(BF16)
+        out_ref[r * span : (r + 1) * span, :] = rows
 
 
 def finish_body(in_ref, mix0_ref, mix1_ref, mix2_ref, mixed_ref, out_ref):
@@ -353,6 +352,10 @@
 
 def partner(x):
     return lax.ppermute(x, "c", [(0, 1), (1, 0)])
+
+
+def neighbour(x):
+    return lax.ppermute(x, "y", [(i, i ^ 1) for i in range(N_Y)])
 
 
 def per_device(
@@ -432,8 +435,12 @@
     kv_all = exchange(kvs, "z")
     q_all = [qs] + [shifted(qs, "x", N_X, i) for i in range(1, N_X)]
     out_other = partner(out_weight)
+    gate_y, up_y = neighbour(gate), neighbour(up)
+    down_y = neighbour(down)
     gate_o, up_o = partner(gate), partner(up)
     down_o = partner(down)
+    gate_yo, up_yo = partner(gate_y), partner(up_y)
+    down_yo = partner(down_y)
     slot_table = shaped((EXPERTS * CAP_PAD, TOK))
     place = call(route_body, slot_table, routes)
     mixes = [
@@ -476,31 +483,29 @@
         place,
     )
     arrived = exchange(outgoing.reshape(N_SP, CAP_PAD, LANES), ("z", "x"))
-    pieces = call(
+    spread = call(
         spread_body,
-        [shaped((N_TP, ROWS, LANES))] * PIECES,
+        shaped((N_TP, ROWS, LANES)),
         arrived.reshape(N_SP * CAP_PAD, LANES),
         jnp.asarray(drop, BF16),
     )
-    pieces = [exchange(p, ("y", "c")) for p in pieces]
-    weights = (gate, up, gate_o, up_o, down, down_o)
-    parts = []
-    for columns in pieces:
-        part = call(
-            expert_body,
-            shaped((N_TP, ROWS, LANES)),
-            columns,
-            gain_all,
-            *weights,
-            scratch=[pltpu.VMEM((ROWS, D), BF16)]
-            + [pltpu.VMEM(w.shape, BF16) for w in weights]
-            + [pltpu.SemaphoreType.DMA((len(weights),))],
-            mib=24,
-            far=len(weights),
-        )
-        parts.append(exchange(part, ("y", "c")))
+    columns = exchange(spread, ("y", "c"))
+    weights = (gate, up, gate_o, up_o, gate_y, up_y, gate_yo, up_yo, down, down_o, down_y, down_yo)
+    parts = call(
+        expert_body,
+        shaped((N_TP, ROWS, LANES)),
+        columns,
+        gain_all,
+        *weights,
+        scratch=[pltpu.VMEM((ROWS, D), BF16)]
+        + [pltpu.VMEM(w.shape, BF16) for w in weights]
+        + [pltpu.SemaphoreType.DMA((len(weights),))],
+        mib=32,
+        far=len(weights),
+    )
+    parts = exchange(parts, ("y", "c"))
     expert_out = call(
-        gather_body, shaped((N_SP * CAP_PAD, LANES)), *parts, jnp.asarray(drop.T, BF16)
+        gather_body, shaped((N_SP * CAP_PAD, LANES)), parts, jnp.asarray(drop.T, BF16)
     )
     returned = exchange(expert_out.reshape(N_SP, CAP_PAD, LANES), ("z", "x"))
     return call(

time: 198 us -> 212 us (1.071)
  starting transfers between devices: 51.5 us -> 72 us
  blocking collectives: 54.6 us -> 39.9 us
  waiting for transfers between devices: 66.5 us -> 72.5 us
    ppermute x0 -> x3, waiting for transfers between devices: none -> 37.3 us  [neighbour(): return lax.ppermute(x, 'y', [(i, i ^ 1) for i in range(N_Y)])]
    all_to_all x5, waiting for transfers between devices: 63.2 us -> 32.5 us  [exchange(): return lax.all_to_all(x, axes, 0, 0, tiled=True)]
    all_to_all x2, blocking collectives: 54.6 us -> 39.9 us  [exchange(): return lax.all_to_all(x, axes, 0, 0, tiled=True)]
    ppermute x4 -> x7, starting transfers between devices: 9.21 us -> 19.1 us  [partner(): return lax.ppermute(x, 'c', [(0, 1), (1, 0)])]
    ppermute x0 -> x3, starting transfers between devices: none -> 8.54 us  [neighbour(): return lax.ppermute(x, 'y', [(i, i ^ 1) for i in range(N_Y)])]
  transfers between devices with their start and end apart: 12 -> 18, of which waited for: 8 -> 10; matrix products, arithmetic and copies ran while one was open for 0% -> 0% of each run, Pallas kernels for 5% -> 5%
where the time goes in v3:
time: 212 us; the launch traced here: 211 us
  waiting for transfers between devices  72.5 us (34%)
  starting transfers between devices  72 us (34%)
  blocking collectives  39.9 us (19%)
  Pallas kernels  23.3 us (11%)
  local copies, waits for them, and re-layouts  2.87 us (1%)
    all_to_all x2, blocking collectives, exchange(): return lax.all_to_all(x, axes, 0, 0, tiled=True)  39.9 us
    ppermute x3, waiting for transfers between devices, neighbour(): return lax.ppermute(x, 'y', [(i, i ^ 1) for i in range(N_Y)])  37.3 us
    all_to_all x5, starting transfers between devices, exchange(): return lax.all_to_all(x, axes, 0, 0, tiled=True)  33.8 us
    all_to_all x5, waiting for transfers between devices, exchange(): return lax.all_to_all(x, axes, 0, 0, tiled=True)  32.5 us
    pallas_call x12, Pallas kernels, call(): pl.pallas_call(body, out_shape=outs, in_specs=specs, out_specs=[VMEM] * l...  23.3 us
    ppermute x7, starting transfers between devices, partner(): return lax.ppermute(x, 'c', [(0, 1), (1, 0)])  19.1 us
    ppermute x3, starting transfers between devices, shifted(): return lax.ppermute(x, axis, [(i, (i + by) % size) for i in range(size)])  10.5 us
    ppermute x3, starting transfers between devices, neighbour(): return lax.ppermute(x, 'y', [(i, i ^ 1) for i in range(N_Y)])  8.54 us
  transfers between devices with their start and end apart: 18, of which 10 were waited for; matrix products, arithmetic and copies ran while one was open for 0% of the time, Pallas kernels for 5%

profile of v3, /device:TPU:1, one launch (start us, length us, event | category | flops | bytes accessed | tf_op | source)
XLA Modules:
  0.0 210.8 jit_solution(8555735323478126606)
XLA Ops:
  0.0 2.3 %shard_map.172 = (bf16[272,128]{1,0:T(8,128)(2,1)S(1)}, bf16[8,272,128]{2,1,0:T(8,128)(2,1)}) custom-call(s32[1]{0:T(128)} %bitcast.2.blk, bf16[256,128]{1,0:T(8,128)(2,1)} %refs_0_.1, bf16[64,256]{1,0:T(8,128)(2,1)} %bitcast.38, bf16[64,256]{1,0:T(8,128)(2,1)} %bitcast.39, s32[2,128]{1,0:T(2,128)} %bitcast.40, f32[1,64]{1,0:T(1,128)} %bitcast.41, ...), custom_call_target="tpu_custom_call" | custom-call | tf_op jit(solution)/shard_map/pallas_call | solution.py:335
  2.4 11.0 %all-to-all-start = ((bf16[8,272,128]{2,1,0:T(8,128)(2,1)}), bf16[8,272,128]{2,1,0:T(8,128)(2,1)S(1)}, u32[]{:S(2)}, u32[]{:S(2)}) async-start(bf16[8,272,128]{2,1,0:T(8,128)(2,1)} %get-tuple-element.11), calls=%async_computation | async-start | bytes 1114112 | tf_op jit(solution)/shard_map/all_to_all | solution.py:346
  13.4 2.9 %collective-permute-start.3 = (bf16[128,2048]{1,0:T(8,128)(2,1)S(1)}, bf16[128,2048]{1,0:T(8,128)(2,1)S(1)}, u32[]{:S(2)}, u32[]{:S(2)}) collective-permute-start(bf16[128,2048]{1,0:T(8,128)(2,1)S(1)} %copy-done), channel_id=1, source_target_pairs={{0,1},{1,0},{2,3},{3,2},{4,5},{5,4},{6,7},{7,6},{8,9},{9,8},{10,11... | collective-permute-start | bytes 1572872 | tf_op jit(solution)/shard_map/ppermute | solution.py:354
  16.2 3.1 %collective-permute-start = (bf16[272,128]{1,0:T(8,128)(2,1)S(1)}, bf16[272,128]{1,0:T(8,128)(2,1)S(1)}, u32[]{:S(2)}, u32[]{:S(2)}) collective-permute-start(bf16[272,128]{1,0:T(8,128)(2,1)S(1)} %get-tuple-element.10.refs_0_), channel_id=1, source_target_pairs={{0,16},{16,32},{32,48},{48,0},{1,17},{17,33},{33,49},{49,1},{2,18}... | collective-permute-start | bytes 208904 | tf_op jit(solution)/shard_map/ppermute | solution.py:350
  19.4 4.4 %collective-permute-start.1 = (bf16[272,128]{1,0:T(8,128)(2,1)S(1)}, bf16[272,128]{1,0:T(8,128)(2,1)S(1)}, u32[]{:S(2)}, u32[]{:S(2)}) collective-permute-start(bf16[272,128]{1,0:T(8,128)(2,1)S(1)} %get-tuple-element.10.refs_0_), channel_id=1, source_target_pairs={{0,32},{16,48},{32,0},{48,16},{1,33},{17,49},{33,1},{49,17},{2,34}... | collective-permute-start | bytes 208904 | tf_op jit(solution)/shard_map/ppermute | solution.py:350
  23.7 3.1 %collective-permute-start.2 = (bf16[272,128]{1,0:T(8,128)(2,1)S(1)}, bf16[272,128]{1,0:T(8,128)(2,1)S(1)}, u32[]{:S(2)}, u32[]{:S(2)}) collective-permute-start(bf16[272,128]{1,0:T(8,128)(2,1)S(1)} %get-tuple-element.10.refs_0_), channel_id=1, source_target_pairs={{0,48},{16,0},{32,16},{48,32},{1,49},{17,1},{33,17},{49,33},{2,50}... | collective-permute-start | bytes 208904 | tf_op jit(solution)/shard_map/ppermute | solution.py:350
  26.8 2.0 collective-permute-done.2.refs_3_
  28.8 3.2 %all-to-all-done.refs_4_ = bf16[8,272,128]{2,1,0:T(8,128)(2,1)S(1)} async-done(((bf16[8,272,128]{2,1,0:T(8,128)(2,1)}), bf16[8,272,128]{2,1,0:T(8,128)(2,1)S(1)}, u32[]{:S(2)}, u32[]{:S(2)}) %all-to-all-start) | async-done | bytes 557088 | tf_op jit(solution)/shard_map/all_to_all | solution.py:346
  32.0 8.8 %shard_map.173 = bf16[8,144,128]{2,1,0:T(8,128)(2,1)} custom-call(s32[1]{0:T(128)} %bitcast.1.spot, bf16[272,128]{1,0:T(8,128)(2,1)S(1)} %get-tuple-element.10.refs_0_, bf16[272,128]{1,0:T(8,128)(2,1)S(1)} %collective-permute-done.refs_1_, bf16[272,128]{1,0:T(8,128)(2,1)S(1)} %collective-permute-done.1.refs_2_, ...), custom_call_target="tpu_custom_call" | custom-call | tf_op jit(solution)/shard_map/pallas_call | solution.py:335
  40.9 4.8 %all-to-all-start.1 = ((bf16[8,144,128]{2,1,0:T(8,128)(2,1)}), bf16[8,144,128]{2,1,0:T(8,128)(2,1)S(1)}, u32[]{:S(2)}, u32[]{:S(2)}) async-start(bf16[8,144,128]{2,1,0:T(8,128)(2,1)} %shard_map.173), calls=%async_computation.1 | async-start | bytes 589824 | tf_op jit(solution)/shard_map/all_to_all | solution.py:346
  45.6 6.8 %all-to-all-done.1.in_ref = bf16[8,144,128]{2,1,0:T(8,128)(2,1)S(1)} async-done(((bf16[8,144,128]{2,1,0:T(8,128)(2,1)}), bf16[8,144,128]{2,1,0:T(8,128)(2,1)S(1)}, u32[]{:S(2)}, u32[]{:S(2)}) %all-to-all-start.1) | async-done | bytes 294944 | tf_op jit(solution)/shard_map/all_to_all | solution.py:346
  53.1 1.6 shard_map.174
  54.7 8.3 %all-to-all-start.2 = ((bf16[16,144,128]{2,1,0:T(8,128)(2,1)}), bf16[16,144,128]{2,1,0:T(8,128)(2,1)S(1)}, u32[]{:S(2)}, u32[]{:S(2)}) async-start(bf16[16,144,128]{2,1,0:T(8,128)(2,1)} %shard_map.174), calls=%async_computation.2 | async-start | bytes 1179648 | tf_op jit(solution)/shard_map/all_to_all | solution.py:346
  63.0 3.3 %collective-permute-start.11 = (bf16[256,2048]{1,0:T(8,128)(2,1)}, bf16[256,2048]{1,0:T(8,128)(2,1)}, u32[]{:S(2)}, u32[]{:S(2)}) collective-permute-start(bf16[256,2048]{1,0:T(8,128)(2,1)} %bitcast.35), channel_id=1, source_target_pairs={{0,2},{2,0},{4,6},{6,4},{8,10},{10,8},{12,14},{14,12},{1,3},{3,1},... | collective-permute-start | bytes 3145736 | tf_op jit(solution)/shard_map/ppermute | solution.py:358
  66.3 2.0 collective-permute-start.6
  68.3 3.3 %collective-permute-start.7 = (bf16[2048,256]{1,0:T(8,128)(2,1)S(1)}, bf16[2048,256]{1,0:T(8,128)(2,1)}, u32[]{:S(2)}, u32[]{:S(2)}) collective-permute-start(bf16[2048,256]{1,0:T(8,128)(2,1)S(1)} %bitcast.33), channel_id=1, source_target_pairs={{0,2},{2,0},{4,6},{6,4},{8,10},{10,8},{12,14},{14,12},{1,3},{3,1},... | collective-permute-start | bytes 3145736 | tf_op jit(solution)/shard_map/ppermute | solution.py:358
  71.6 3.1 %collective-permute-start.10 = (bf16[256,2048]{1,0:T(8,128)(2,1)}, bf16[256,2048]{1,0:T(8,128)(2,1)}, u32[]{:S(2)}, u32[]{:S(2)}) collective-permute-start(bf16[256,2048]{1,0:T(8,128)(2,1)} %bitcast.36), channel_id=1, source_target_pairs={{0,1},{1,0},{2,3},{3,2},{4,5},{5,4},{6,7},{7,6},{8,9},{9,8},{10,11... | collective-permute-start | bytes 3145736 | tf_op jit(solution)/shard_map/ppermute | solution.py:354
  75.0 6.7 %all-to-all-done.2.in_ref = bf16[16,144,128]{2,1,0:T(8,128)(2,1)S(1)} async-done(((bf16[16,144,128]{2,1,0:T(8,128)(2,1)}), bf16[16,144,128]{2,1,0:T(8,128)(2,1)S(1)}, u32[]{:S(2)}, u32[]{:S(2)}) %all-to-all-start.2) | async-done | bytes 589856 | tf_op jit(solution)/shard_map/all_to_all | solution.py:346
  82.1 16.7 %all_to_all.35 = bf16[32,24,128]{2,1,0:T(8,128)(2,1)S(1)} all-to-all(bf16[32,24,128]{2,1,0:T(8,128)(2,1)S(1)} %bitcast.20), channel_id=1, replica_groups=mesh['z'=8,'x'=4,'y'=8,'c'=2] {'z','x'}, dimensions={0} | all-to-all | bytes 393216 | tf_op jit(solution)/shard_map/all_to_all | solution.py:346
  99.8 4.0 %all-to-all-start.4 = ((bf16[16,160,128]{2,1,0:T(8,128)(2,1)}), bf16[16,160,128]{2,1,0:T(8,128)(2,1)S(1)}, u32[]{:S(2)}, u32[]{:S(2)}) async-start(bf16[16,160,128]{2,1,0:T(8,128)(2,1)} %shard_map.177), calls=%async_computation.4 | async-start | bytes 1310720 | tf_op jit(solution)/shard_map/all_to_all | solution.py:346
  103.8 2.0 collective-permute-start.4
  105.9 2.3 %collective-permute-start.5 = (bf16[2048,256]{1,0:T(8,128)(2,1)S(1)}, bf16[2048,256]{1,0:T(8,128)(2,1)S(1)}, u32[]{:S(2)}, u32[]{:S(2)}) collective-permute-start(bf16[2048,256]{1,0:T(8,128)(2,1)S(1)} %bitcast.34), channel_id=1, source_target_pairs={{0,1},{1,0},{2,3},{3,2},{4,5},{5,4},{6,7},{7,6},{8,9},{9,8},{10,11... | collective-permute-start | bytes 3145736 | tf_op jit(solution)/shard_map/ppermute | solution.py:354
  108.2 18.3 %collective-permute-done.6.refs_4_ = bf16[2048,256]{1,0:T(8,128)(2,1)} collective-permute-done((bf16[2048,256]{1,0:T(8,128)(2,1)S(1)}, bf16[2048,256]{1,0:T(8,128)(2,1)}, u32[]{:S(2)}, u32[]{:S(2)}) %collective-permute-start.6) | collective-permute-done | bytes 1048608 | tf_op jit(solution)/shard_map/ppermute | solution.py:358
  126.5 3.4 %collective-permute-start.12 = (bf16[256,2048]{1,0:T(8,128)(2,1)}, bf16[256,2048]{1,0:T(8,128)(2,1)S(1)}, u32[]{:S(2)}, u32[]{:S(2)}) collective-permute-start(bf16[256,2048]{1,0:T(8,128)(2,1)} %collective-permute-done.11.refs_10_), channel_id=1, source_target_pairs={{0,1},{1,0},{2,3},{3,2},{4,5},{5,4},{6,7},{7,6},{8,9},{9,8},{10,11... | collective-permute-start | bytes 3145736 | tf_op jit(solution)/shard_map/ppermute | solution.py:354
  129.9 19.0 %collective-permute-done.7.refs_5_ = bf16[2048,256]{1,0:T(8,128)(2,1)} collective-permute-done((bf16[2048,256]{1,0:T(8,128)(2,1)S(1)}, bf16[2048,256]{1,0:T(8,128)(2,1)}, u32[]{:S(2)}, u32[]{:S(2)}) %collective-permute-start.7) | collective-permute-done | bytes 1048608 | tf_op jit(solution)/shard_map/ppermute | solution.py:358
  148.9 3.4 %collective-permute-start.8 = (bf16[2048,256]{1,0:T(8,128)(2,1)}, bf16[2048,256]{1,0:T(8,128)(2,1)S(1)}, u32[]{:S(2)}, u32[]{:S(2)}) collective-permute-start(bf16[2048,256]{1,0:T(8,128)(2,1)} %collective-permute-done.6.refs_4_), channel_id=1, source_target_pairs={{0,1},{1,0},{2,3},{3,2},{4,5},{5,4},{6,7},{7,6},{8,9},{9,8},{10,11... | collective-permute-start | bytes 3145736 | tf_op jit(solution)/shard_map/ppermute | solution.py:354
  152.4 1.9 collective-permute-start.9
  157.3 5.7 %all-to-all-done.4.in_ref = bf16[16,160,128]{2,1,0:T(8,128)(2,1)S(1)} async-done(((bf16[16,160,128]{2,1,0:T(8,128)(2,1)}), bf16[16,160,128]{2,1,0:T(8,128)(2,1)S(1)}, u32[]{:S(2)}, u32[]{:S(2)}) %all-to-all-start.4) | async-done | bytes 655392 | tf_op jit(solution)/shard_map/all_to_all | solution.py:346
  163.0 6.1 %shard_map.178 = bf16[16,160,128]{2,1,0:T(8,128)(2,1)S(1)} custom-call(bf16[16,160,128]{2,1,0:T(8,128)(2,1)S(1)} %all-to-all-done.4.in_ref, f32[16,8,128]{2,1,0:T(8,128)S(1)} %get-tuple-element.13.gain_ref, bf16[2048,256]{1,0:T(8,128)(2,1)} %bitcast.29, bf16[2048,256]{1,0:T(8,128)(2,1)} %bitcast.32, bf16[2048,256]{1,0:T(8,128)(2,1)} %copy-done.9, ...), custom_call_target="tpu_custom_call" | custom-call | tf_op jit(solution)/shard_map/pallas_call | solution.py:335
  169.1 23.2 %all_to_all.36.in_ref = bf16[16,160,128]{2,1,0:T(8,128)(2,1)S(1)} all-to-all(bf16[16,160,128]{2,1,0:T(8,128)(2,1)S(1)} %shard_map.178), channel_id=1, replica_groups=mesh['z'=8,'x'=4,'y'=8,'c'=2] {'y','c'}, dimensions={0} | all-to-all | bytes 1310720 | tf_op jit(solution)/shard_map/all_to_all | solution.py:346
  193.2 5.7 %all-to-all-start.6 = ((bf16[32,24,128]{2,1,0:T(8,128)(2,1)}), bf16[32,24,128]{2,1,0:T(8,128)(2,1)S(1)}, u32[]{:S(2)}, u32[]{:S(2)}) async-start(bf16[32,24,128]{2,1,0:T(8,128)(2,1)} %bitcast.15), calls=%async_computation.6 | async-start | bytes 393216 | tf_op jit(solution)/shard_map/all_to_all | solution.py:346
  199.6 10.1 %all-to-all-done.6 = bf16[32,24,128]{2,1,0:T(8,128)(2,1)S(1)} async-done(((bf16[32,24,128]{2,1,0:T(8,128)(2,1)}), bf16[32,24,128]{2,1,0:T(8,128)(2,1)S(1)}, u32[]{:S(2)}, u32[]{:S(2)}) %all-to-all-start.6) | async-done | bytes 196640 | tf_op jit(solution)/shard_map/all_to_all | solution.py:346
  (44 shorter events, 8.0 us)
Async XLA Ops:
  2.3 11.0 %copy-start = (bf16[128,2048]{1,0:T(8,128)(2,1)S(1)}, bf16[128,2048]{1,0:T(8,128)(2,1)}, u32[]{:S(2)}) copy-start(bf16[128,2048]{1,0:T(8,128)(2,1)} %w_own_ref.1) | copy-start | bytes 1572868
  2.4 29.7 %all-to-all-start = ((bf16[8,272,128]{2,1,0:T(8,128)(2,1)}), bf16[8,272,128]{2,1,0:T(8,128)(2,1)S(1)}, u32[]{:S(2)}, u32[]{:S(2)}) async-start(bf16[8,272,128]{2,1,0:T(8,128)(2,1)} %get-tuple-element.11), calls=%async_computation | async-start | bytes 1114112 | tf_op jit(solution)/shard_map/all_to_all | solution.py:346
  13.4 32.3 %collective-permute-start.3 = (bf16[128,2048]{1,0:T(8,128)(2,1)S(1)}, bf16[128,2048]{1,0:T(8,128)(2,1)S(1)}, u32[]{:S(2)}, u32[]{:S(2)}) collective-permute-start(bf16[128,2048]{1,0:T(8,128)(2,1)S(1)} %copy-done), channel_id=1, source_target_pairs={{0,1},{1,0},{2,3},{3,2},{4,5},{5,4},{6,7},{7,6},{8,9},{9,8},{10,11... | collective-permute-start | bytes 1572872 | tf_op jit(solution)/shard_map/ppermute | solution.py:354
  16.2 10.6 %collective-permute-start = (bf16[272,128]{1,0:T(8,128)(2,1)S(1)}, bf16[272,128]{1,0:T(8,128)(2,1)S(1)}, u32[]{:S(2)}, u32[]{:S(2)}) collective-permute-start(bf16[272,128]{1,0:T(8,128)(2,1)S(1)} %get-tuple-element.10.refs_0_), channel_id=1, source_target_pairs={{0,16},{16,32},{32,48},{48,0},{1,17},{17,33},{33,49},{49,1},{2,18}... | collective-permute-start | bytes 208904 | tf_op jit(solution)/shard_map/ppermute | solution.py:350
  19.4 7.4 %collective-permute-start.1 = (bf16[272,128]{1,0:T(8,128)(2,1)S(1)}, bf16[272,128]{1,0:T(8,128)(2,1)S(1)}, u32[]{:S(2)}, u32[]{:S(2)}) collective-permute-start(bf16[272,128]{1,0:T(8,128)(2,1)S(1)} %get-tuple-element.10.refs_0_), channel_id=1, source_target_pairs={{0,32},{16,48},{32,0},{48,16},{1,33},{17,49},{33,1},{49,17},{2,34}... | collective-permute-start | bytes 208904 | tf_op jit(solution)/shard_map/ppermute | solution.py:350
  23.7 5.1 %collective-permute-start.2 = (bf16[272,128]{1,0:T(8,128)(2,1)S(1)}, bf16[272,128]{1,0:T(8,128)(2,1)S(1)}, u32[]{:S(2)}, u32[]{:S(2)}) collective-permute-start(bf16[272,128]{1,0:T(8,128)(2,1)S(1)} %get-tuple-element.10.refs_0_), channel_id=1, source_target_pairs={{0,48},{16,0},{32,16},{48,32},{1,49},{17,1},{33,17},{49,33},{2,50}... | collective-permute-start | bytes 208904 | tf_op jit(solution)/shard_map/ppermute | solution.py:350
  40.9 11.6 %all-to-all-start.1 = ((bf16[8,144,128]{2,1,0:T(8,128)(2,1)}), bf16[8,144,128]{2,1,0:T(8,128)(2,1)S(1)}, u32[]{:S(2)}, u32[]{:S(2)}) async-start(bf16[8,144,128]{2,1,0:T(8,128)(2,1)} %shard_map.173), calls=%async_computation.1 | async-start | bytes 589824 | tf_op jit(solution)/shard_map/all_to_all | solution.py:346
  52.4 0.7 copy-start.6
  53.1 15.2 %copy-start.8 = (bf16[1,2048,256]{2,1,0:T(8,128)(2,1)S(1)}, bf16[1,2048,256]{2,1,0:T(8,128)(2,1)}, u32[]{:S(2)}) copy-start(bf16[1,2048,256]{2,1,0:T(8,128)(2,1)} %param.30) | copy-start | bytes 3145732
  54.7 11.6 %copy-start.7 = (bf16[1,2048,256]{2,1,0:T(8,128)(2,1)S(1)}, bf16[1,2048,256]{2,1,0:T(8,128)(2,1)}, u32[]{:S(2)}) copy-start(bf16[1,2048,256]{2,1,0:T(8,128)(2,1)} %param.29) | copy-start | bytes 3145732
  54.7 27.1 %all-to-all-start.2 = ((bf16[16,144,128]{2,1,0:T(8,128)(2,1)}), bf16[16,144,128]{2,1,0:T(8,128)(2,1)S(1)}, u32[]{:S(2)}, u32[]{:S(2)}) async-start(bf16[16,144,128]{2,1,0:T(8,128)(2,1)} %shard_map.174), calls=%async_computation.2 | async-start | bytes 1179648 | tf_op jit(solution)/shard_map/all_to_all | solution.py:346
  63.0 42.9 %collective-permute-start.11 = (bf16[256,2048]{1,0:T(8,128)(2,1)}, bf16[256,2048]{1,0:T(8,128)(2,1)}, u32[]{:S(2)}, u32[]{:S(2)}) collective-permute-start(bf16[256,2048]{1,0:T(8,128)(2,1)} %bitcast.35), channel_id=1, source_target_pairs={{0,2},{2,0},{4,6},{6,4},{8,10},{10,8},{12,14},{14,12},{1,3},{3,1},... | collective-permute-start | bytes 3145736 | tf_op jit(solution)/shard_map/ppermute | solution.py:358
  66.3 8.5 %copy-start.4 = (s32[256,2]{0,1:T(2,128)S(1)}, s32[256,2]{0,1:T(2,128)}, u32[]{:S(2)}) copy-start(s32[256,2]{0,1:T(2,128)} %param.27) | copy-start | bytes 6148
  66.3 60.2 %collective-permute-start.6 = (bf16[2048,256]{1,0:T(8,128)(2,1)S(1)}, bf16[2048,256]{1,0:T(8,128)(2,1)}, u32[]{:S(2)}, u32[]{:S(2)}) collective-permute-start(bf16[2048,256]{1,0:T(8,128)(2,1)S(1)} %bitcast.30), channel_id=1, source_target_pairs={{0,2},{2,0},{4,6},{6,4},{8,10},{10,8},{12,14},{14,12},{1,3},{3,1},... | collective-permute-start | bytes 3145736 | tf_op jit(solution)/shard_map/ppermute | solution.py:358
  68.3 80.6 %collective-permute-start.7 = (bf16[2048,256]{1,0:T(8,128)(2,1)S(1)}, bf16[2048,256]{1,0:T(8,128)(2,1)}, u32[]{:S(2)}, u32[]{:S(2)}) collective-permute-start(bf16[2048,256]{1,0:T(8,128)(2,1)S(1)} %bitcast.33), channel_id=1, source_target_pairs={{0,2},{2,0},{4,6},{6,4},{8,10},{10,8},{12,14},{14,12},{1,3},{3,1},... | collective-permute-start | bytes 3145736 | tf_op jit(solution)/shard_map/ppermute | solution.py:358
  71.6 80.8 %collective-permute-start.10 = (bf16[256,2048]{1,0:T(8,128)(2,1)}, bf16[256,2048]{1,0:T(8,128)(2,1)}, u32[]{:S(2)}, u32[]{:S(2)}) collective-permute-start(bf16[256,2048]{1,0:T(8,128)(2,1)} %bitcast.36), channel_id=1, source_target_pairs={{0,1},{1,0},{2,3},{3,2},{4,5},{5,4},{6,7},{7,6},{8,9},{9,8},{10,11... | collective-permute-start | bytes 3145736 | tf_op jit(solution)/shard_map/ppermute | solution.py:354
  74.8 7.0 %copy-start.3 = (bf16[256,128]{1,0:T(8,128)(2,1)S(1)}, bf16[256,128]{1,0:T(8,128)(2,1)}, u32[]{:S(2)}) copy-start(bf16[256,128]{1,0:T(8,128)(2,1)} %residual_ref.1) | copy-start | bytes 196612
  82.0 16.7 %copy-start.2 = (bf16[160,192]{1,0:T(8,128)(2,1)S(1)}, bf16[160,192]{1,0:T(8,128)(2,1)}, u32[]{:S(2)}) copy-start(bf16[160,192]{1,0:T(8,128)(2,1)} %constant.28.clone.drop_ref) | copy-start | bytes 184324
  99.8 63.1 %all-to-all-start.4 = ((bf16[16,160,128]{2,1,0:T(8,128)(2,1)}), bf16[16,160,128]{2,1,0:T(8,128)(2,1)S(1)}, u32[]{:S(2)}, u32[]{:S(2)}) async-start(bf16[16,160,128]{2,1,0:T(8,128)(2,1)} %shard_map.177), calls=%async_computation.4 | async-start | bytes 1310720 | tf_op jit(solution)/shard_map/all_to_all | solution.py:346
  103.8 50.5 %collective-permute-start.4 = (bf16[2048,256]{1,0:T(8,128)(2,1)S(1)}, bf16[2048,256]{1,0:T(8,128)(2,1)S(1)}, u32[]{:S(2)}, u32[]{:S(2)}) collective-permute-start(bf16[2048,256]{1,0:T(8,128)(2,1)S(1)} %bitcast.31), channel_id=1, source_target_pairs={{0,1},{1,0},{2,3},{3,2},{4,5},{5,4},{6,7},{7,6},{8,9},{9,8},{10,11... | collective-permute-start | bytes 3145736 | tf_op jit(solution)/shard_map/ppermute | solution.py:354
  105.9 48.5 %collective-permute-start.5 = (bf16[2048,256]{1,0:T(8,128)(2,1)S(1)}, bf16[2048,256]{1,0:T(8,128)(2,1)S(1)}, u32[]{:S(2)}, u32[]{:S(2)}) collective-permute-start(bf16[2048,256]{1,0:T(8,128)(2,1)S(1)} %bitcast.34), channel_id=1, source_target_pairs={{0,1},{1,0},{2,3},{3,2},{4,5},{5,4},{6,7},{7,6},{8,9},{9,8},{10,11... | collective-permute-start | bytes 3145736 | tf_op jit(solution)/shard_map/ppermute | solution.py:354
  126.5 27.9 %collective-permute-start.12 = (bf16[256,2048]{1,0:T(8,128)(2,1)}, bf16[256,2048]{1,0:T(8,128)(2,1)S(1)}, u32[]{:S(2)}, u32[]{:S(2)}) collective-permute-start(bf16[256,2048]{1,0:T(8,128)(2,1)} %collective-permute-done.11.refs_10_), channel_id=1, source_target_pairs={{0,1},{1,0},{2,3},{3,2},{4,5},{5,4},{6,7},{7,6},{8,9},{9,8},{10,11... | collective-permute-start | bytes 3145736 | tf_op jit(solution)/shard_map/ppermute | solution.py:354
  148.9 5.9 %collective-permute-start.8 = (bf16[2048,256]{1,0:T(8,128)(2,1)}, bf16[2048,256]{1,0:T(8,128)(2,1)S(1)}, u32[]{:S(2)}, u32[]{:S(2)}) collective-permute-start(bf16[2048,256]{1,0:T(8,128)(2,1)} %collective-permute-done.6.refs_4_), channel_id=1, source_target_pairs={{0,1},{1,0},{2,3},{3,2},{4,5},{5,4},{6,7},{7,6},{8,9},{9,8},{10,11... | collective-permute-start | bytes 3145736 | tf_op jit(solution)/shard_map/ppermute | solution.py:354
  152.4 4.9 %collective-permute-start.9 = (bf16[2048,256]{1,0:T(8,128)(2,1)}, bf16[2048,256]{1,0:T(8,128)(2,1)}, u32[]{:S(2)}, u32[]{:S(2)}) collective-permute-start(bf16[2048,256]{1,0:T(8,128)(2,1)} %collective-permute-done.7.refs_5_), channel_id=1, source_target_pairs={{0,1},{1,0},{2,3},{3,2},{4,5},{5,4},{6,7},{7,6},{8,9},{9,8},{10,11... | collective-permute-start | bytes 3145736 | tf_op jit(solution)/shard_map/ppermute | solution.py:354
  154.3 1.0 copy-start.9
  154.3 1.4 copy-start.10
  154.4 1.7 copy-start.11
  156.1 1.0 copy-start.12
  169.1 23.2 %copy-start.1 = (bf16[192,160]{1,0:T(8,128)(2,1)S(1)}, bf16[192,160]{1,0:T(8,128)(2,1)}, u32[]{:S(2)}) copy-start(bf16[192,160]{1,0:T(8,128)(2,1)} %constant.29.clone.widen_ref) | copy-start | bytes 184324
  193.2 5.7 %copy-start.5 = (f32[256,2]{0,1:T(2,128)S(1)}, f32[256,2]{0,1:T(2,128)}, u32[]{:S(2)}) copy-start(f32[256,2]{0,1:T(2,128)} %param.28) | copy-start | bytes 6148
  193.2 16.4 %all-to-all-start.6 = ((bf16[32,24,128]{2,1,0:T(8,128)(2,1)}), bf16[32,24,128]{2,1,0:T(8,128)(2,1)S(1)}, u32[]{:S(2)}, u32[]{:S(2)}) async-start(bf16[32,24,128]{2,1,0:T(8,128)(2,1)} %bitcast.15), calls=%async_computation.6 | async-start | bytes 393216 | tf_op jit(solution)/shard_map/all_to_all | solution.py:346

commit v4 on v3

--- a/solution.py
+++ b/solution.py
@@ -235,10 +235,11 @@
     weight = jnp.where(first, weight_ref[0:1, :], jnp.where(second, weight_ref[1:2, :], 0.0))
     part = split3(weight)[term]
 
-    def write(rows, value):
-        mix_ref[rows, :] = value
-
-    laid_out(slot, lambda e: part[e : e + 1, :], write)
+    parts = []
+    laid_out(slot, lambda e: part[e : e + 1, :], lambda rows, value: parts.append(value))
+    for i in range(0, len(parts), 8):
+        some = jnp.concatenate(parts[i : i + 8], axis=0).astype(F32)
+        mix_ref[:, i * 2 * CAP_PAD : (i + 8) * 2 * CAP_PAD] = some.T.astype(BF16)
 
 
 def dispatch_body(in_ref, residual_ref, place_ref, mixed_ref, gain_ref, out_ref):
@@ -314,12 +315,12 @@
     total = mixed_ref[...]
     rows = in_ref[...]
     for mix_ref in (mix0_ref, mix1_ref, mix2_ref):
-        total = total + dot(mix_ref[...], rows, 0, 0)
+        total = total + dot(mix_ref[...], rows)
     out_ref[...] = total.astype(BF16)
 
 
 def shaped(shape, dtype=BF16):
-    return jax.ShapeDtypeStruct(shape, dtype)
+    return pltpu.VMEM(shape, dtype)
 
 
 VMEM = pl.BlockSpec(memory_space=pltpu.VMEM)
@@ -442,9 +443,10 @@
     gate_yo, up_yo = partner(gate_y), partner(up_y)
     down_yo = partner(down_y)
     slot_table = shaped((EXPERTS * CAP_PAD, TOK))
+    mix_table = shaped((TOK, EXPERTS * CAP_PAD))
     place = call(route_body, slot_table, routes)
     mixes = [
-        call(functools.partial(mix_body, i), slot_table, routes, route_weight)
+        call(functools.partial(mix_body, i), mix_table, routes, route_weight)
         for i in range(3)
     ]
     partial = call(
@@ -509,7 +511,11 @@
     )
     returned = exchange(expert_out.reshape(N_SP, CAP_PAD, LANES), ("z", "x"))
     return call(
-        finish_body, shaped((TOK, LANES)), returned.reshape(N_SP * CAP_PAD, LANES), *mixes, mixed
+        finish_body,
+        jax.ShapeDtypeStruct((TOK, LANES), BF16),
+        returned.reshape(N_SP * CAP_PAD, LANES),
+        *mixes,
+        mixed,
     )
 
 

time: 212 us -> 212 us (level)
  no operation moved by 1% of the time
where the time goes in v4:
time: 212 us; the launch traced here: 211 us
  waiting for transfers between devices  72.2 us (34%)
  starting transfers between devices  72 us (34%)
  blocking collectives  39.9 us (19%)
  Pallas kernels  23.5 us (11%)
  local copies, waits for them, and re-layouts  2.87 us (1%)
    all_to_all x2, blocking collectives, exchange(): return lax.all_to_all(x, axes, 0, 0, tiled=True)  39.9 us
    ppermute x3, waiting for transfers between devices, neighbour(): return lax.ppermute(x, 'y', [(i, i ^ 1) for i in range(N_Y)])  37.3 us
    all_to_all x5, starting transfers between devices, exchange(): return lax.all_to_all(x, axes, 0, 0, tiled=True)  33.8 us
    all_to_all x5, waiting for transfers between devices, exchange(): return lax.all_to_all(x, axes, 0, 0, tiled=True)  32.2 us
    pallas_call x12, Pallas kernels, call(): pl.pallas_call(body, out_shape=outs, in_specs=specs, out_specs=[VMEM] * l...  23.5 us
    ppermute x7, starting transfers between devices, partner(): return lax.ppermute(x, 'c', [(0, 1), (1, 0)])  19.1 us
    ppermute x3, starting transfers between devices, shifted(): return lax.ppermute(x, axis, [(i, (i + by) % size) for i in range(size)])  10.5 us
    ppermute x3, starting transfers between devices, neighbour(): return lax.ppermute(x, 'y', [(i, i ^ 1) for i in range(N_Y)])  8.54 us
  transfers between devices with their start and end apart: 18, of which 10 were waited for; matrix products, arithmetic and copies ran while one was open for 0% of the time, Pallas kernels for 5%

profile of v4, /device:TPU:1, one launch (start us, length us, event | category | flops | bytes accessed | tf_op | source)
XLA Modules:
  0.0 210.8 jit_solution(3499622125774613831)
XLA Ops:
  0.0 2.3 %shard_map.172 = (bf16[272,128]{1,0:T(8,128)(2,1)S(1)}, bf16[8,272,128]{2,1,0:T(8,128)(2,1)}) custom-call(s32[1]{0:T(128)} %bitcast.2.blk, bf16[256,128]{1,0:T(8,128)(2,1)} %refs_0_.1, bf16[64,256]{1,0:T(8,128)(2,1)} %bitcast.38, bf16[64,256]{1,0:T(8,128)(2,1)} %bitcast.39, s32[2,128]{1,0:T(2,128)} %bitcast.40, f32[1,64]{1,0:T(1,128)} %bitcast.41, ...), custom_call_target="tpu_custom_call" | custom-call | tf_op jit(solution)/shard_map/pallas_call | solution.py:336
  2.4 11.0 %all-to-all-start = ((bf16[8,272,128]{2,1,0:T(8,128)(2,1)}), bf16[8,272,128]{2,1,0:T(8,128)(2,1)S(1)}, u32[]{:S(2)}, u32[]{:S(2)}) async-start(bf16[8,272,128]{2,1,0:T(8,128)(2,1)} %get-tuple-element.11), calls=%async_computation | async-start | bytes 1114112 | tf_op jit(solution)/shard_map/all_to_all | solution.py:347
  13.4 2.9 %collective-permute-start.3 = (bf16[128,2048]{1,0:T(8,128)(2,1)S(1)}, bf16[128,2048]{1,0:T(8,128)(2,1)S(1)}, u32[]{:S(2)}, u32[]{:S(2)}) collective-permute-start(bf16[128,2048]{1,0:T(8,128)(2,1)S(1)} %copy-done), channel_id=1, source_target_pairs={{0,1},{1,0},{2,3},{3,2},{4,5},{5,4},{6,7},{7,6},{8,9},{9,8},{10,11... | collective-permute-start | bytes 1572872 | tf_op jit(solution)/shard_map/ppermute | solution.py:355
  16.2 3.1 %collective-permute-start = (bf16[272,128]{1,0:T(8,128)(2,1)S(1)}, bf16[272,128]{1,0:T(8,128)(2,1)S(1)}, u32[]{:S(2)}, u32[]{:S(2)}) collective-permute-start(bf16[272,128]{1,0:T(8,128)(2,1)S(1)} %get-tuple-element.10.refs_0_), channel_id=1, source_target_pairs={{0,16},{16,32},{32,48},{48,0},{1,17},{17,33},{33,49},{49,1},{2,18}... | collective-permute-start | bytes 208904 | tf_op jit(solution)/shard_map/ppermute | solution.py:351
  19.4 4.4 %collective-permute-start.1 = (bf16[272,128]{1,0:T(8,128)(2,1)S(1)}, bf16[272,128]{1,0:T(8,128)(2,1)S(1)}, u32[]{:S(2)}, u32[]{:S(2)}) collective-permute-start(bf16[272,128]{1,0:T(8,128)(2,1)S(1)} %get-tuple-element.10.refs_0_), channel_id=1, source_target_pairs={{0,32},{16,48},{32,0},{48,16},{1,33},{17,49},{33,1},{49,17},{2,34}... | collective-permute-start | bytes 208904 | tf_op jit(solution)/shard_map/ppermute | solution.py:351
  23.7 3.1 %collective-permute-start.2 = (bf16[272,128]{1,0:T(8,128)(2,1)S(1)}, bf16[272,128]{1,0:T(8,128)(2,1)S(1)}, u32[]{:S(2)}, u32[]{:S(2)}) collective-permute-start(bf16[272,128]{1,0:T(8,128)(2,1)S(1)} %get-tuple-element.10.refs_0_), channel_id=1, source_target_pairs={{0,48},{16,0},{32,16},{48,32},{1,49},{17,1},{33,17},{49,33},{2,50}... | collective-permute-start | bytes 208904 | tf_op jit(solution)/shard_map/ppermute | solution.py:351
  26.8 2.0 collective-permute-done.2.refs_3_
  28.8 3.2 %all-to-all-done.refs_4_ = bf16[8,272,128]{2,1,0:T(8,128)(2,1)S(1)} async-done(((bf16[8,272,128]{2,1,0:T(8,128)(2,1)}), bf16[8,272,128]{2,1,0:T(8,128)(2,1)S(1)}, u32[]{:S(2)}, u32[]{:S(2)}) %all-to-all-start) | async-done | bytes 557088 | tf_op jit(solution)/shard_map/all_to_all | solution.py:347
  32.0 8.8 %shard_map.173 = bf16[8,144,128]{2,1,0:T(8,128)(2,1)} custom-call(s32[1]{0:T(128)} %bitcast.1.spot, bf16[272,128]{1,0:T(8,128)(2,1)S(1)} %get-tuple-element.10.refs_0_, bf16[272,128]{1,0:T(8,128)(2,1)S(1)} %collective-permute-done.refs_1_, bf16[272,128]{1,0:T(8,128)(2,1)S(1)} %collective-permute-done.1.refs_2_, ...), custom_call_target="tpu_custom_call" | custom-call | tf_op jit(solution)/shard_map/pallas_call | solution.py:336
  40.9 4.8 %all-to-all-start.1 = ((bf16[8,144,128]{2,1,0:T(8,128)(2,1)}), bf16[8,144,128]{2,1,0:T(8,128)(2,1)S(1)}, u32[]{:S(2)}, u32[]{:S(2)}) async-start(bf16[8,144,128]{2,1,0:T(8,128)(2,1)} %shard_map.173), calls=%async_computation.1 | async-start | bytes 589824 | tf_op jit(solution)/shard_map/all_to_all | solution.py:347
  45.6 6.8 %all-to-all-done.1.in_ref = bf16[8,144,128]{2,1,0:T(8,128)(2,1)S(1)} async-done(((bf16[8,144,128]{2,1,0:T(8,128)(2,1)}), bf16[8,144,128]{2,1,0:T(8,128)(2,1)S(1)}, u32[]{:S(2)}, u32[]{:S(2)}) %all-to-all-start.1) | async-done | bytes 294944 | tf_op jit(solution)/shard_map/all_to_all | solution.py:347
  53.1 1.6 shard_map.174
  54.7 8.3 %all-to-all-start.2 = ((bf16[16,144,128]{2,1,0:T(8,128)(2,1)}), bf16[16,144,128]{2,1,0:T(8,128)(2,1)S(1)}, u32[]{:S(2)}, u32[]{:S(2)}) async-start(bf16[16,144,128]{2,1,0:T(8,128)(2,1)} %shard_map.174), calls=%async_computation.2 | async-start | bytes 1179648 | tf_op jit(solution)/shard_map/all_to_all | solution.py:347
  63.0 3.3 %collective-permute-start.11 = (bf16[256,2048]{1,0:T(8,128)(2,1)}, bf16[256,2048]{1,0:T(8,128)(2,1)}, u32[]{:S(2)}, u32[]{:S(2)}) collective-permute-start(bf16[256,2048]{1,0:T(8,128)(2,1)} %bitcast.35), channel_id=1, source_target_pairs={{0,2},{2,0},{4,6},{6,4},{8,10},{10,8},{12,14},{14,12},{1,3},{3,1},... | collective-permute-start | bytes 3145736 | tf_op jit(solution)/shard_map/ppermute | solution.py:359
  66.3 2.0 collective-permute-start.6
  68.3 3.3 %collective-permute-start.7 = (bf16[2048,256]{1,0:T(8,128)(2,1)S(1)}, bf16[2048,256]{1,0:T(8,128)(2,1)}, u32[]{:S(2)}, u32[]{:S(2)}) collective-permute-start(bf16[2048,256]{1,0:T(8,128)(2,1)S(1)} %bitcast.33), channel_id=1, source_target_pairs={{0,2},{2,0},{4,6},{6,4},{8,10},{10,8},{12,14},{14,12},{1,3},{3,1},... | collective-permute-start | bytes 3145736 | tf_op jit(solution)/shard_map/ppermute | solution.py:359
  71.6 3.1 %collective-permute-start.10 = (bf16[256,2048]{1,0:T(8,128)(2,1)}, bf16[256,2048]{1,0:T(8,128)(2,1)}, u32[]{:S(2)}, u32[]{:S(2)}) collective-permute-start(bf16[256,2048]{1,0:T(8,128)(2,1)} %bitcast.36), channel_id=1, source_target_pairs={{0,1},{1,0},{2,3},{3,2},{4,5},{5,4},{6,7},{7,6},{8,9},{9,8},{10,11... | collective-permute-start | bytes 3145736 | tf_op jit(solution)/shard_map/ppermute | solution.py:355
  75.0 6.7 %all-to-all-done.2.in_ref = bf16[16,144,128]{2,1,0:T(8,128)(2,1)S(1)} async-done(((bf16[16,144,128]{2,1,0:T(8,128)(2,1)}), bf16[16,144,128]{2,1,0:T(8,128)(2,1)S(1)}, u32[]{:S(2)}, u32[]{:S(2)}) %all-to-all-start.2) | async-done | bytes 589856 | tf_op jit(solution)/shard_map/all_to_all | solution.py:347
  82.1 16.7 %all_to_all.35 = bf16[32,24,128]{2,1,0:T(8,128)(2,1)S(1)} all-to-all(bf16[32,24,128]{2,1,0:T(8,128)(2,1)S(1)} %bitcast.20), channel_id=1, replica_groups=mesh['z'=8,'x'=4,'y'=8,'c'=2] {'z','x'}, dimensions={0} | all-to-all | bytes 393216 | tf_op jit(solution)/shard_map/all_to_all | solution.py:347
  99.8 4.0 %all-to-all-start.4 = ((bf16[16,160,128]{2,1,0:T(8,128)(2,1)}), bf16[16,160,128]{2,1,0:T(8,128)(2,1)S(1)}, u32[]{:S(2)}, u32[]{:S(2)}) async-start(bf16[16,160,128]{2,1,0:T(8,128)(2,1)} %shard_map.177), calls=%async_computation.4 | async-start | bytes 1310720 | tf_op jit(solution)/shard_map/all_to_all | solution.py:347
  103.8 2.0 collective-permute-start.4
  105.9 2.3 %collective-permute-start.5 = (bf16[2048,256]{1,0:T(8,128)(2,1)S(1)}, bf16[2048,256]{1,0:T(8,128)(2,1)S(1)}, u32[]{:S(2)}, u32[]{:S(2)}) collective-permute-start(bf16[2048,256]{1,0:T(8,128)(2,1)S(1)} %bitcast.34), channel_id=1, source_target_pairs={{0,1},{1,0},{2,3},{3,2},{4,5},{5,4},{6,7},{7,6},{8,9},{9,8},{10,11... | collective-permute-start | bytes 3145736 | tf_op jit(solution)/shard_map/ppermute | solution.py:355
  108.2 18.3 %collective-permute-done.6.refs_4_ = bf16[2048,256]{1,0:T(8,128)(2,1)} collective-permute-done((bf16[2048,256]{1,0:T(8,128)(2,1)S(1)}, bf16[2048,256]{1,0:T(8,128)(2,1)}, u32[]{:S(2)}, u32[]{:S(2)}) %collective-permute-start.6) | collective-permute-done | bytes 1048608 | tf_op jit(solution)/shard_map/ppermute | solution.py:359
  126.5 3.4 %collective-permute-start.12 = (bf16[256,2048]{1,0:T(8,128)(2,1)}, bf16[256,2048]{1,0:T(8,128)(2,1)S(1)}, u32[]{:S(2)}, u32[]{:S(2)}) collective-permute-start(bf16[256,2048]{1,0:T(8,128)(2,1)} %collective-permute-done.11.refs_10_), channel_id=1, source_target_pairs={{0,1},{1,0},{2,3},{3,2},{4,5},{5,4},{6,7},{7,6},{8,9},{9,8},{10,11... | collective-permute-start | bytes 3145736 | tf_op jit(solution)/shard_map/ppermute | solution.py:355
  129.9 19.0 %collective-permute-done.7.refs_5_ = bf16[2048,256]{1,0:T(8,128)(2,1)} collective-permute-done((bf16[2048,256]{1,0:T(8,128)(2,1)S(1)}, bf16[2048,256]{1,0:T(8,128)(2,1)}, u32[]{:S(2)}, u32[]{:S(2)}) %collective-permute-start.7) | collective-permute-done | bytes 1048608 | tf_op jit(solution)/shard_map/ppermute | solution.py:359
  148.9 3.4 %collective-permute-start.8 = (bf16[2048,256]{1,0:T(8,128)(2,1)}, bf16[2048,256]{1,0:T(8,128)(2,1)S(1)}, u32[]{:S(2)}, u32[]{:S(2)}) collective-permute-start(bf16[2048,256]{1,0:T(8,128)(2,1)} %collective-permute-done.6.refs_4_), channel_id=1, source_target_pairs={{0,1},{1,0},{2,3},{3,2},{4,5},{5,4},{6,7},{7,6},{8,9},{9,8},{10,11... | collective-permute-start | bytes 3145736 | tf_op jit(solution)/shard_map/ppermute | solution.py:355
  152.4 1.9 collective-permute-start.9
  157.3 5.7 %all-to-all-done.4.in_ref = bf16[16,160,128]{2,1,0:T(8,128)(2,1)S(1)} async-done(((bf16[16,160,128]{2,1,0:T(8,128)(2,1)}), bf16[16,160,128]{2,1,0:T(8,128)(2,1)S(1)}, u32[]{:S(2)}, u32[]{:S(2)}) %all-to-all-start.4) | async-done | bytes 655392 | tf_op jit(solution)/shard_map/all_to_all | solution.py:347
  163.0 6.1 %shard_map.178 = bf16[16,160,128]{2,1,0:T(8,128)(2,1)S(1)} custom-call(bf16[16,160,128]{2,1,0:T(8,128)(2,1)S(1)} %all-to-all-done.4.in_ref, f32[16,8,128]{2,1,0:T(8,128)S(1)} %get-tuple-element.13.gain_ref, bf16[2048,256]{1,0:T(8,128)(2,1)} %bitcast.29, bf16[2048,256]{1,0:T(8,128)(2,1)} %bitcast.32, bf16[2048,256]{1,0:T(8,128)(2,1)} %copy-done.9, ...), custom_call_target="tpu_custom_call" | custom-call | tf_op jit(solution)/shard_map/pallas_call | solution.py:336
  169.1 23.2 %all_to_all.36.in_ref = bf16[16,160,128]{2,1,0:T(8,128)(2,1)S(1)} all-to-all(bf16[16,160,128]{2,1,0:T(8,128)(2,1)S(1)} %shard_map.178), channel_id=1, replica_groups=mesh['z'=8,'x'=4,'y'=8,'c'=2] {'y','c'}, dimensions={0} | all-to-all | bytes 1310720 | tf_op jit(solution)/shard_map/all_to_all | solution.py:347
  193.2 5.7 %all-to-all-start.6 = ((bf16[32,24,128]{2,1,0:T(8,128)(2,1)}), bf16[32,24,128]{2,1,0:T(8,128)(2,1)S(1)}, u32[]{:S(2)}, u32[]{:S(2)}) async-start(bf16[32,24,128]{2,1,0:T(8,128)(2,1)} %bitcast.15), calls=%async_computation.6 | async-start | bytes 393216 | tf_op jit(solution)/shard_map/all_to_all | solution.py:347
  199.9 9.8 %all-to-all-done.6 = bf16[32,24,128]{2,1,0:T(8,128)(2,1)S(1)} async-done(((bf16[32,24,128]{2,1,0:T(8,128)(2,1)}), bf16[32,24,128]{2,1,0:T(8,128)(2,1)S(1)}, u32[]{:S(2)}, u32[]{:S(2)}) %all-to-all-start.6) | async-done | bytes 196640 | tf_op jit(solution)/shard_map/all_to_all | solution.py:347
  (44 shorter events, 8.3 us)
Async XLA Ops:
  2.3 11.0 %copy-start = (bf16[128,2048]{1,0:T(8,128)(2,1)S(1)}, bf16[128,2048]{1,0:T(8,128)(2,1)}, u32[]{:S(2)}) copy-start(bf16[128,2048]{1,0:T(8,128)(2,1)} %w_own_ref.1) | copy-start | bytes 1572868
  2.4 29.7 %all-to-all-start = ((bf16[8,272,128]{2,1,0:T(8,128)(2,1)}), bf16[8,272,128]{2,1,0:T(8,128)(2,1)S(1)}, u32[]{:S(2)}, u32[]{:S(2)}) async-start(bf16[8,272,128]{2,1,0:T(8,128)(2,1)} %get-tuple-element.11), calls=%async_computation | async-start | bytes 1114112 | tf_op jit(solution)/shard_map/all_to_all | solution.py:347
  13.4 32.3 %collective-permute-start.3 = (bf16[128,2048]{1,0:T(8,128)(2,1)S(1)}, bf16[128,2048]{1,0:T(8,128)(2,1)S(1)}, u32[]{:S(2)}, u32[]{:S(2)}) collective-permute-start(bf16[128,2048]{1,0:T(8,128)(2,1)S(1)} %copy-done), channel_id=1, source_target_pairs={{0,1},{1,0},{2,3},{3,2},{4,5},{5,4},{6,7},{7,6},{8,9},{9,8},{10,11... | collective-permute-start | bytes 1572872 | tf_op jit(solution)/shard_map/ppermute | solution.py:355
  16.2 10.6 %collective-permute-start = (bf16[272,128]{1,0:T(8,128)(2,1)S(1)}, bf16[272,128]{1,0:T(8,128)(2,1)S(1)}, u32[]{:S(2)}, u32[]{:S(2)}) collective-permute-start(bf16[272,128]{1,0:T(8,128)(2,1)S(1)} %get-tuple-element.10.refs_0_), channel_id=1, source_target_pairs={{0,16},{16,32},{32,48},{48,0},{1,17},{17,33},{33,49},{49,1},{2,18}... | collective-permute-start | bytes 208904 | tf_op jit(solution)/shard_map/ppermute | solution.py:351
  19.4 7.4 %collective-permute-start.1 = (bf16[272,128]{1,0:T(8,128)(2,1)S(1)}, bf16[272,128]{1,0:T(8,128)(2,1)S(1)}, u32[]{:S(2)}, u32[]{:S(2)}) collective-permute-start(bf16[272,128]{1,0:T(8,128)(2,1)S(1)} %get-tuple-element.10.refs_0_), channel_id=1, source_target_pairs={{0,32},{16,48},{32,0},{48,16},{1,33},{17,49},{33,1},{49,17},{2,34}... | collective-permute-start | bytes 208904 | tf_op jit(solution)/shard_map/ppermute | solution.py:351
  23.7 5.1 %collective-permute-start.2 = (bf16[272,128]{1,0:T(8,128)(2,1)S(1)}, bf16[272,128]{1,0:T(8,128)(2,1)S(1)}, u32[]{:S(2)}, u32[]{:S(2)}) collective-permute-start(bf16[272,128]{1,0:T(8,128)(2,1)S(1)} %get-tuple-element.10.refs_0_), channel_id=1, source_target_pairs={{0,48},{16,0},{32,16},{48,32},{1,49},{17,1},{33,17},{49,33},{2,50}... | collective-permute-start | bytes 208904 | tf_op jit(solution)/shard_map/ppermute | solution.py:351
  40.9 11.6 %all-to-all-start.1 = ((bf16[8,144,128]{2,1,0:T(8,128)(2,1)}), bf16[8,144,128]{2,1,0:T(8,128)(2,1)S(1)}, u32[]{:S(2)}, u32[]{:S(2)}) async-start(bf16[8,144,128]{2,1,0:T(8,128)(2,1)} %shard_map.173), calls=%async_computation.1 | async-start | bytes 589824 | tf_op jit(solution)/shard_map/all_to_all | solution.py:347
  52.4 0.7 copy-start.6
  53.1 15.2 %copy-start.8 = (bf16[1,2048,256]{2,1,0:T(8,128)(2,1)S(1)}, bf16[1,2048,256]{2,1,0:T(8,128)(2,1)}, u32[]{:S(2)}) copy-start(bf16[1,2048,256]{2,1,0:T(8,128)(2,1)} %param.30) | copy-start | bytes 3145732
  54.7 11.6 %copy-start.7 = (bf16[1,2048,256]{2,1,0:T(8,128)(2,1)S(1)}, bf16[1,2048,256]{2,1,0:T(8,128)(2,1)}, u32[]{:S(2)}) copy-start(bf16[1,2048,256]{2,1,0:T(8,128)(2,1)} %param.29) | copy-start | bytes 3145732
  54.7 27.1 %all-to-all-start.2 = ((bf16[16,144,128]{2,1,0:T(8,128)(2,1)}), bf16[16,144,128]{2,1,0:T(8,128)(2,1)S(1)}, u32[]{:S(2)}, u32[]{:S(2)}) async-start(bf16[16,144,128]{2,1,0:T(8,128)(2,1)} %shard_map.174), calls=%async_computation.2 | async-start | bytes 1179648 | tf_op jit(solution)/shard_map/all_to_all | solution.py:347
  63.0 42.9 %collective-permute-start.11 = (bf16[256,2048]{1,0:T(8,128)(2,1)}, bf16[256,2048]{1,0:T(8,128)(2,1)}, u32[]{:S(2)}, u32[]{:S(2)}) collective-permute-start(bf16[256,2048]{1,0:T(8,128)(2,1)} %bitcast.35), channel_id=1, source_target_pairs={{0,2},{2,0},{4,6},{6,4},{8,10},{10,8},{12,14},{14,12},{1,3},{3,1},... | collective-permute-start | bytes 3145736 | tf_op jit(solution)/shard_map/ppermute | solution.py:359
  66.3 8.5 %copy-start.4 = (s32[256,2]{0,1:T(2,128)S(1)}, s32[256,2]{0,1:T(2,128)}, u32[]{:S(2)}) copy-start(s32[256,2]{0,1:T(2,128)} %param.27) | copy-start | bytes 6148
  66.3 60.2 %collective-permute-start.6 = (bf16[2048,256]{1,0:T(8,128)(2,1)S(1)}, bf16[2048,256]{1,0:T(8,128)(2,1)}, u32[]{:S(2)}, u32[]{:S(2)}) collective-permute-start(bf16[2048,256]{1,0:T(8,128)(2,1)S(1)} %bitcast.30), channel_id=1, source_target_pairs={{0,2},{2,0},{4,6},{6,4},{8,10},{10,8},{12,14},{14,12},{1,3},{3,1},... | collective-permute-start | bytes 3145736 | tf_op jit(solution)/shard_map/ppermute | solution.py:359
  68.3 80.6 %collective-permute-start.7 = (bf16[2048,256]{1,0:T(8,128)(2,1)S(1)}, bf16[2048,256]{1,0:T(8,128)(2,1)}, u32[]{:S(2)}, u32[]{:S(2)}) collective-permute-start(bf16[2048,256]{1,0:T(8,128)(2,1)S(1)} %bitcast.33), channel_id=1, source_target_pairs={{0,2},{2,0},{4,6},{6,4},{8,10},{10,8},{12,14},{14,12},{1,3},{3,1},... | collective-permute-start | bytes 3145736 | tf_op jit(solution)/shard_map/ppermute | solution.py:359
  71.6 80.8 %collective-permute-start.10 = (bf16[256,2048]{1,0:T(8,128)(2,1)}, bf16[256,2048]{1,0:T(8,128)(2,1)}, u32[]{:S(2)}, u32[]{:S(2)}) collective-permute-start(bf16[256,2048]{1,0:T(8,128)(2,1)} %bitcast.36), channel_id=1, source_target_pairs={{0,1},{1,0},{2,3},{3,2},{4,5},{5,4},{6,7},{7,6},{8,9},{9,8},{10,11... | collective-permute-start | bytes 3145736 | tf_op jit(solution)/shard_map/ppermute | solution.py:355
  74.8 7.0 %copy-start.3 = (bf16[256,128]{1,0:T(8,128)(2,1)S(1)}, bf16[256,128]{1,0:T(8,128)(2,1)}, u32[]{:S(2)}) copy-start(bf16[256,128]{1,0:T(8,128)(2,1)} %residual_ref.1) | copy-start | bytes 196612
  82.0 16.7 %copy-start.2 = (bf16[160,192]{1,0:T(8,128)(2,1)S(1)}, bf16[160,192]{1,0:T(8,128)(2,1)}, u32[]{:S(2)}) copy-start(bf16[160,192]{1,0:T(8,128)(2,1)} %constant.28.clone.drop_ref) | copy-start | bytes 184324
  99.8 63.1 %all-to-all-start.4 = ((bf16[16,160,128]{2,1,0:T(8,128)(2,1)}), bf16[16,160,128]{2,1,0:T(8,128)(2,1)S(1)}, u32[]{:S(2)}, u32[]{:S(2)}) async-start(bf16[16,160,128]{2,1,0:T(8,128)(2,1)} %shard_map.177), calls=%async_computation.4 | async-start | bytes 1310720 | tf_op jit(solution)/shard_map/all_to_all | solution.py:347
  103.8 50.5 %collective-permute-start.4 = (bf16[2048,256]{1,0:T(8,128)(2,1)S(1)}, bf16[2048,256]{1,0:T(8,128)(2,1)S(1)}, u32[]{:S(2)}, u32[]{:S(2)}) collective-permute-start(bf16[2048,256]{1,0:T(8,128)(2,1)S(1)} %bitcast.31), channel_id=1, source_target_pairs={{0,1},{1,0},{2,3},{3,2},{4,5},{5,4},{6,7},{7,6},{8,9},{9,8},{10,11... | collective-permute-start | bytes 3145736 | tf_op jit(solution)/shard_map/ppermute | solution.py:355
  105.9 48.5 %collective-permute-start.5 = (bf16[2048,256]{1,0:T(8,128)(2,1)S(1)}, bf16[2048,256]{1,0:T(8,128)(2,1)S(1)}, u32[]{:S(2)}, u32[]{:S(2)}) collective-permute-start(bf16[2048,256]{1,0:T(8,128)(2,1)S(1)} %bitcast.34), channel_id=1, source_target_pairs={{0,1},{1,0},{2,3},{3,2},{4,5},{5,4},{6,7},{7,6},{8,9},{9,8},{10,11... | collective-permute-start | bytes 3145736 | tf_op jit(solution)/shard_map/ppermute | solution.py:355
  126.5 27.9 %collective-permute-start.12 = (bf16[256,2048]{1,0:T(8,128)(2,1)}, bf16[256,2048]{1,0:T(8,128)(2,1)S(1)}, u32[]{:S(2)}, u32[]{:S(2)}) collective-permute-start(bf16[256,2048]{1,0:T(8,128)(2,1)} %collective-permute-done.11.refs_10_), channel_id=1, source_target_pairs={{0,1},{1,0},{2,3},{3,2},{4,5},{5,4},{6,7},{7,6},{8,9},{9,8},{10,11... | collective-permute-start | bytes 3145736 | tf_op jit(solution)/shard_map/ppermute | solution.py:355
  148.9 5.9 %collective-permute-start.8 = (bf16[2048,256]{1,0:T(8,128)(2,1)}, bf16[2048,256]{1,0:T(8,128)(2,1)S(1)}, u32[]{:S(2)}, u32[]{:S(2)}) collective-permute-start(bf16[2048,256]{1,0:T(8,128)(2,1)} %collective-permute-done.6.refs_4_), channel_id=1, source_target_pairs={{0,1},{1,0},{2,3},{3,2},{4,5},{5,4},{6,7},{7,6},{8,9},{9,8},{10,11... | collective-permute-start | bytes 3145736 | tf_op jit(solution)/shard_map/ppermute | solution.py:355
  152.4 4.9 %collective-permute-start.9 = (bf16[2048,256]{1,0:T(8,128)(2,1)}, bf16[2048,256]{1,0:T(8,128)(2,1)}, u32[]{:S(2)}, u32[]{:S(2)}) collective-permute-start(bf16[2048,256]{1,0:T(8,128)(2,1)} %collective-permute-done.7.refs_5_), channel_id=1, source_target_pairs={{0,1},{1,0},{2,3},{3,2},{4,5},{5,4},{6,7},{7,6},{8,9},{9,8},{10,11... | collective-permute-start | bytes 3145736 | tf_op jit(solution)/shard_map/ppermute | solution.py:355
  154.3 1.0 copy-start.9
  154.3 1.4 copy-start.10
  154.4 1.7 copy-start.11
  156.1 1.0 copy-start.12
  169.1 23.2 %copy-start.1 = (bf16[192,160]{1,0:T(8,128)(2,1)S(1)}, bf16[192,160]{1,0:T(8,128)(2,1)}, u32[]{:S(2)}) copy-start(bf16[192,160]{1,0:T(8,128)(2,1)} %constant.29.clone.widen_ref) | copy-start | bytes 184324
  193.2 5.7 %copy-start.5 = (f32[256,2]{0,1:T(2,128)S(1)}, f32[256,2]{0,1:T(2,128)}, u32[]{:S(2)}) copy-start(f32[256,2]{0,1:T(2,128)} %param.28) | copy-start | bytes 6148
  193.2 16.4 %all-to-all-start.6 = ((bf16[32,24,128]{2,1,0:T(8,128)(2,1)}), bf16[32,24,128]{2,1,0:T(8,128)(2,1)S(1)}, u32[]{:S(2)}, u32[]{:S(2)}) async-start(bf16[32,24,128]{2,1,0:T(8,128)(2,1)} %bitcast.15), calls=%async_computation.6 | async-start | bytes 393216 | tf_op jit(solution)/shard_map/all_to_all | solution.py:347

commit v5 on v4

--- a/solution.py
+++ b/solution.py
@@ -29,6 +29,7 @@
 BLOCKS = N_SP // GROUPS
 NOTE = 16
 MASK_BIG = 16384.0
+WINDOWS = (5, 6, N_Z)
 
 F32 = jnp.float32
 BF16 = jnp.bfloat16
@@ -126,7 +127,7 @@
 
 
 def attend_body(spot, *refs):
-    q_refs, (kv_ref, out_ref, q_ref, kp_ref, vp_ref) = refs[:N_X], refs[N_X:]
+    q_refs, (kv_ref, out_ref, q_ref, kp_ref, vp_ref, plan_ref) = refs[:N_X], refs[N_X:]
     for i in range(N_X):
         q_ref[i] = q_refs[i][...]
     lane = iota((TOK, LANES), 1)
@@ -144,21 +145,41 @@
         kvf = kv.astype(F32)
         kp_ref[j * TOK : (j + 1) * TOK, :] = jnp.where(low, kvf, mark).astype(BF16)
         vp_ref[j * TOK : (j + 1) * TOK, :] = jnp.where(low, 1.0, kvf).astype(BF16)
+
+    def documents(note):
+        n0, n1 = note[0:1, :].astype(F32), note[1:2, :].astype(F32)
+        one = jnp.ones((1, LANES), F32)
+        least = jnp.where(n0 <= 0.0, one, 0.0) + jnp.where(n1 <= 0.0, one, 0.0)
+        most = jnp.where(n0 < TOK, one, 0.0) + jnp.where(n1 < TOK, one, 0.0)
+        return least, most
+
+    ranges = [documents(kv_ref[j, TOK:, :]) for j in range(N_Z)]
+    for b in range(N_X):
+        least, most = documents(q_ref[b, TOK:, :])
+        first = jnp.full((1, LANES), float(N_Z), F32)
+        last = jnp.full((1, LANES), -1.0, F32)
+        for j, (low_doc, high_doc) in enumerate(ranges):
+            meet = (low_doc <= most) & (least <= high_doc)
+            first = jnp.where(meet, jnp.minimum(first, float(j)), first)
+            last = jnp.where(meet, float(j), last)
+        code = jnp.where(last < 0.0, 0.0, first * 16.0 + (last - first + 1.0))
+        plan_ref[b] = jnp.max(code).astype(jnp.int32)
     eye = (iota((HALF, LANES), 0) == iota((HALF, LANES), 1)).astype(BF16)
     lane_h = iota((HALF, LANES), 1)
 
-    def block(b, carry):
+    def block(b, start, size):
         qf = q_ref[b, :TOK, :].astype(F32) * (HD**-0.5)
         doc = doc_of(q_ref[b, TOK:, :])
         other = jnp.where((doc == lane) | (lane > HD + 2), 0.0, -MASK_BIG)
+        keys = pl.ds(start * TOK, size * TOK)
         heads = []
         for h in range(2):
             qh = qf if h == 0 else pltpu.roll(qf, HD, 1)
             qp = jnp.where(low, qh, other).astype(BF16)
-            s = dot(qp, kp_ref[...], 1, 1)
+            s = dot(qp, kp_ref[keys, :], 1, 1)
             peak = jnp.max(s, axis=1, keepdims=True)
             p = jnp.exp(s - peak).astype(BF16)
-            acc = dot(p, vp_ref[...])
+            acc = dot(p, vp_ref[keys, :])
             total = acc[:, 0:1]
             o = acc / total
             heads.append((pltpu.roll(o, HD, 1) if h == 0 else o, peak + jnp.log(total)))
@@ -173,9 +194,22 @@
             to = lax.rem(spot[0] + N_X - b, N_X) * 2 + half
             out_ref[to, :HALF, :] = o[rows]
             out_ref[to, HALF:, :] = stat_t[:NOTE].astype(BF16)
+
+    def step(b, carry):
+        code = plan_ref[b]
+        first, count = code // 16, code % 16
+        fewer = -1
+        for size in WINDOWS:
+
+            @pl.when((count > fewer) & (count <= size))
+            def _(size=size):
+                start = 0 if size == N_Z else jnp.minimum(first, N_Z - size)
+                block(b, start, size)
+
+            fewer = size
         return carry
 
-    lax.fori_loop(0, N_X, block, 0)
+    lax.fori_loop(0, N_X, step, 0)
 
 
 def project_body(core, in_ref, w_own_ref, w_other_ref, gain_ref, out_ref):
@@ -266,8 +300,8 @@
             out_ref[g] = kept
 
 
-def expert_body(in_ref, gain_ref, *refs):
-    many = 3 * GROUPS
+def expert_body(in_ref, gain_ref, late_ref, *refs):
+    many = 3 * GROUPS - 1
     far, (out_ref, x_ref), weights, sems = refs[:many], refs[many : many + 2], refs[many + 2 : -1], refs[-1]
     copies = [pltpu.make_async_copy(far[i], weights[i], sems.at[i]) for i in range(many)]
     for copy in copies:
@@ -290,7 +324,7 @@
         hidden.append(unit.astype(BF16))
     for copy in copies[2 * GROUPS :]:
         copy.wait()
-    downs = weights[2 * GROUPS :]
+    downs = weights[2 * GROUPS :] + (late_ref,)
     for g in range(0, N_TP, 2):
         cols = slice(g * LANES, (g + 2) * LANES)
         part = dot(hidden[0], downs[0][:, cols])
@@ -459,6 +493,7 @@
             pltpu.VMEM((N_X, TOK + NOTE, LANES), BF16),
             pltpu.VMEM((N_Z * TOK, LANES), BF16),
             pltpu.VMEM((N_Z * TOK, LANES), BF16),
+            pltpu.SMEM((N_X,), jnp.int32),
         ],
         mib=24,
     )
@@ -492,12 +527,13 @@
         jnp.asarray(drop, BF16),
     )
     columns = exchange(spread, ("y", "c"))
-    weights = (gate, up, gate_o, up_o, gate_y, up_y, gate_yo, up_yo, down, down_o, down_y, down_yo)
+    weights = (gate, up, gate_o, up_o, gate_y, up_y, gate_yo, up_yo, down, down_o, down_y)
     parts = call(
         expert_body,
         shaped((N_TP, ROWS, LANES)),
         columns,
         gain_all,
+        down_yo,
         *weights,
         scratch=[pltpu.VMEM((ROWS, D), BF16)]
         + [pltpu.VMEM(w.shape, BF16) for w in weights]

time: 212 us -> 211 us (level)
  transfers between devices with their start and end apart: 18 -> 18, of which waited for: 10 -> 9; matrix products, arithmetic and copies ran while one was open for 0% -> 0% of each run, Pallas kernels for 5% -> 5%
where the time goes in v5:
time: 211 us; the launch traced here: 210 us
  starting transfers between devices  72.2 us (34%)
  waiting for transfers between devices  71.7 us (34%)
  blocking collectives  39.9 us (19%)
  Pallas kernels  22.3 us (11%)
  local copies, waits for them, and re-layouts  3.1 us (1%)
    all_to_all x2, blocking collectives, exchange(): return lax.all_to_all(x, axes, 0, 0, tiled=True)  39.9 us
    ppermute x3, waiting for transfers between devices, neighbour(): return lax.ppermute(x, 'y', [(i, i ^ 1) for i in range(N_Y)])  37.2 us
    all_to_all x5, starting transfers between devices, exchange(): return lax.all_to_all(x, axes, 0, 0, tiled=True)  33.8 us
    all_to_all x5, waiting for transfers between devices, exchange(): return lax.all_to_all(x, axes, 0, 0, tiled=True)  32.2 us
    pallas_call x12, Pallas kernels, call(): pl.pallas_call(body, out_shape=outs, in_specs=specs, out_specs=[VMEM] * l...  22.3 us
    ppermute x7, starting transfers between devices, partner(): return lax.ppermute(x, 'c', [(0, 1), (1, 0)])  19.3 us
    ppermute x3, starting transfers between devices, shifted(): return lax.ppermute(x, axis, [(i, (i + by) % size) for i in range(size)])  10.5 us
    ppermute x3, starting transfers between devices, neighbour(): return lax.ppermute(x, 'y', [(i, i ^ 1) for i in range(N_Y)])  8.54 us
  transfers between devices with their start and end apart: 18, of which 9 were waited for; matrix products, arithmetic and copies ran while one was open for 0% of the time, Pallas kernels for 5%

profile of v5, /device:TPU:1, one launch (start us, length us, event | category | flops | bytes accessed | tf_op | source)
XLA Modules:
  0.0 209.5 jit_solution(7992676680418355052)
XLA Ops:
  0.0 2.3 %shard_map.172 = (bf16[272,128]{1,0:T(8,128)(2,1)S(1)}, bf16[8,272,128]{2,1,0:T(8,128)(2,1)}) custom-call(s32[1]{0:T(128)} %bitcast.2.blk, bf16[256,128]{1,0:T(8,128)(2,1)} %refs_0_.1, bf16[64,256]{1,0:T(8,128)(2,1)} %bitcast.32, bf16[64,256]{1,0:T(8,128)(2,1)} %bitcast.33, s32[2,128]{1,0:T(2,128)} %bitcast.34, f32[1,64]{1,0:T(1,128)} %bitcast.35, ...), custom_call_target="tpu_custom_call" | custom-call | tf_op jit(solution)/shard_map/pallas_call | solution.py:370
  2.4 11.0 %all-to-all-start = ((bf16[8,272,128]{2,1,0:T(8,128)(2,1)}), bf16[8,272,128]{2,1,0:T(8,128)(2,1)S(1)}, u32[]{:S(2)}, u32[]{:S(2)}) async-start(bf16[8,272,128]{2,1,0:T(8,128)(2,1)} %get-tuple-element.11), calls=%async_computation | async-start | bytes 1114112 | tf_op jit(solution)/shard_map/all_to_all | solution.py:381
  13.4 2.9 %collective-permute-start.3 = (bf16[128,2048]{1,0:T(8,128)(2,1)S(1)}, bf16[128,2048]{1,0:T(8,128)(2,1)S(1)}, u32[]{:S(2)}, u32[]{:S(2)}) collective-permute-start(bf16[128,2048]{1,0:T(8,128)(2,1)S(1)} %copy-done), channel_id=1, source_target_pairs={{0,1},{1,0},{2,3},{3,2},{4,5},{5,4},{6,7},{7,6},{8,9},{9,8},{10,11... | collective-permute-start | bytes 1572872 | tf_op jit(solution)/shard_map/ppermute | solution.py:389
  16.2 3.1 %collective-permute-start = (bf16[272,128]{1,0:T(8,128)(2,1)S(1)}, bf16[272,128]{1,0:T(8,128)(2,1)S(1)}, u32[]{:S(2)}, u32[]{:S(2)}) collective-permute-start(bf16[272,128]{1,0:T(8,128)(2,1)S(1)} %get-tuple-element.10.refs_0_), channel_id=1, source_target_pairs={{0,16},{16,32},{32,48},{48,0},{1,17},{17,33},{33,49},{49,1},{2,18}... | collective-permute-start | bytes 208904 | tf_op jit(solution)/shard_map/ppermute | solution.py:385
  19.4 4.4 %collective-permute-start.1 = (bf16[272,128]{1,0:T(8,128)(2,1)S(1)}, bf16[272,128]{1,0:T(8,128)(2,1)S(1)}, u32[]{:S(2)}, u32[]{:S(2)}) collective-permute-start(bf16[272,128]{1,0:T(8,128)(2,1)S(1)} %get-tuple-element.10.refs_0_), channel_id=1, source_target_pairs={{0,32},{16,48},{32,0},{48,16},{1,33},{17,49},{33,1},{49,17},{2,34}... | collective-permute-start | bytes 208904 | tf_op jit(solution)/shard_map/ppermute | solution.py:385
  23.7 3.1 %collective-permute-start.2 = (bf16[272,128]{1,0:T(8,128)(2,1)S(1)}, bf16[272,128]{1,0:T(8,128)(2,1)S(1)}, u32[]{:S(2)}, u32[]{:S(2)}) collective-permute-start(bf16[272,128]{1,0:T(8,128)(2,1)S(1)} %get-tuple-element.10.refs_0_), channel_id=1, source_target_pairs={{0,48},{16,0},{32,16},{48,32},{1,49},{17,1},{33,17},{49,33},{2,50}... | collective-permute-start | bytes 208904 | tf_op jit(solution)/shard_map/ppermute | solution.py:385
  26.8 2.0 collective-permute-done.2.refs_3_
  28.8 3.2 %all-to-all-done.refs_4_ = bf16[8,272,128]{2,1,0:T(8,128)(2,1)S(1)} async-done(((bf16[8,272,128]{2,1,0:T(8,128)(2,1)}), bf16[8,272,128]{2,1,0:T(8,128)(2,1)S(1)}, u32[]{:S(2)}, u32[]{:S(2)}) %all-to-all-start) | async-done | bytes 557088 | tf_op jit(solution)/shard_map/all_to_all | solution.py:381
  32.0 7.6 %shard_map.173 = bf16[8,144,128]{2,1,0:T(8,128)(2,1)} custom-call(s32[1]{0:T(128)} %bitcast.1.spot, bf16[272,128]{1,0:T(8,128)(2,1)S(1)} %get-tuple-element.10.refs_0_, bf16[272,128]{1,0:T(8,128)(2,1)S(1)} %collective-permute-done.refs_1_, bf16[272,128]{1,0:T(8,128)(2,1)S(1)} %collective-permute-done.1.refs_2_, ...), custom_call_target="tpu_custom_call" | custom-call | tf_op jit(solution)/shard_map/pallas_call | solution.py:370
  39.6 4.8 %all-to-all-start.1 = ((bf16[8,144,128]{2,1,0:T(8,128)(2,1)}), bf16[8,144,128]{2,1,0:T(8,128)(2,1)S(1)}, u32[]{:S(2)}, u32[]{:S(2)}) async-start(bf16[8,144,128]{2,1,0:T(8,128)(2,1)} %shard_map.173), calls=%async_computation.1 | async-start | bytes 589824 | tf_op jit(solution)/shard_map/all_to_all | solution.py:381
  44.5 6.8 %all-to-all-done.1.in_ref = bf16[8,144,128]{2,1,0:T(8,128)(2,1)S(1)} async-done(((bf16[8,144,128]{2,1,0:T(8,128)(2,1)}), bf16[8,144,128]{2,1,0:T(8,128)(2,1)S(1)}, u32[]{:S(2)}, u32[]{:S(2)}) %all-to-all-start.1) | async-done | bytes 294944 | tf_op jit(solution)/shard_map/all_to_all | solution.py:381
  51.9 1.6 shard_map.174
  53.5 8.3 %all-to-all-start.2 = ((bf16[16,144,128]{2,1,0:T(8,128)(2,1)}), bf16[16,144,128]{2,1,0:T(8,128)(2,1)S(1)}, u32[]{:S(2)}, u32[]{:S(2)}) async-start(bf16[16,144,128]{2,1,0:T(8,128)(2,1)} %shard_map.174), calls=%async_computation.2 | async-start | bytes 1179648 | tf_op jit(solution)/shard_map/all_to_all | solution.py:381
  61.8 3.3 %collective-permute-start.8 = (bf16[2048,256]{1,0:T(8,128)(2,1)}, bf16[2048,256]{1,0:T(8,128)(2,1)}, u32[]{:S(2)}, u32[]{:S(2)}) collective-permute-start(bf16[2048,256]{1,0:T(8,128)(2,1)} %bitcast.13.refs_0_), channel_id=1, source_target_pairs={{0,2},{2,0},{4,6},{6,4},{8,10},{10,8},{12,14},{14,12},{1,3},{3,1},... | collective-permute-start | bytes 3145736 | tf_op jit(solution)/shard_map/ppermute | solution.py:393
  65.1 2.0 collective-permute-start.9
  67.1 3.3 %collective-permute-start.4 = (bf16[256,2048]{1,0:T(8,128)(2,1)S(1)}, bf16[256,2048]{1,0:T(8,128)(2,1)}, u32[]{:S(2)}, u32[]{:S(2)}) collective-permute-start(bf16[256,2048]{1,0:T(8,128)(2,1)S(1)} %bitcast.30), channel_id=1, source_target_pairs={{0,2},{2,0},{4,6},{6,4},{8,10},{10,8},{12,14},{14,12},{1,3},{3,1},... | collective-permute-start | bytes 3145736 | tf_op jit(solution)/shard_map/ppermute | solution.py:393
  70.4 3.1 %collective-permute-start.12 = (bf16[256,2048]{1,0:T(8,128)(2,1)S(1)}, bf16[256,2048]{1,0:T(8,128)(2,1)}, u32[]{:S(2)}, u32[]{:S(2)}) collective-permute-start(bf16[256,2048]{1,0:T(8,128)(2,1)S(1)} %bitcast.31), channel_id=1, source_target_pairs={{0,1},{1,0},{2,3},{3,2},{4,5},{5,4},{6,7},{7,6},{8,9},{9,8},{10,11... | collective-permute-start | bytes 3145736 | tf_op jit(solution)/shard_map/ppermute | solution.py:389
  73.8 6.7 %all-to-all-done.2.in_ref = bf16[16,144,128]{2,1,0:T(8,128)(2,1)S(1)} async-done(((bf16[16,144,128]{2,1,0:T(8,128)(2,1)}), bf16[16,144,128]{2,1,0:T(8,128)(2,1)S(1)}, u32[]{:S(2)}, u32[]{:S(2)}) %all-to-all-start.2) | async-done | bytes 589856 | tf_op jit(solution)/shard_map/all_to_all | solution.py:381
  80.9 16.7 %all_to_all.35 = bf16[32,24,128]{2,1,0:T(8,128)(2,1)S(1)} all-to-all(bf16[32,24,128]{2,1,0:T(8,128)(2,1)S(1)} %bitcast.20), channel_id=1, replica_groups=mesh['z'=8,'x'=4,'y'=8,'c'=2] {'z','x'}, dimensions={0} | all-to-all | bytes 393216 | tf_op jit(solution)/shard_map/all_to_all | solution.py:381
  98.7 4.0 %all-to-all-start.4 = ((bf16[16,160,128]{2,1,0:T(8,128)(2,1)}), bf16[16,160,128]{2,1,0:T(8,128)(2,1)S(1)}, u32[]{:S(2)}, u32[]{:S(2)}) async-start(bf16[16,160,128]{2,1,0:T(8,128)(2,1)} %shard_map.177), calls=%async_computation.4 | async-start | bytes 1310720 | tf_op jit(solution)/shard_map/all_to_all | solution.py:381
  102.7 2.0 collective-permute-start.6
  104.7 2.3 %collective-permute-start.7 = (bf16[2048,256]{1,0:T(8,128)(2,1)}, bf16[2048,256]{1,0:T(8,128)(2,1)S(1)}, u32[]{:S(2)}, u32[]{:S(2)}) collective-permute-start(bf16[2048,256]{1,0:T(8,128)(2,1)} %bitcast.14.refs_1_), channel_id=1, source_target_pairs={{0,1},{1,0},{2,3},{3,2},{4,5},{5,4},{6,7},{7,6},{8,9},{9,8},{10,11... | collective-permute-start | bytes 3145736 | tf_op jit(solution)/shard_map/ppermute | solution.py:389
  107.1 18.2 %collective-permute-done.9.refs_5_ = bf16[2048,256]{1,0:T(8,128)(2,1)} collective-permute-done((bf16[2048,256]{1,0:T(8,128)(2,1)}, bf16[2048,256]{1,0:T(8,128)(2,1)}, u32[]{:S(2)}, u32[]{:S(2)}) %collective-permute-start.9) | collective-permute-done | bytes 1048608 | tf_op jit(solution)/shard_map/ppermute | solution.py:393
  125.3 3.4 %collective-permute-start.10 = (bf16[2048,256]{1,0:T(8,128)(2,1)}, bf16[2048,256]{1,0:T(8,128)(2,1)S(1)}, u32[]{:S(2)}, u32[]{:S(2)}) collective-permute-start(bf16[2048,256]{1,0:T(8,128)(2,1)} %collective-permute-done.8.refs_4_), channel_id=1, source_target_pairs={{0,1},{1,0},{2,3},{3,2},{4,5},{5,4},{6,7},{7,6},{8,9},{9,8},{10,11... | collective-permute-start | bytes 3145736 | tf_op jit(solution)/shard_map/ppermute | solution.py:389
  128.7 19.0 %collective-permute-done.4.refs_10_ = bf16[256,2048]{1,0:T(8,128)(2,1)} collective-permute-done((bf16[256,2048]{1,0:T(8,128)(2,1)S(1)}, bf16[256,2048]{1,0:T(8,128)(2,1)}, u32[]{:S(2)}, u32[]{:S(2)}) %collective-permute-start.4) | collective-permute-done | bytes 1048608 | tf_op jit(solution)/shard_map/ppermute | solution.py:393
  147.7 3.4 %collective-permute-start.11 = (bf16[2048,256]{1,0:T(8,128)(2,1)}, bf16[2048,256]{1,0:T(8,128)(2,1)S(1)}, u32[]{:S(2)}, u32[]{:S(2)}) collective-permute-start(bf16[2048,256]{1,0:T(8,128)(2,1)} %collective-permute-done.9.refs_5_), channel_id=1, source_target_pairs={{0,1},{1,0},{2,3},{3,2},{4,5},{5,4},{6,7},{7,6},{8,9},{9,8},{10,11... | collective-permute-start | bytes 3145736 | tf_op jit(solution)/shard_map/ppermute | solution.py:389
  151.2 2.1 %collective-permute-start.5 = (bf16[256,2048]{1,0:T(8,128)(2,1)}, bf16[256,2048]{1,0:T(8,128)(2,1)S(1)}, u32[]{:S(2)}, u32[]{:S(2)}) collective-permute-start(bf16[256,2048]{1,0:T(8,128)(2,1)} %collective-permute-done.4.refs_10_), channel_id=1, source_target_pairs={{0,1},{1,0},{2,3},{3,2},{4,5},{5,4},{6,7},{7,6},{8,9},{9,8},{10,11... | collective-permute-start | bytes 3145736 | tf_op jit(solution)/shard_map/ppermute | solution.py:389
  156.1 5.7 %all-to-all-done.4.in_ref = bf16[16,160,128]{2,1,0:T(8,128)(2,1)S(1)} async-done(((bf16[16,160,128]{2,1,0:T(8,128)(2,1)}), bf16[16,160,128]{2,1,0:T(8,128)(2,1)S(1)}, u32[]{:S(2)}, u32[]{:S(2)}) %all-to-all-start.4) | async-done | bytes 655392 | tf_op jit(solution)/shard_map/all_to_all | solution.py:381
  161.8 6.1 %shard_map.178 = bf16[16,160,128]{2,1,0:T(8,128)(2,1)S(1)} custom-call(bf16[16,160,128]{2,1,0:T(8,128)(2,1)S(1)} %all-to-all-done.4.in_ref, f32[16,8,128]{2,1,0:T(8,128)S(1)} %get-tuple-element.13.gain_ref, bf16[256,2048]{1,0:T(8,128)(2,1)S(1)} %collective-permute-done.5.late_ref, bf16[2048,256]{1,0:T(8,128)(2,1)} %bitcast.13.refs_0_, ...), custom_call_target="tpu_custom_call" | custom-call | tf_op jit(solution)/shard_map/pallas_call | solution.py:370
  167.9 23.2 %all_to_all.36.in_ref = bf16[16,160,128]{2,1,0:T(8,128)(2,1)S(1)} all-to-all(bf16[16,160,128]{2,1,0:T(8,128)(2,1)S(1)} %shard_map.178), channel_id=1, replica_groups=mesh['z'=8,'x'=4,'y'=8,'c'=2] {'y','c'}, dimensions={0} | all-to-all | bytes 1310720 | tf_op jit(solution)/shard_map/all_to_all | solution.py:381
  192.0 5.7 %all-to-all-start.6 = ((bf16[32,24,128]{2,1,0:T(8,128)(2,1)}), bf16[32,24,128]{2,1,0:T(8,128)(2,1)S(1)}, u32[]{:S(2)}, u32[]{:S(2)}) async-start(bf16[32,24,128]{2,1,0:T(8,128)(2,1)} %bitcast.15), calls=%async_computation.6 | async-start | bytes 393216 | tf_op jit(solution)/shard_map/all_to_all | solution.py:381
  198.7 9.7 %all-to-all-done.6 = bf16[32,24,128]{2,1,0:T(8,128)(2,1)S(1)} async-done(((bf16[32,24,128]{2,1,0:T(8,128)(2,1)}), bf16[32,24,128]{2,1,0:T(8,128)(2,1)S(1)}, u32[]{:S(2)}, u32[]{:S(2)}) %all-to-all-start.6) | async-done | bytes 196640 | tf_op jit(solution)/shard_map/all_to_all | solution.py:381
  (42 shorter events, 8.1 us)
Async XLA Ops:
  2.3 11.0 %copy-start = (bf16[128,2048]{1,0:T(8,128)(2,1)S(1)}, bf16[128,2048]{1,0:T(8,128)(2,1)}, u32[]{:S(2)}) copy-start(bf16[128,2048]{1,0:T(8,128)(2,1)} %w_own_ref.1) | copy-start | bytes 1572868
  2.4 29.7 %all-to-all-start = ((bf16[8,272,128]{2,1,0:T(8,128)(2,1)}), bf16[8,272,128]{2,1,0:T(8,128)(2,1)S(1)}, u32[]{:S(2)}, u32[]{:S(2)}) async-start(bf16[8,272,128]{2,1,0:T(8,128)(2,1)} %get-tuple-element.11), calls=%async_computation | async-start | bytes 1114112 | tf_op jit(solution)/shard_map/all_to_all | solution.py:381
  13.4 31.1 %collective-permute-start.3 = (bf16[128,2048]{1,0:T(8,128)(2,1)S(1)}, bf16[128,2048]{1,0:T(8,128)(2,1)S(1)}, u32[]{:S(2)}, u32[]{:S(2)}) collective-permute-start(bf16[128,2048]{1,0:T(8,128)(2,1)S(1)} %copy-done), channel_id=1, source_target_pairs={{0,1},{1,0},{2,3},{3,2},{4,5},{5,4},{6,7},{7,6},{8,9},{9,8},{10,11... | collective-permute-start | bytes 1572872 | tf_op jit(solution)/shard_map/ppermute | solution.py:389
  16.2 10.6 %collective-permute-start = (bf16[272,128]{1,0:T(8,128)(2,1)S(1)}, bf16[272,128]{1,0:T(8,128)(2,1)S(1)}, u32[]{:S(2)}, u32[]{:S(2)}) collective-permute-start(bf16[272,128]{1,0:T(8,128)(2,1)S(1)} %get-tuple-element.10.refs_0_), channel_id=1, source_target_pairs={{0,16},{16,32},{32,48},{48,0},{1,17},{17,33},{33,49},{49,1},{2,18}... | collective-permute-start | bytes 208904 | tf_op jit(solution)/shard_map/ppermute | solution.py:385
  19.4 7.4 %collective-permute-start.1 = (bf16[272,128]{1,0:T(8,128)(2,1)S(1)}, bf16[272,128]{1,0:T(8,128)(2,1)S(1)}, u32[]{:S(2)}, u32[]{:S(2)}) collective-permute-start(bf16[272,128]{1,0:T(8,128)(2,1)S(1)} %get-tuple-element.10.refs_0_), channel_id=1, source_target_pairs={{0,32},{16,48},{32,0},{48,16},{1,33},{17,49},{33,1},{49,17},{2,34}... | collective-permute-start | bytes 208904 | tf_op jit(solution)/shard_map/ppermute | solution.py:385
  23.7 5.1 %collective-permute-start.2 = (bf16[272,128]{1,0:T(8,128)(2,1)S(1)}, bf16[272,128]{1,0:T(8,128)(2,1)S(1)}, u32[]{:S(2)}, u32[]{:S(2)}) collective-permute-start(bf16[272,128]{1,0:T(8,128)(2,1)S(1)} %get-tuple-element.10.refs_0_), channel_id=1, source_target_pairs={{0,48},{16,0},{32,16},{48,32},{1,49},{17,1},{33,17},{49,33},{2,50}... | collective-permute-start | bytes 208904 | tf_op jit(solution)/shard_map/ppermute | solution.py:385
  39.6 11.6 %all-to-all-start.1 = ((bf16[8,144,128]{2,1,0:T(8,128)(2,1)}), bf16[8,144,128]{2,1,0:T(8,128)(2,1)S(1)}, u32[]{:S(2)}, u32[]{:S(2)}) async-start(bf16[8,144,128]{2,1,0:T(8,128)(2,1)} %shard_map.173), calls=%async_computation.1 | async-start | bytes 589824 | tf_op jit(solution)/shard_map/all_to_all | solution.py:381
  51.2 0.7 copy-start.6
  53.5 13.6 %copy-start.7 = (bf16[1,256,2048]{2,1,0:T(8,128)(2,1)S(1)}, bf16[1,256,2048]{2,1,0:T(8,128)(2,1)}, u32[]{:S(2)}) copy-start(bf16[1,256,2048]{2,1,0:T(8,128)(2,1)} %param.31) | copy-start | bytes 3145732
  53.5 27.1 %all-to-all-start.2 = ((bf16[16,144,128]{2,1,0:T(8,128)(2,1)}), bf16[16,144,128]{2,1,0:T(8,128)(2,1)S(1)}, u32[]{:S(2)}, u32[]{:S(2)}) async-start(bf16[16,144,128]{2,1,0:T(8,128)(2,1)} %shard_map.174), calls=%async_computation.2 | async-start | bytes 1179648 | tf_op jit(solution)/shard_map/all_to_all | solution.py:381
  61.8 42.9 %collective-permute-start.8 = (bf16[2048,256]{1,0:T(8,128)(2,1)}, bf16[2048,256]{1,0:T(8,128)(2,1)}, u32[]{:S(2)}, u32[]{:S(2)}) collective-permute-start(bf16[2048,256]{1,0:T(8,128)(2,1)} %bitcast.13.refs_0_), channel_id=1, source_target_pairs={{0,2},{2,0},{4,6},{6,4},{8,10},{10,8},{12,14},{14,12},{1,3},{3,1},... | collective-permute-start | bytes 3145736 | tf_op jit(solution)/shard_map/ppermute | solution.py:393
  65.1 8.5 %copy-start.4 = (s32[256,2]{0,1:T(2,128)S(1)}, s32[256,2]{0,1:T(2,128)}, u32[]{:S(2)}) copy-start(s32[256,2]{0,1:T(2,128)} %param.27) | copy-start | bytes 6148
  65.1 60.2 %collective-permute-start.9 = (bf16[2048,256]{1,0:T(8,128)(2,1)}, bf16[2048,256]{1,0:T(8,128)(2,1)}, u32[]{:S(2)}, u32[]{:S(2)}) collective-permute-start(bf16[2048,256]{1,0:T(8,128)(2,1)} %bitcast.14.refs_1_), channel_id=1, source_target_pairs={{0,2},{2,0},{4,6},{6,4},{8,10},{10,8},{12,14},{14,12},{1,3},{3,1},... | collective-permute-start | bytes 3145736 | tf_op jit(solution)/shard_map/ppermute | solution.py:393
  67.1 80.6 %collective-permute-start.4 = (bf16[256,2048]{1,0:T(8,128)(2,1)S(1)}, bf16[256,2048]{1,0:T(8,128)(2,1)}, u32[]{:S(2)}, u32[]{:S(2)}) collective-permute-start(bf16[256,2048]{1,0:T(8,128)(2,1)S(1)} %bitcast.30), channel_id=1, source_target_pairs={{0,2},{2,0},{4,6},{6,4},{8,10},{10,8},{12,14},{14,12},{1,3},{3,1},... | collective-permute-start | bytes 3145736 | tf_op jit(solution)/shard_map/ppermute | solution.py:393
  70.4 80.8 %collective-permute-start.12 = (bf16[256,2048]{1,0:T(8,128)(2,1)S(1)}, bf16[256,2048]{1,0:T(8,128)(2,1)}, u32[]{:S(2)}, u32[]{:S(2)}) collective-permute-start(bf16[256,2048]{1,0:T(8,128)(2,1)S(1)} %bitcast.31), channel_id=1, source_target_pairs={{0,1},{1,0},{2,3},{3,2},{4,5},{5,4},{6,7},{7,6},{8,9},{9,8},{10,11... | collective-permute-start | bytes 3145736 | tf_op jit(solution)/shard_map/ppermute | solution.py:389
  73.6 7.0 %copy-start.3 = (bf16[256,128]{1,0:T(8,128)(2,1)S(1)}, bf16[256,128]{1,0:T(8,128)(2,1)}, u32[]{:S(2)}) copy-start(bf16[256,128]{1,0:T(8,128)(2,1)} %residual_ref.1) | copy-start | bytes 196612
  80.9 16.7 %copy-start.2 = (bf16[160,192]{1,0:T(8,128)(2,1)S(1)}, bf16[160,192]{1,0:T(8,128)(2,1)}, u32[]{:S(2)}) copy-start(bf16[160,192]{1,0:T(8,128)(2,1)} %constant.28.clone.drop_ref) | copy-start | bytes 184324
  98.7 63.1 %all-to-all-start.4 = ((bf16[16,160,128]{2,1,0:T(8,128)(2,1)}), bf16[16,160,128]{2,1,0:T(8,128)(2,1)S(1)}, u32[]{:S(2)}, u32[]{:S(2)}) async-start(bf16[16,160,128]{2,1,0:T(8,128)(2,1)} %shard_map.177), calls=%async_computation.4 | async-start | bytes 1310720 | tf_op jit(solution)/shard_map/all_to_all | solution.py:381
  102.7 50.6 %collective-permute-start.6 = (bf16[2048,256]{1,0:T(8,128)(2,1)}, bf16[2048,256]{1,0:T(8,128)(2,1)S(1)}, u32[]{:S(2)}, u32[]{:S(2)}) collective-permute-start(bf16[2048,256]{1,0:T(8,128)(2,1)} %bitcast.13.refs_0_), channel_id=1, source_target_pairs={{0,1},{1,0},{2,3},{3,2},{4,5},{5,4},{6,7},{7,6},{8,9},{9,8},{10,11... | collective-permute-start | bytes 3145736 | tf_op jit(solution)/shard_map/ppermute | solution.py:389
  104.7 48.6 %collective-permute-start.7 = (bf16[2048,256]{1,0:T(8,128)(2,1)}, bf16[2048,256]{1,0:T(8,128)(2,1)S(1)}, u32[]{:S(2)}, u32[]{:S(2)}) collective-permute-start(bf16[2048,256]{1,0:T(8,128)(2,1)} %bitcast.14.refs_1_), channel_id=1, source_target_pairs={{0,1},{1,0},{2,3},{3,2},{4,5},{5,4},{6,7},{7,6},{8,9},{9,8},{10,11... | collective-permute-start | bytes 3145736 | tf_op jit(solution)/shard_map/ppermute | solution.py:389
  125.3 28.1 %collective-permute-start.10 = (bf16[2048,256]{1,0:T(8,128)(2,1)}, bf16[2048,256]{1,0:T(8,128)(2,1)S(1)}, u32[]{:S(2)}, u32[]{:S(2)}) collective-permute-start(bf16[2048,256]{1,0:T(8,128)(2,1)} %collective-permute-done.8.refs_4_), channel_id=1, source_target_pairs={{0,1},{1,0},{2,3},{3,2},{4,5},{5,4},{6,7},{7,6},{8,9},{9,8},{10,11... | collective-permute-start | bytes 3145736 | tf_op jit(solution)/shard_map/ppermute | solution.py:389
  147.7 5.9 %collective-permute-start.11 = (bf16[2048,256]{1,0:T(8,128)(2,1)}, bf16[2048,256]{1,0:T(8,128)(2,1)S(1)}, u32[]{:S(2)}, u32[]{:S(2)}) collective-permute-start(bf16[2048,256]{1,0:T(8,128)(2,1)} %collective-permute-done.9.refs_5_), channel_id=1, source_target_pairs={{0,1},{1,0},{2,3},{3,2},{4,5},{5,4},{6,7},{7,6},{8,9},{9,8},{10,11... | collective-permute-start | bytes 3145736 | tf_op jit(solution)/shard_map/ppermute | solution.py:389
  151.2 4.9 %collective-permute-start.5 = (bf16[256,2048]{1,0:T(8,128)(2,1)}, bf16[256,2048]{1,0:T(8,128)(2,1)S(1)}, u32[]{:S(2)}, u32[]{:S(2)}) collective-permute-start(bf16[256,2048]{1,0:T(8,128)(2,1)} %collective-permute-done.4.refs_10_), channel_id=1, source_target_pairs={{0,1},{1,0},{2,3},{3,2},{4,5},{5,4},{6,7},{7,6},{8,9},{9,8},{10,11... | collective-permute-start | bytes 3145736 | tf_op jit(solution)/shard_map/ppermute | solution.py:389
  153.3 1.0 copy-start.8
  153.3 1.4 copy-start.9
  153.4 1.6 copy-start.10
  155.0 1.1 copy-start.11
  167.9 23.2 %copy-start.1 = (bf16[192,160]{1,0:T(8,128)(2,1)S(1)}, bf16[192,160]{1,0:T(8,128)(2,1)}, u32[]{:S(2)}) copy-start(bf16[192,160]{1,0:T(8,128)(2,1)} %constant.29.clone.widen_ref) | copy-start | bytes 184324
  192.0 5.7 %copy-start.5 = (f32[256,2]{0,1:T(2,128)S(1)}, f32[256,2]{0,1:T(2,128)}, u32[]{:S(2)}) copy-start(f32[256,2]{0,1:T(2,128)} %param.28) | copy-start | bytes 6148
  192.0 16.4 %all-to-all-start.6 = ((bf16[32,24,128]{2,1,0:T(8,128)(2,1)}), bf16[32,24,128]{2,1,0:T(8,128)(2,1)S(1)}, u32[]{:S(2)}, u32[]{:S(2)}) async-start(bf16[32,24,128]{2,1,0:T(8,128)(2,1)} %bitcast.15), calls=%async_computation.6 | async-start | bytes 393216 | tf_op jit(solution)/shard_map/all_to_all | solution.py:381

commit v6 on v5

--- a/solution.py
+++ b/solution.py
@@ -102,11 +102,13 @@
     gain = jnp.concatenate([qg_ref[...], qg_ref[...]], axis=1)
     q_out = turn(x * jnp.where(low, r0, r1) * gain).astype(BF16)
 
-    kv = jnp.concatenate([k_ref[...], v_ref[...]], axis=0).astype(F32).T
-    sk = jnp.sum(jnp.where(low, kv * kv, 0.0), axis=1, keepdims=True)
-    rk = lax.rsqrt(sk * (1.0 / HD) + EPSILON)
+    flat = k_ref[...].astype(F32)
+    k = jnp.concatenate([flat, jnp.zeros_like(flat)], axis=0).T
+    rk = lax.rsqrt(jnp.sum(k * k, axis=1, keepdims=True) * (1.0 / HD) + EPSILON)
     gain_k = jnp.concatenate([kg_ref[...], kg_ref[...]], axis=1)
-    kv_out = jnp.where(low, turn(kv * rk * gain_k), kv).astype(BF16)
+    k = turn(k * rk * gain_k)
+    keys = jnp.where(low[:HALF], k[:HALF], pltpu.roll(k[HALF:], HD, 1)).astype(BF16)
+    values = v_ref[...]
 
     docs = docs_ref[...]
     n0 = jnp.sum((docs < 1).astype(F32))
@@ -116,7 +118,9 @@
     qs_ref[:TOK, :] = q_out
     qs_ref[TOK:, :] = note
     for i in range(N_Z):
-        kvs_ref[i, :TOK, :] = kv_out
+        kvs_ref[i, :HALF, :] = keys
+        kvs_ref[i, HALF : HALF + HD, :] = values[:, :HALF]
+        kvs_ref[i, HALF + HD : TOK, :] = values[:, HALF:]
         kvs_ref[i, TOK:, :] = note
 
 
@@ -127,7 +131,7 @@
 
 
 def attend_body(spot, *refs):
-    q_refs, (kv_ref, out_ref, q_ref, kp_ref, vp_ref, plan_ref) = refs[:N_X], refs[N_X:]
+    q_refs, (kv_ref, out_ref, q_ref, kp_ref, vt_ref, score_ref, plan_ref) = refs[:N_X], refs[N_X:]
     for i in range(N_X):
         q_ref[i] = q_refs[i][...]
     lane = iota((TOK, LANES), 1)
@@ -140,11 +144,13 @@
         return jnp.where(idx < n0, HD, jnp.where(idx < n1, HD + 1, HD + 2))
 
     for j in range(N_Z):
-        kv = kv_ref[j, :TOK, :]
         mark = (doc_of(kv_ref[j, TOK:, :]) == lane).astype(F32)
-        kvf = kv.astype(F32)
-        kp_ref[j * TOK : (j + 1) * TOK, :] = jnp.where(low, kvf, mark).astype(BF16)
-        vp_ref[j * TOK : (j + 1) * TOK, :] = jnp.where(low, 1.0, kvf).astype(BF16)
+        pair = kv_ref[j, :HALF, :].astype(F32)
+        kf = jnp.concatenate([pair, pltpu.roll(pair, HD, 1)], axis=0)
+        kp_ref[j * TOK : (j + 1) * TOK, :] = jnp.where(low, kf, mark).astype(BF16)
+        vt_ref[j, :HD, :HALF] = kv_ref[j, HALF : HALF + HD, :]
+        vt_ref[j, :HD, HALF:] = kv_ref[j, HALF + HD : TOK, :]
+        vt_ref[j, HD:, :] = jnp.ones((NOTE, TOK), BF16)
 
     def documents(note):
         n0, n1 = note[0:1, :].astype(F32), note[1:2, :].astype(F32)
@@ -164,36 +170,49 @@
             last = jnp.where(meet, float(j), last)
         code = jnp.where(last < 0.0, 0.0, first * 16.0 + (last - first + 1.0))
         plan_ref[b] = jnp.max(code).astype(jnp.int32)
-    eye = (iota((HALF, LANES), 0) == iota((HALF, LANES), 1)).astype(BF16)
-    lane_h = iota((HALF, LANES), 1)
+    note_row = iota((NOTE, HALF), 0)
 
     def block(b, start, size):
         qf = q_ref[b, :TOK, :].astype(F32) * (HD**-0.5)
         doc = doc_of(q_ref[b, TOK:, :])
         other = jnp.where((doc == lane) | (lane > HD + 2), 0.0, -MASK_BIG)
-        keys = pl.ds(start * TOK, size * TOK)
-        heads = []
-        for h in range(2):
-            qh = qf if h == 0 else pltpu.roll(qf, HD, 1)
-            qp = jnp.where(low, qh, other).astype(BF16)
-            s = dot(qp, kp_ref[keys, :], 1, 1)
-            peak = jnp.max(s, axis=1, keepdims=True)
-            p = jnp.exp(s - peak).astype(BF16)
-            acc = dot(p, vp_ref[keys, :])
-            total = acc[:, 0:1]
-            o = acc / total
-            heads.append((pltpu.roll(o, HD, 1) if h == 0 else o, peak + jnp.log(total)))
-        o = jnp.where(low, heads[0][0], heads[1][0]).astype(BF16)
-        parts = split3(heads[0][1]) + split3(heads[1][1])
+        heads = [jnp.where(low, qh, other).astype(BF16) for qh in (qf, pltpu.roll(qf, HD, 1))]
+        peaks = [jnp.full((8, TOK), -jnp.inf, F32) for _ in heads]
+        accs = [jnp.zeros((HD + NOTE, TOK), F32) for _ in heads]
+        tops = [None, None]
+
+        def score(h, j):
+            at = pl.multiple_of((start + j) * TOK, TOK)
+            part = dot(kp_ref[pl.ds(at, TOK), :], heads[h], 1, 1)
+            score_ref[h, j] = part
+            peaks[h] = jnp.maximum(peaks[h], jnp.max(part.reshape(TOK // 8, 8, TOK), axis=0))
+
+        def weigh(h, j):
+            p = jnp.exp(score_ref[h, j] - tops[h]).astype(BF16)
+            accs[h] = accs[h] + dot(vt_ref[start + j], p)
+
+        for j in range(size):
+            score(0, j)
+        tops[0] = jnp.max(peaks[0], axis=0, keepdims=True)
+        for j in range(size):
+            score(1, j)
+            weigh(0, j)
+        tops[1] = jnp.max(peaks[1], axis=0, keepdims=True)
+        for j in range(size):
+            weigh(1, j)
+        peak = jnp.concatenate(tops, axis=1)
+        total = jnp.concatenate([acc[HD : HD + 1, :] for acc in accs], axis=1)
+        o = [acc[:HD, :] / acc[HD : HD + 1, :] for acc in accs]
+        o = jnp.concatenate(o, axis=0).T.astype(BF16)
+        terms = split3(peak + jnp.log(total))
         for half in range(2):
-            rows = slice(half * HALF, (half + 1) * HALF)
-            stat = jnp.zeros((HALF, LANES), F32)
-            for i, part in enumerate(parts):
-                stat = jnp.where(lane_h == i, part[rows], stat)
-            stat_t = dot(stat.astype(BF16), eye, 0, 0)
+            stat = jnp.zeros((NOTE, HALF), F32)
+            for i in range(6):
+                at = (i // 3) * TOK + half * HALF
+                stat = jnp.where(note_row == i, terms[i % 3][:, at : at + HALF], stat)
             to = lax.rem(spot[0] + N_X - b, N_X) * 2 + half
-            out_ref[to, :HALF, :] = o[rows]
-            out_ref[to, HALF:, :] = stat_t[:NOTE].astype(BF16)
+            out_ref[to, :HALF, :] = o[half * HALF : (half + 1) * HALF]
+            out_ref[to, HALF:, :] = stat.astype(BF16)
 
     def step(b, carry):
         code = plan_ref[b]
@@ -492,7 +511,8 @@
         scratch=[
             pltpu.VMEM((N_X, TOK + NOTE, LANES), BF16),
             pltpu.VMEM((N_Z * TOK, LANES), BF16),
-            pltpu.VMEM((N_Z * TOK, LANES), BF16),
+            pltpu.VMEM((N_Z, HD + NOTE, TOK), BF16),
+            pltpu.VMEM((2, N_Z, TOK, TOK), F32),
             pltpu.SMEM((N_X,), jnp.int32),
         ],
         mib=24,

time: 211 us -> 209 us (level)
  transfers between devices with their start and end apart: 18 -> 18, of which waited for: 9 -> 10; matrix products, arithmetic and copies ran while one was open for 0% -> 0% of each run, Pallas kernels for 5% -> 4%
where the time goes in v6:
time: 209 us; the launch traced here: 208 us
  waiting for transfers between devices  72.1 us (34%)
  starting transfers between devices  72 us (34%)
  blocking collectives  39.9 us (19%)
  Pallas kernels  20.6 us (10%)
  local copies, waits for them, and re-layouts  2.92 us (1%)
    all_to_all x2, blocking collectives, exchange(): return lax.all_to_all(x, axes, 0, 0, tiled=True)  39.9 us
    ppermute x3, waiting for transfers between devices, neighbour(): return lax.ppermute(x, 'y', [(i, i ^ 1) for i in range(N_Y)])  37.2 us
    all_to_all x5, starting transfers between devices, exchange(): return lax.all_to_all(x, axes, 0, 0, tiled=True)  33.8 us
    all_to_all x5, waiting for transfers between devices, exchange(): return lax.all_to_all(x, axes, 0, 0, tiled=True)  32.3 us
    pallas_call x12, Pallas kernels, call(): pl.pallas_call(body, out_shape=outs, in_specs=specs, out_specs=[VMEM] * l...  20.6 us
    ppermute x7, starting transfers between devices, partner(): return lax.ppermute(x, 'c', [(0, 1), (1, 0)])  19.1 us
    ppermute x3, starting transfers between devices, shifted(): return lax.ppermute(x, axis, [(i, (i + by) % size) for i in range(size)])  10.5 us
    ppermute x3, starting transfers between devices, neighbour(): return lax.ppermute(x, 'y', [(i, i ^ 1) for i in range(N_Y)])  8.54 us
  transfers between devices with their start and end apart: 18, of which 10 were waited for; matrix products, arithmetic and copies ran while one was open for 0% of the time, Pallas kernels for 4%

profile of v6, /device:TPU:1, one launch (start us, length us, event | category | flops | bytes accessed | tf_op | source)
XLA Modules:
  0.0 207.8 jit_solution(16643923340697504291)
XLA Ops:
  0.0 2.4 %shard_map.172 = (bf16[272,128]{1,0:T(8,128)(2,1)S(1)}, bf16[8,272,128]{2,1,0:T(8,128)(2,1)}) custom-call(s32[1]{0:T(128)} %bitcast.2.blk, bf16[256,128]{1,0:T(8,128)(2,1)} %refs_0_.1, bf16[64,256]{1,0:T(8,128)(2,1)} %bitcast.32, bf16[64,256]{1,0:T(8,128)(2,1)} %bitcast.33, s32[2,128]{1,0:T(2,128)} %bitcast.34, f32[1,64]{1,0:T(1,128)} %bitcast.35, ...), custom_call_target="tpu_custom_call" | custom-call | tf_op jit(solution)/shard_map/pallas_call | solution.py:389
  2.5 11.0 %all-to-all-start = ((bf16[8,272,128]{2,1,0:T(8,128)(2,1)}), bf16[8,272,128]{2,1,0:T(8,128)(2,1)S(1)}, u32[]{:S(2)}, u32[]{:S(2)}) async-start(bf16[8,272,128]{2,1,0:T(8,128)(2,1)} %get-tuple-element.11), calls=%async_computation | async-start | bytes 1114112 | tf_op jit(solution)/shard_map/all_to_all | solution.py:400
  13.5 2.9 %collective-permute-start.3 = (bf16[128,2048]{1,0:T(8,128)(2,1)S(1)}, bf16[128,2048]{1,0:T(8,128)(2,1)S(1)}, u32[]{:S(2)}, u32[]{:S(2)}) collective-permute-start(bf16[128,2048]{1,0:T(8,128)(2,1)S(1)} %copy-done), channel_id=1, source_target_pairs={{0,1},{1,0},{2,3},{3,2},{4,5},{5,4},{6,7},{7,6},{8,9},{9,8},{10,11... | collective-permute-start | bytes 1572872 | tf_op jit(solution)/shard_map/ppermute | solution.py:408
  16.3 3.1 %collective-permute-start = (bf16[272,128]{1,0:T(8,128)(2,1)S(1)}, bf16[272,128]{1,0:T(8,128)(2,1)S(1)}, u32[]{:S(2)}, u32[]{:S(2)}) collective-permute-start(bf16[272,128]{1,0:T(8,128)(2,1)S(1)} %get-tuple-element.10.refs_0_), channel_id=1, source_target_pairs={{0,16},{16,32},{32,48},{48,0},{1,17},{17,33},{33,49},{49,1},{2,18}... | collective-permute-start | bytes 208904 | tf_op jit(solution)/shard_map/ppermute | solution.py:404
  19.5 4.4 %collective-permute-start.1 = (bf16[272,128]{1,0:T(8,128)(2,1)S(1)}, bf16[272,128]{1,0:T(8,128)(2,1)S(1)}, u32[]{:S(2)}, u32[]{:S(2)}) collective-permute-start(bf16[272,128]{1,0:T(8,128)(2,1)S(1)} %get-tuple-element.10.refs_0_), channel_id=1, source_target_pairs={{0,32},{16,48},{32,0},{48,16},{1,33},{17,49},{33,1},{49,17},{2,34}... | collective-permute-start | bytes 208904 | tf_op jit(solution)/shard_map/ppermute | solution.py:404
  23.8 3.1 %collective-permute-start.2 = (bf16[272,128]{1,0:T(8,128)(2,1)S(1)}, bf16[272,128]{1,0:T(8,128)(2,1)S(1)}, u32[]{:S(2)}, u32[]{:S(2)}) collective-permute-start(bf16[272,128]{1,0:T(8,128)(2,1)S(1)} %get-tuple-element.10.refs_0_), channel_id=1, source_target_pairs={{0,48},{16,0},{32,16},{48,32},{1,49},{17,1},{33,17},{49,33},{2,50}... | collective-permute-start | bytes 208904 | tf_op jit(solution)/shard_map/ppermute | solution.py:404
  26.9 2.0 collective-permute-done.2.refs_3_
  28.9 3.2 %all-to-all-done.refs_4_ = bf16[8,272,128]{2,1,0:T(8,128)(2,1)S(1)} async-done(((bf16[8,272,128]{2,1,0:T(8,128)(2,1)}), bf16[8,272,128]{2,1,0:T(8,128)(2,1)S(1)}, u32[]{:S(2)}, u32[]{:S(2)}) %all-to-all-start) | async-done | bytes 557088 | tf_op jit(solution)/shard_map/all_to_all | solution.py:400
  32.1 5.9 %shard_map.173 = bf16[8,144,128]{2,1,0:T(8,128)(2,1)} custom-call(s32[1]{0:T(128)} %bitcast.1.spot, bf16[272,128]{1,0:T(8,128)(2,1)S(1)} %get-tuple-element.10.refs_0_, bf16[272,128]{1,0:T(8,128)(2,1)S(1)} %collective-permute-done.refs_1_, bf16[272,128]{1,0:T(8,128)(2,1)S(1)} %collective-permute-done.1.refs_2_, ...), custom_call_target="tpu_custom_call" | custom-call | tf_op jit(solution)/shard_map/pallas_call | solution.py:389
  38.0 4.8 %all-to-all-start.1 = ((bf16[8,144,128]{2,1,0:T(8,128)(2,1)}), bf16[8,144,128]{2,1,0:T(8,128)(2,1)S(1)}, u32[]{:S(2)}, u32[]{:S(2)}) async-start(bf16[8,144,128]{2,1,0:T(8,128)(2,1)} %shard_map.173), calls=%async_computation.1 | async-start | bytes 589824 | tf_op jit(solution)/shard_map/all_to_all | solution.py:400
  42.8 6.8 %all-to-all-done.1.in_ref = bf16[8,144,128]{2,1,0:T(8,128)(2,1)S(1)} async-done(((bf16[8,144,128]{2,1,0:T(8,128)(2,1)}), bf16[8,144,128]{2,1,0:T(8,128)(2,1)S(1)}, u32[]{:S(2)}, u32[]{:S(2)}) %all-to-all-start.1) | async-done | bytes 294944 | tf_op jit(solution)/shard_map/all_to_all | solution.py:400
  50.2 1.6 shard_map.174
  51.8 8.3 %all-to-all-start.2 = ((bf16[16,144,128]{2,1,0:T(8,128)(2,1)}), bf16[16,144,128]{2,1,0:T(8,128)(2,1)S(1)}, u32[]{:S(2)}, u32[]{:S(2)}) async-start(bf16[16,144,128]{2,1,0:T(8,128)(2,1)} %shard_map.174), calls=%async_computation.2 | async-start | bytes 1179648 | tf_op jit(solution)/shard_map/all_to_all | solution.py:400
  60.1 3.3 %collective-permute-start.8 = (bf16[2048,256]{1,0:T(8,128)(2,1)}, bf16[2048,256]{1,0:T(8,128)(2,1)}, u32[]{:S(2)}, u32[]{:S(2)}) collective-permute-start(bf16[2048,256]{1,0:T(8,128)(2,1)} %bitcast.13.refs_0_), channel_id=1, source_target_pairs={{0,2},{2,0},{4,6},{6,4},{8,10},{10,8},{12,14},{14,12},{1,3},{3,1},... | collective-permute-start | bytes 3145736 | tf_op jit(solution)/shard_map/ppermute | solution.py:412
  63.4 2.0 collective-permute-start.9
  65.4 3.3 %collective-permute-start.4 = (bf16[256,2048]{1,0:T(8,128)(2,1)S(1)}, bf16[256,2048]{1,0:T(8,128)(2,1)}, u32[]{:S(2)}, u32[]{:S(2)}) collective-permute-start(bf16[256,2048]{1,0:T(8,128)(2,1)S(1)} %bitcast.30), channel_id=1, source_target_pairs={{0,2},{2,0},{4,6},{6,4},{8,10},{10,8},{12,14},{14,12},{1,3},{3,1},... | collective-permute-start | bytes 3145736 | tf_op jit(solution)/shard_map/ppermute | solution.py:412
  68.7 3.1 %collective-permute-start.12 = (bf16[256,2048]{1,0:T(8,128)(2,1)S(1)}, bf16[256,2048]{1,0:T(8,128)(2,1)}, u32[]{:S(2)}, u32[]{:S(2)}) collective-permute-start(bf16[256,2048]{1,0:T(8,128)(2,1)S(1)} %bitcast.31), channel_id=1, source_target_pairs={{0,1},{1,0},{2,3},{3,2},{4,5},{5,4},{6,7},{7,6},{8,9},{9,8},{10,11... | collective-permute-start | bytes 3145736 | tf_op jit(solution)/shard_map/ppermute | solution.py:408
  72.1 6.7 %all-to-all-done.2.in_ref = bf16[16,144,128]{2,1,0:T(8,128)(2,1)S(1)} async-done(((bf16[16,144,128]{2,1,0:T(8,128)(2,1)}), bf16[16,144,128]{2,1,0:T(8,128)(2,1)S(1)}, u32[]{:S(2)}, u32[]{:S(2)}) %all-to-all-start.2) | async-done | bytes 589856 | tf_op jit(solution)/shard_map/all_to_all | solution.py:400
  79.2 16.7 %all_to_all.35 = bf16[32,24,128]{2,1,0:T(8,128)(2,1)S(1)} all-to-all(bf16[32,24,128]{2,1,0:T(8,128)(2,1)S(1)} %bitcast.20), channel_id=1, replica_groups=mesh['z'=8,'x'=4,'y'=8,'c'=2] {'z','x'}, dimensions={0} | all-to-all | bytes 393216 | tf_op jit(solution)/shard_map/all_to_all | solution.py:400
  97.0 4.0 %all-to-all-start.4 = ((bf16[16,160,128]{2,1,0:T(8,128)(2,1)}), bf16[16,160,128]{2,1,0:T(8,128)(2,1)S(1)}, u32[]{:S(2)}, u32[]{:S(2)}) async-start(bf16[16,160,128]{2,1,0:T(8,128)(2,1)} %shard_map.177), calls=%async_computation.4 | async-start | bytes 1310720 | tf_op jit(solution)/shard_map/all_to_all | solution.py:400
  101.0 2.0 collective-permute-start.6
  103.0 2.3 %collective-permute-start.7 = (bf16[2048,256]{1,0:T(8,128)(2,1)}, bf16[2048,256]{1,0:T(8,128)(2,1)S(1)}, u32[]{:S(2)}, u32[]{:S(2)}) collective-permute-start(bf16[2048,256]{1,0:T(8,128)(2,1)} %bitcast.14.refs_1_), channel_id=1, source_target_pairs={{0,1},{1,0},{2,3},{3,2},{4,5},{5,4},{6,7},{7,6},{8,9},{9,8},{10,11... | collective-permute-start | bytes 3145736 | tf_op jit(solution)/shard_map/ppermute | solution.py:408
  105.3 18.2 %collective-permute-done.9.refs_5_ = bf16[2048,256]{1,0:T(8,128)(2,1)} collective-permute-done((bf16[2048,256]{1,0:T(8,128)(2,1)}, bf16[2048,256]{1,0:T(8,128)(2,1)}, u32[]{:S(2)}, u32[]{:S(2)}) %collective-permute-start.9) | collective-permute-done | bytes 1048608 | tf_op jit(solution)/shard_map/ppermute | solution.py:412
  123.6 3.4 %collective-permute-start.10 = (bf16[2048,256]{1,0:T(8,128)(2,1)}, bf16[2048,256]{1,0:T(8,128)(2,1)S(1)}, u32[]{:S(2)}, u32[]{:S(2)}) collective-permute-start(bf16[2048,256]{1,0:T(8,128)(2,1)} %collective-permute-done.8.refs_4_), channel_id=1, source_target_pairs={{0,1},{1,0},{2,3},{3,2},{4,5},{5,4},{6,7},{7,6},{8,9},{9,8},{10,11... | collective-permute-start | bytes 3145736 | tf_op jit(solution)/shard_map/ppermute | solution.py:408
  127.0 19.0 %collective-permute-done.4.refs_10_ = bf16[256,2048]{1,0:T(8,128)(2,1)} collective-permute-done((bf16[256,2048]{1,0:T(8,128)(2,1)S(1)}, bf16[256,2048]{1,0:T(8,128)(2,1)}, u32[]{:S(2)}, u32[]{:S(2)}) %collective-permute-start.4) | collective-permute-done | bytes 1048608 | tf_op jit(solution)/shard_map/ppermute | solution.py:412
  146.0 3.4 %collective-permute-start.11 = (bf16[2048,256]{1,0:T(8,128)(2,1)}, bf16[2048,256]{1,0:T(8,128)(2,1)S(1)}, u32[]{:S(2)}, u32[]{:S(2)}) collective-permute-start(bf16[2048,256]{1,0:T(8,128)(2,1)} %collective-permute-done.9.refs_5_), channel_id=1, source_target_pairs={{0,1},{1,0},{2,3},{3,2},{4,5},{5,4},{6,7},{7,6},{8,9},{9,8},{10,11... | collective-permute-start | bytes 3145736 | tf_op jit(solution)/shard_map/ppermute | solution.py:408
  149.5 1.9 collective-permute-start.5
  154.3 5.8 %all-to-all-done.4.in_ref = bf16[16,160,128]{2,1,0:T(8,128)(2,1)S(1)} async-done(((bf16[16,160,128]{2,1,0:T(8,128)(2,1)}), bf16[16,160,128]{2,1,0:T(8,128)(2,1)S(1)}, u32[]{:S(2)}, u32[]{:S(2)}) %all-to-all-start.4) | async-done | bytes 655392 | tf_op jit(solution)/shard_map/all_to_all | solution.py:400
  160.1 6.1 %shard_map.178 = bf16[16,160,128]{2,1,0:T(8,128)(2,1)S(1)} custom-call(bf16[16,160,128]{2,1,0:T(8,128)(2,1)S(1)} %all-to-all-done.4.in_ref, f32[16,8,128]{2,1,0:T(8,128)S(1)} %get-tuple-element.13.gain_ref, bf16[256,2048]{1,0:T(8,128)(2,1)S(1)} %collective-permute-done.5.late_ref, bf16[2048,256]{1,0:T(8,128)(2,1)} %bitcast.13.refs_0_, ...), custom_call_target="tpu_custom_call" | custom-call | tf_op jit(solution)/shard_map/pallas_call | solution.py:389
  166.2 23.2 %all_to_all.36.in_ref = bf16[16,160,128]{2,1,0:T(8,128)(2,1)S(1)} all-to-all(bf16[16,160,128]{2,1,0:T(8,128)(2,1)S(1)} %shard_map.178), channel_id=1, replica_groups=mesh['z'=8,'x'=4,'y'=8,'c'=2] {'y','c'}, dimensions={0} | all-to-all | bytes 1310720 | tf_op jit(solution)/shard_map/all_to_all | solution.py:400
  190.3 5.7 %all-to-all-start.6 = ((bf16[32,24,128]{2,1,0:T(8,128)(2,1)}), bf16[32,24,128]{2,1,0:T(8,128)(2,1)S(1)}, u32[]{:S(2)}, u32[]{:S(2)}) async-start(bf16[32,24,128]{2,1,0:T(8,128)(2,1)} %bitcast.15), calls=%async_computation.6 | async-start | bytes 393216 | tf_op jit(solution)/shard_map/all_to_all | solution.py:400
  197.0 9.7 %all-to-all-done.6 = bf16[32,24,128]{2,1,0:T(8,128)(2,1)S(1)} async-done(((bf16[32,24,128]{2,1,0:T(8,128)(2,1)}), bf16[32,24,128]{2,1,0:T(8,128)(2,1)S(1)}, u32[]{:S(2)}, u32[]{:S(2)}) %all-to-all-start.6) | async-done | bytes 196640 | tf_op jit(solution)/shard_map/all_to_all | solution.py:400
  (42 shorter events, 8.2 us)
Async XLA Ops:
  2.4 11.0 %copy-start = (bf16[128,2048]{1,0:T(8,128)(2,1)S(1)}, bf16[128,2048]{1,0:T(8,128)(2,1)}, u32[]{:S(2)}) copy-start(bf16[128,2048]{1,0:T(8,128)(2,1)} %w_own_ref.1) | copy-start | bytes 1572868
  2.5 29.7 %all-to-all-start = ((bf16[8,272,128]{2,1,0:T(8,128)(2,1)}), bf16[8,272,128]{2,1,0:T(8,128)(2,1)S(1)}, u32[]{:S(2)}, u32[]{:S(2)}) async-start(bf16[8,272,128]{2,1,0:T(8,128)(2,1)} %get-tuple-element.11), calls=%async_computation | async-start | bytes 1114112 | tf_op jit(solution)/shard_map/all_to_all | solution.py:400
  13.5 29.3 %collective-permute-start.3 = (bf16[128,2048]{1,0:T(8,128)(2,1)S(1)}, bf16[128,2048]{1,0:T(8,128)(2,1)S(1)}, u32[]{:S(2)}, u32[]{:S(2)}) collective-permute-start(bf16[128,2048]{1,0:T(8,128)(2,1)S(1)} %copy-done), channel_id=1, source_target_pairs={{0,1},{1,0},{2,3},{3,2},{4,5},{5,4},{6,7},{7,6},{8,9},{9,8},{10,11... | collective-permute-start | bytes 1572872 | tf_op jit(solution)/shard_map/ppermute | solution.py:408
  16.3 10.6 %collective-permute-start = (bf16[272,128]{1,0:T(8,128)(2,1)S(1)}, bf16[272,128]{1,0:T(8,128)(2,1)S(1)}, u32[]{:S(2)}, u32[]{:S(2)}) collective-permute-start(bf16[272,128]{1,0:T(8,128)(2,1)S(1)} %get-tuple-element.10.refs_0_), channel_id=1, source_target_pairs={{0,16},{16,32},{32,48},{48,0},{1,17},{17,33},{33,49},{49,1},{2,18}... | collective-permute-start | bytes 208904 | tf_op jit(solution)/shard_map/ppermute | solution.py:404
  19.5 7.4 %collective-permute-start.1 = (bf16[272,128]{1,0:T(8,128)(2,1)S(1)}, bf16[272,128]{1,0:T(8,128)(2,1)S(1)}, u32[]{:S(2)}, u32[]{:S(2)}) collective-permute-start(bf16[272,128]{1,0:T(8,128)(2,1)S(1)} %get-tuple-element.10.refs_0_), channel_id=1, source_target_pairs={{0,32},{16,48},{32,0},{48,16},{1,33},{17,49},{33,1},{49,17},{2,34}... | collective-permute-start | bytes 208904 | tf_op jit(solution)/shard_map/ppermute | solution.py:404
  23.8 5.1 %collective-permute-start.2 = (bf16[272,128]{1,0:T(8,128)(2,1)S(1)}, bf16[272,128]{1,0:T(8,128)(2,1)S(1)}, u32[]{:S(2)}, u32[]{:S(2)}) collective-permute-start(bf16[272,128]{1,0:T(8,128)(2,1)S(1)} %get-tuple-element.10.refs_0_), channel_id=1, source_target_pairs={{0,48},{16,0},{32,16},{48,32},{1,49},{17,1},{33,17},{49,33},{2,50}... | collective-permute-start | bytes 208904 | tf_op jit(solution)/shard_map/ppermute | solution.py:404
  38.0 11.6 %all-to-all-start.1 = ((bf16[8,144,128]{2,1,0:T(8,128)(2,1)}), bf16[8,144,128]{2,1,0:T(8,128)(2,1)S(1)}, u32[]{:S(2)}, u32[]{:S(2)}) async-start(bf16[8,144,128]{2,1,0:T(8,128)(2,1)} %shard_map.173), calls=%async_computation.1 | async-start | bytes 589824 | tf_op jit(solution)/shard_map/all_to_all | solution.py:400
  49.5 0.7 copy-start.6
  51.8 13.6 %copy-start.7 = (bf16[1,256,2048]{2,1,0:T(8,128)(2,1)S(1)}, bf16[1,256,2048]{2,1,0:T(8,128)(2,1)}, u32[]{:S(2)}) copy-start(bf16[1,256,2048]{2,1,0:T(8,128)(2,1)} %param.31) | copy-start | bytes 3145732
  51.8 27.1 %all-to-all-start.2 = ((bf16[16,144,128]{2,1,0:T(8,128)(2,1)}), bf16[16,144,128]{2,1,0:T(8,128)(2,1)S(1)}, u32[]{:S(2)}, u32[]{:S(2)}) async-start(bf16[16,144,128]{2,1,0:T(8,128)(2,1)} %shard_map.174), calls=%async_computation.2 | async-start | bytes 1179648 | tf_op jit(solution)/shard_map/all_to_all | solution.py:400
  60.1 42.9 %collective-permute-start.8 = (bf16[2048,256]{1,0:T(8,128)(2,1)}, bf16[2048,256]{1,0:T(8,128)(2,1)}, u32[]{:S(2)}, u32[]{:S(2)}) collective-permute-start(bf16[2048,256]{1,0:T(8,128)(2,1)} %bitcast.13.refs_0_), channel_id=1, source_target_pairs={{0,2},{2,0},{4,6},{6,4},{8,10},{10,8},{12,14},{14,12},{1,3},{3,1},... | collective-permute-start | bytes 3145736 | tf_op jit(solution)/shard_map/ppermute | solution.py:412
  63.4 8.5 %copy-start.4 = (s32[256,2]{0,1:T(2,128)S(1)}, s32[256,2]{0,1:T(2,128)}, u32[]{:S(2)}) copy-start(s32[256,2]{0,1:T(2,128)} %param.27) | copy-start | bytes 6148
  63.4 60.2 %collective-permute-start.9 = (bf16[2048,256]{1,0:T(8,128)(2,1)}, bf16[2048,256]{1,0:T(8,128)(2,1)}, u32[]{:S(2)}, u32[]{:S(2)}) collective-permute-start(bf16[2048,256]{1,0:T(8,128)(2,1)} %bitcast.14.refs_1_), channel_id=1, source_target_pairs={{0,2},{2,0},{4,6},{6,4},{8,10},{10,8},{12,14},{14,12},{1,3},{3,1},... | collective-permute-start | bytes 3145736 | tf_op jit(solution)/shard_map/ppermute | solution.py:412
  65.4 80.6 %collective-permute-start.4 = (bf16[256,2048]{1,0:T(8,128)(2,1)S(1)}, bf16[256,2048]{1,0:T(8,128)(2,1)}, u32[]{:S(2)}, u32[]{:S(2)}) collective-permute-start(bf16[256,2048]{1,0:T(8,128)(2,1)S(1)} %bitcast.30), channel_id=1, source_target_pairs={{0,2},{2,0},{4,6},{6,4},{8,10},{10,8},{12,14},{14,12},{1,3},{3,1},... | collective-permute-start | bytes 3145736 | tf_op jit(solution)/shard_map/ppermute | solution.py:412
  68.7 80.8 %collective-permute-start.12 = (bf16[256,2048]{1,0:T(8,128)(2,1)S(1)}, bf16[256,2048]{1,0:T(8,128)(2,1)}, u32[]{:S(2)}, u32[]{:S(2)}) collective-permute-start(bf16[256,2048]{1,0:T(8,128)(2,1)S(1)} %bitcast.31), channel_id=1, source_target_pairs={{0,1},{1,0},{2,3},{3,2},{4,5},{5,4},{6,7},{7,6},{8,9},{9,8},{10,11... | collective-permute-start | bytes 3145736 | tf_op jit(solution)/shard_map/ppermute | solution.py:408
  71.8 7.0 %copy-start.3 = (bf16[256,128]{1,0:T(8,128)(2,1)S(1)}, bf16[256,128]{1,0:T(8,128)(2,1)}, u32[]{:S(2)}) copy-start(bf16[256,128]{1,0:T(8,128)(2,1)} %residual_ref.1) | copy-start | bytes 196612
  79.2 16.7 %copy-start.2 = (bf16[160,192]{1,0:T(8,128)(2,1)S(1)}, bf16[160,192]{1,0:T(8,128)(2,1)}, u32[]{:S(2)}) copy-start(bf16[160,192]{1,0:T(8,128)(2,1)} %constant.28.clone.drop_ref) | copy-start | bytes 184324
  97.0 63.1 %all-to-all-start.4 = ((bf16[16,160,128]{2,1,0:T(8,128)(2,1)}), bf16[16,160,128]{2,1,0:T(8,128)(2,1)S(1)}, u32[]{:S(2)}, u32[]{:S(2)}) async-start(bf16[16,160,128]{2,1,0:T(8,128)(2,1)} %shard_map.177), calls=%async_computation.4 | async-start | bytes 1310720 | tf_op jit(solution)/shard_map/all_to_all | solution.py:400
  101.0 50.4 %collective-permute-start.6 = (bf16[2048,256]{1,0:T(8,128)(2,1)}, bf16[2048,256]{1,0:T(8,128)(2,1)S(1)}, u32[]{:S(2)}, u32[]{:S(2)}) collective-permute-start(bf16[2048,256]{1,0:T(8,128)(2,1)} %bitcast.13.refs_0_), channel_id=1, source_target_pairs={{0,1},{1,0},{2,3},{3,2},{4,5},{5,4},{6,7},{7,6},{8,9},{9,8},{10,11... | collective-permute-start | bytes 3145736 | tf_op jit(solution)/shard_map/ppermute | solution.py:408
  103.0 48.4 %collective-permute-start.7 = (bf16[2048,256]{1,0:T(8,128)(2,1)}, bf16[2048,256]{1,0:T(8,128)(2,1)S(1)}, u32[]{:S(2)}, u32[]{:S(2)}) collective-permute-start(bf16[2048,256]{1,0:T(8,128)(2,1)} %bitcast.14.refs_1_), channel_id=1, source_target_pairs={{0,1},{1,0},{2,3},{3,2},{4,5},{5,4},{6,7},{7,6},{8,9},{9,8},{10,11... | collective-permute-start | bytes 3145736 | tf_op jit(solution)/shard_map/ppermute | solution.py:408
  123.6 27.9 %collective-permute-start.10 = (bf16[2048,256]{1,0:T(8,128)(2,1)}, bf16[2048,256]{1,0:T(8,128)(2,1)S(1)}, u32[]{:S(2)}, u32[]{:S(2)}) collective-permute-start(bf16[2048,256]{1,0:T(8,128)(2,1)} %collective-permute-done.8.refs_4_), channel_id=1, source_target_pairs={{0,1},{1,0},{2,3},{3,2},{4,5},{5,4},{6,7},{7,6},{8,9},{9,8},{10,11... | collective-permute-start | bytes 3145736 | tf_op jit(solution)/shard_map/ppermute | solution.py:408
  146.0 5.9 %collective-permute-start.11 = (bf16[2048,256]{1,0:T(8,128)(2,1)}, bf16[2048,256]{1,0:T(8,128)(2,1)S(1)}, u32[]{:S(2)}, u32[]{:S(2)}) collective-permute-start(bf16[2048,256]{1,0:T(8,128)(2,1)} %collective-permute-done.9.refs_5_), channel_id=1, source_target_pairs={{0,1},{1,0},{2,3},{3,2},{4,5},{5,4},{6,7},{7,6},{8,9},{9,8},{10,11... | collective-permute-start | bytes 3145736 | tf_op jit(solution)/shard_map/ppermute | solution.py:408
  149.5 4.8 %collective-permute-start.5 = (bf16[256,2048]{1,0:T(8,128)(2,1)}, bf16[256,2048]{1,0:T(8,128)(2,1)S(1)}, u32[]{:S(2)}, u32[]{:S(2)}) collective-permute-start(bf16[256,2048]{1,0:T(8,128)(2,1)} %collective-permute-done.4.refs_10_), channel_id=1, source_target_pairs={{0,1},{1,0},{2,3},{3,2},{4,5},{5,4},{6,7},{7,6},{8,9},{9,8},{10,11... | collective-permute-start | bytes 3145736 | tf_op jit(solution)/shard_map/ppermute | solution.py:408
  151.4 1.0 copy-start.8
  151.5 1.4 copy-start.9
  151.5 1.6 copy-start.10
  153.1 1.1 copy-start.11
  166.2 23.2 %copy-start.1 = (bf16[192,160]{1,0:T(8,128)(2,1)S(1)}, bf16[192,160]{1,0:T(8,128)(2,1)}, u32[]{:S(2)}) copy-start(bf16[192,160]{1,0:T(8,128)(2,1)} %constant.29.clone.widen_ref) | copy-start | bytes 184324
  190.3 5.7 %copy-start.5 = (f32[256,2]{0,1:T(2,128)S(1)}, f32[256,2]{0,1:T(2,128)}, u32[]{:S(2)}) copy-start(f32[256,2]{0,1:T(2,128)} %param.28) | copy-start | bytes 6148
  190.3 16.4 %all-to-all-start.6 = ((bf16[32,24,128]{2,1,0:T(8,128)(2,1)}), bf16[32,24,128]{2,1,0:T(8,128)(2,1)S(1)}, u32[]{:S(2)}, u32[]{:S(2)}) async-start(bf16[32,24,128]{2,1,0:T(8,128)(2,1)} %bitcast.15), calls=%async_computation.6 | async-start | bytes 393216 | tf_op jit(solution)/shard_map/all_to_all | solution.py:400

commit v7 on v6

--- a/solution.py
+++ b/solution.py
@@ -71,7 +71,7 @@
 
 
 def prep_body(blk, *refs):
-    sources, (qs_ref, kvs_ref), kept, sems = refs[:8], refs[8:10], refs[10:18], refs[18]
+    sources, (qs_ref, kvs_ref, gain_ref), kept, sems = refs[:9], refs[9:12], refs[12:21], refs[21]
     copies = []
     for i, (src, dst) in enumerate(zip(sources, kept)):
         src = src.at[blk[0]] if i == 6 else src
@@ -80,7 +80,8 @@
         copy.start()
     for copy in copies:
         copy.wait()
-    q_ref, k_ref, v_ref, docs_ref, qg_ref, kg_ref, row_ref, col_ref = kept
+    q_ref, k_ref, v_ref, docs_ref, qg_ref, kg_ref, row_ref, col_ref, norm_ref = kept
+    gain_ref[...] = norm_ref[...]
     lane = iota((TOK, LANES), 1)
     low = lane < HD
     even = (lane & 1) == 0
@@ -323,7 +324,7 @@
     many = 3 * GROUPS - 1
     far, (out_ref, x_ref), weights, sems = refs[:many], refs[many : many + 2], refs[many + 2 : -1], refs[-1]
     copies = [pltpu.make_async_copy(far[i], weights[i], sems.at[i]) for i in range(many)]
-    for copy in copies:
+    for copy in copies[:4]:
         copy.start()
     total = jnp.zeros((ROWS, LANES), F32)
     for g in range(N_TP):
@@ -336,8 +337,10 @@
     hidden = []
     for i in range(GROUPS):
         copies[2 * i].wait()
+        copies[2 * i + 1].wait()
+        for copy in copies[2 * i + 4 : 2 * i + 6]:
+            copy.start()
         gate = jnp.minimum(dot(x_ref[...], weights[2 * i][...]), CLAMP_LIMIT)
-        copies[2 * i + 1].wait()
         up = jnp.clip(dot(x_ref[...], weights[2 * i + 1][...]), -CLAMP_LIMIT, CLAMP_LIMIT)
         unit = gate * (1.0 / (1.0 + jnp.exp(-SIGMOID_SCALE * gate))) * (up + 1.0)
         hidden.append(unit.astype(BF16))
@@ -409,7 +412,11 @@
 
 
 def neighbour(x):
-    return lax.ppermute(x, "y", [(i, i ^ 1) for i in range(N_Y)])
+    pairs = []
+    for y in range(N_Y):
+        for c, to in ((0, y ^ 1), (1, (((y + 1) ^ 1) - 1) % N_Y)):
+            pairs.append((y * N_C + c, to * N_C + c))
+    return lax.ppermute(x, ("y", "c"), pairs)
 
 
 def per_device(
@@ -476,11 +483,16 @@
         key_gain,
         jnp.asarray(row_tab),
         jnp.asarray(col_tab),
+        norm_gain.reshape(1, LANES),
     )
     kept = [pltpu.VMEM(a.shape[1:] if i == 6 else a.shape, a.dtype) for i, a in enumerate(sources)]
-    qs, kvs = call(
+    qs, kvs, gain_own = call(
         prep_body,
-        [shaped((TOK + NOTE, LANES)), shaped((N_Z, TOK + NOTE, LANES))],
+        [
+            shaped((TOK + NOTE, LANES)),
+            shaped((N_Z, TOK + NOTE, LANES)),
+            shaped((1, LANES), F32),
+        ],
         block,
         *sources,
         scratch=kept + [pltpu.SemaphoreType.DMA((len(sources),))],
@@ -525,7 +537,7 @@
         partial,
         out_weight,
         out_other,
-        norm_gain.reshape(1, LANES),
+        gain_own,
     )
     projected = exchange(projected, ("y", "c"))
     mixed, gain_all, outgoing = call(

time: 209 us -> 175 us (0.84)
  waiting for transfers between devices: 72.1 us -> 38.8 us
    ppermute x3, waiting for transfers between devices: 37.2 us -> 10.1 us  [neighbour(): return lax.ppermute(x, ('y', 'c'), pairs)]
    all_to_all x5, waiting for transfers between devices: 32.3 us -> 26.3 us  [exchange(): return lax.all_to_all(x, axes, 0, 0, tiled=True)]
    ppermute x7, starting transfers between devices: 19.1 us -> 15.4 us  [partner(): return lax.ppermute(x, 'c', [(0, 1), (1, 0)])]
    ppermute x3, starting transfers between devices: 8.54 us -> 11 us  [neighbour(): return lax.ppermute(x, ('y', 'c'), pairs)]
  transfers between devices with their start and end apart: 18 -> 18, of which waited for: 10 -> 8; matrix products, arithmetic and copies ran while one was open for 0% -> 0% of each run, Pallas kernels for 4% -> 5%
where the time goes in v7:
time: 175 us; the launch traced here: 174 us
  starting transfers between devices  70.4 us (40%)
  blocking collectives  41.3 us (24%)
  waiting for transfers between devices  38.8 us (22%)
  Pallas kernels  20.7 us (12%)
  local copies, waits for them, and re-layouts  2.38 us (1%)
    all_to_all x2, blocking collectives, exchange(): return lax.all_to_all(x, axes, 0, 0, tiled=True)  41.3 us
    all_to_all x5, starting transfers between devices, exchange(): return lax.all_to_all(x, axes, 0, 0, tiled=True)  33.5 us
    all_to_all x5, waiting for transfers between devices, exchange(): return lax.all_to_all(x, axes, 0, 0, tiled=True)  26.3 us
    pallas_call x12, Pallas kernels, call(): pl.pallas_call(body, out_shape=outs, in_specs=specs, out_specs=[VMEM] * l...  20.7 us
    ppermute x7, starting transfers between devices, partner(): return lax.ppermute(x, 'c', [(0, 1), (1, 0)])  15.4 us
    ppermute x3, starting transfers between devices, neighbour(): return lax.ppermute(x, ('y', 'c'), pairs)  11 us
    ppermute x3, starting transfers between devices, shifted(): return lax.ppermute(x, axis, [(i, (i + by) % size) for i in range(size)])  10.5 us
    ppermute x3, waiting for transfers between devices, neighbour(): return lax.ppermute(x, ('y', 'c'), pairs)  10.1 us
  transfers between devices with their start and end apart: 18, of which 8 were waited for; matrix products, arithmetic and copies ran while one was open for 0% of the time, Pallas kernels for 5%

profile of v7, /device:TPU:1, one launch (start us, length us, event | category | flops | bytes accessed | tf_op | source)
XLA Modules:
  0.0 174.0 jit_solution(2466641262213392923)
XLA Ops:
  0.0 2.4 %shard_map.172 = (bf16[272,128]{1,0:T(8,128)(2,1)S(1)}, bf16[8,272,128]{2,1,0:T(8,128)(2,1)}, f32[1,128]{1,0:T(1,128)S(1)}) custom-call(s32[1]{0:T(128)} %bitcast.2.blk, bf16[256,128]{1,0:T(8,128)(2,1)} %refs_0_.1, bf16[64,256]{1,0:T(8,128)(2,1)} %bitcast.31, bf16[64,256]{1,0:T(8,128)(2,1)} %bitcast.32, s32[2,128]{1,0:T(2,128)} %bitcast.33, ...), custom_call_target="tpu_custom_call" | custom-call | tf_op jit(solution)/shard_map/pallas_call | solution.py:392
  2.5 11.0 %all-to-all-start = ((bf16[8,272,128]{2,1,0:T(8,128)(2,1)}), bf16[8,272,128]{2,1,0:T(8,128)(2,1)S(1)}, u32[]{:S(2)}, u32[]{:S(2)}) async-start(bf16[8,272,128]{2,1,0:T(8,128)(2,1)} %get-tuple-element.12), calls=%async_computation | async-start | bytes 1114112 | tf_op jit(solution)/shard_map/all_to_all | solution.py:403
  13.5 2.9 %collective-permute-start.3 = (bf16[128,2048]{1,0:T(8,128)(2,1)S(1)}, bf16[128,2048]{1,0:T(8,128)(2,1)S(1)}, u32[]{:S(2)}, u32[]{:S(2)}) collective-permute-start(bf16[128,2048]{1,0:T(8,128)(2,1)S(1)} %copy-done), channel_id=1, source_target_pairs={{0,1},{1,0},{2,3},{3,2},{4,5},{5,4},{6,7},{7,6},{8,9},{9,8},{10,11... | collective-permute-start | bytes 1572872 | tf_op jit(solution)/shard_map/ppermute | solution.py:411
  16.3 3.1 %collective-permute-start = (bf16[272,128]{1,0:T(8,128)(2,1)S(1)}, bf16[272,128]{1,0:T(8,128)(2,1)S(1)}, u32[]{:S(2)}, u32[]{:S(2)}) collective-permute-start(bf16[272,128]{1,0:T(8,128)(2,1)S(1)} %get-tuple-element.11.refs_0_), channel_id=1, source_target_pairs={{0,16},{16,32},{32,48},{48,0},{1,17},{17,33},{33,49},{49,1},{2,18}... | collective-permute-start | bytes 208904 | tf_op jit(solution)/shard_map/ppermute | solution.py:407
  19.5 4.4 %collective-permute-start.1 = (bf16[272,128]{1,0:T(8,128)(2,1)S(1)}, bf16[272,128]{1,0:T(8,128)(2,1)S(1)}, u32[]{:S(2)}, u32[]{:S(2)}) collective-permute-start(bf16[272,128]{1,0:T(8,128)(2,1)S(1)} %get-tuple-element.11.refs_0_), channel_id=1, source_target_pairs={{0,32},{16,48},{32,0},{48,16},{1,33},{17,49},{33,1},{49,17},{2,34}... | collective-permute-start | bytes 208904 | tf_op jit(solution)/shard_map/ppermute | solution.py:407
  23.8 3.1 %collective-permute-start.2 = (bf16[272,128]{1,0:T(8,128)(2,1)S(1)}, bf16[272,128]{1,0:T(8,128)(2,1)S(1)}, u32[]{:S(2)}, u32[]{:S(2)}) collective-permute-start(bf16[272,128]{1,0:T(8,128)(2,1)S(1)} %get-tuple-element.11.refs_0_), channel_id=1, source_target_pairs={{0,48},{16,0},{32,16},{48,32},{1,49},{17,1},{33,17},{49,33},{2,50}... | collective-permute-start | bytes 208904 | tf_op jit(solution)/shard_map/ppermute | solution.py:407
  26.9 2.0 %collective-permute-done.2.refs_3_ = bf16[272,128]{1,0:T(8,128)(2,1)S(1)} collective-permute-done((bf16[272,128]{1,0:T(8,128)(2,1)S(1)}, bf16[272,128]{1,0:T(8,128)(2,1)S(1)}, u32[]{:S(2)}, u32[]{:S(2)}) %collective-permute-start.2) | collective-permute-done | bytes 69664 | tf_op jit(solution)/shard_map/ppermute | solution.py:407
  28.9 3.2 %all-to-all-done.refs_4_ = bf16[8,272,128]{2,1,0:T(8,128)(2,1)S(1)} async-done(((bf16[8,272,128]{2,1,0:T(8,128)(2,1)}), bf16[8,272,128]{2,1,0:T(8,128)(2,1)S(1)}, u32[]{:S(2)}, u32[]{:S(2)}) %all-to-all-start) | async-done | bytes 557088 | tf_op jit(solution)/shard_map/all_to_all | solution.py:403
  32.1 5.8 %shard_map.173 = bf16[8,144,128]{2,1,0:T(8,128)(2,1)} custom-call(s32[1]{0:T(128)} %bitcast.1.spot, bf16[272,128]{1,0:T(8,128)(2,1)S(1)} %get-tuple-element.11.refs_0_, bf16[272,128]{1,0:T(8,128)(2,1)S(1)} %collective-permute-done.refs_1_, bf16[272,128]{1,0:T(8,128)(2,1)S(1)} %collective-permute-done.1.refs_2_, ...), custom_call_target="tpu_custom_call" | custom-call | tf_op jit(solution)/shard_map/pallas_call | solution.py:392
  38.0 4.8 %all-to-all-start.1 = ((bf16[8,144,128]{2,1,0:T(8,128)(2,1)}), bf16[8,144,128]{2,1,0:T(8,128)(2,1)S(1)}, u32[]{:S(2)}, u32[]{:S(2)}) async-start(bf16[8,144,128]{2,1,0:T(8,128)(2,1)} %shard_map.173), calls=%async_computation.1 | async-start | bytes 589824 | tf_op jit(solution)/shard_map/all_to_all | solution.py:403
  42.8 6.8 %all-to-all-done.1.in_ref = bf16[8,144,128]{2,1,0:T(8,128)(2,1)S(1)} async-done(((bf16[8,144,128]{2,1,0:T(8,128)(2,1)}), bf16[8,144,128]{2,1,0:T(8,128)(2,1)S(1)}, u32[]{:S(2)}, u32[]{:S(2)}) %all-to-all-start.1) | async-done | bytes 294944 | tf_op jit(solution)/shard_map/all_to_all | solution.py:403
  49.5 1.6 shard_map.174
  51.1 8.3 %all-to-all-start.2 = ((bf16[16,144,128]{2,1,0:T(8,128)(2,1)}), bf16[16,144,128]{2,1,0:T(8,128)(2,1)S(1)}, u32[]{:S(2)}, u32[]{:S(2)}) async-start(bf16[16,144,128]{2,1,0:T(8,128)(2,1)} %shard_map.174), calls=%async_computation.2 | async-start | bytes 1179648 | tf_op jit(solution)/shard_map/all_to_all | solution.py:403
  59.4 4.5 %collective-permute-start.8 = (bf16[2048,256]{1,0:T(8,128)(2,1)}, bf16[2048,256]{1,0:T(8,128)(2,1)}, u32[]{:S(2)}, u32[]{:S(2)}) collective-permute-start(bf16[2048,256]{1,0:T(8,128)(2,1)} %bitcast.13.refs_0_), channel_id=1, source_target_pairs={{0,2},{1,15},{2,0},{3,5},{4,6},{5,3},{6,4},{7,9},{8,10},{9,7},{10,... | collective-permute-start | bytes 3145736 | tf_op jit(solution)/shard_map/ppermute | solution.py:419
  63.9 2.0 %collective-permute-start.9 = (bf16[2048,256]{1,0:T(8,128)(2,1)}, bf16[2048,256]{1,0:T(8,128)(2,1)}, u32[]{:S(2)}, u32[]{:S(2)}) collective-permute-start(bf16[2048,256]{1,0:T(8,128)(2,1)} %bitcast.14.refs_1_), channel_id=1, source_target_pairs={{0,2},{1,15},{2,0},{3,5},{4,6},{5,3},{6,4},{7,9},{8,10},{9,7},{10,... | collective-permute-start | bytes 3145736 | tf_op jit(solution)/shard_map/ppermute | solution.py:419
  66.0 4.5 %collective-permute-start.4 = (bf16[256,2048]{1,0:T(8,128)(2,1)S(1)}, bf16[256,2048]{1,0:T(8,128)(2,1)}, u32[]{:S(2)}, u32[]{:S(2)}) collective-permute-start(bf16[256,2048]{1,0:T(8,128)(2,1)S(1)} %bitcast.29), channel_id=1, source_target_pairs={{0,2},{1,15},{2,0},{3,5},{4,6},{5,3},{6,4},{7,9},{8,10},{9,7},{10,... | collective-permute-start | bytes 3145736 | tf_op jit(solution)/shard_map/ppermute | solution.py:419
  70.5 1.9 %collective-permute-start.12 = (bf16[256,2048]{1,0:T(8,128)(2,1)S(1)}, bf16[256,2048]{1,0:T(8,128)(2,1)}, u32[]{:S(2)}, u32[]{:S(2)}) collective-permute-start(bf16[256,2048]{1,0:T(8,128)(2,1)S(1)} %bitcast.30), channel_id=1, source_target_pairs={{0,1},{1,0},{2,3},{3,2},{4,5},{5,4},{6,7},{7,6},{8,9},{9,8},{10,11... | collective-permute-start | bytes 3145736 | tf_op jit(solution)/shard_map/ppermute | solution.py:411
  72.6 5.3 %all-to-all-done.2.in_ref = bf16[16,144,128]{2,1,0:T(8,128)(2,1)S(1)} async-done(((bf16[16,144,128]{2,1,0:T(8,128)(2,1)}), bf16[16,144,128]{2,1,0:T(8,128)(2,1)S(1)}, u32[]{:S(2)}, u32[]{:S(2)}) %all-to-all-start.2) | async-done | bytes 589856 | tf_op jit(solution)/shard_map/all_to_all | solution.py:403
  78.3 16.9 %all_to_all.35 = bf16[32,24,128]{2,1,0:T(8,128)(2,1)S(1)} all-to-all(bf16[32,24,128]{2,1,0:T(8,128)(2,1)S(1)} %bitcast.20), channel_id=1, replica_groups=mesh['z'=8,'x'=4,'y'=8,'c'=2] {'z','x'}, dimensions={0} | all-to-all | bytes 393216 | tf_op jit(solution)/shard_map/all_to_all | solution.py:403
  95.2 1.1 shard_map.177
  96.4 3.7 %all-to-all-start.4 = ((bf16[16,160,128]{2,1,0:T(8,128)(2,1)}), bf16[16,160,128]{2,1,0:T(8,128)(2,1)S(1)}, u32[]{:S(2)}, u32[]{:S(2)}) async-start(bf16[16,160,128]{2,1,0:T(8,128)(2,1)} %shard_map.177), calls=%async_computation.4 | async-start | bytes 1310720 | tf_op jit(solution)/shard_map/all_to_all | solution.py:403
  100.1 2.0 %collective-permute-start.6 = (bf16[2048,256]{1,0:T(8,128)(2,1)}, bf16[2048,256]{1,0:T(8,128)(2,1)S(1)}, u32[]{:S(2)}, u32[]{:S(2)}) collective-permute-start(bf16[2048,256]{1,0:T(8,128)(2,1)} %bitcast.13.refs_0_), channel_id=1, source_target_pairs={{0,1},{1,0},{2,3},{3,2},{4,5},{5,4},{6,7},{7,6},{8,9},{9,8},{10,11... | collective-permute-start | bytes 3145736 | tf_op jit(solution)/shard_map/ppermute | solution.py:411
  102.2 2.3 %collective-permute-start.7 = (bf16[2048,256]{1,0:T(8,128)(2,1)}, bf16[2048,256]{1,0:T(8,128)(2,1)S(1)}, u32[]{:S(2)}, u32[]{:S(2)}) collective-permute-start(bf16[2048,256]{1,0:T(8,128)(2,1)} %bitcast.14.refs_1_), channel_id=1, source_target_pairs={{0,1},{1,0},{2,3},{3,2},{4,5},{5,4},{6,7},{7,6},{8,9},{9,8},{10,11... | collective-permute-start | bytes 3145736 | tf_op jit(solution)/shard_map/ppermute | solution.py:411
  104.5 2.0 %collective-permute-start.10 = (bf16[2048,256]{1,0:T(8,128)(2,1)}, bf16[2048,256]{1,0:T(8,128)(2,1)S(1)}, u32[]{:S(2)}, u32[]{:S(2)}) collective-permute-start(bf16[2048,256]{1,0:T(8,128)(2,1)} %collective-permute-done.8.refs_4_), channel_id=1, source_target_pairs={{0,1},{1,0},{2,3},{3,2},{4,5},{5,4},{6,7},{7,6},{8,9},{9,8},{10,11... | collective-permute-start | bytes 3145736 | tf_op jit(solution)/shard_map/ppermute | solution.py:411
  106.5 10.1 %collective-permute-done.4.refs_10_ = bf16[256,2048]{1,0:T(8,128)(2,1)} collective-permute-done((bf16[256,2048]{1,0:T(8,128)(2,1)S(1)}, bf16[256,2048]{1,0:T(8,128)(2,1)}, u32[]{:S(2)}, u32[]{:S(2)}) %collective-permute-start.4) | collective-permute-done | bytes 1048608 | tf_op jit(solution)/shard_map/ppermute | solution.py:419
  116.6 1.9 %collective-permute-start.11 = (bf16[2048,256]{1,0:T(8,128)(2,1)}, bf16[2048,256]{1,0:T(8,128)(2,1)S(1)}, u32[]{:S(2)}, u32[]{:S(2)}) collective-permute-start(bf16[2048,256]{1,0:T(8,128)(2,1)} %collective-permute-done.9.refs_5_), channel_id=1, source_target_pairs={{0,1},{1,0},{2,3},{3,2},{4,5},{5,4},{6,7},{7,6},{8,9},{9,8},{10,11... | collective-permute-start | bytes 3145736 | tf_op jit(solution)/shard_map/ppermute | solution.py:411
  118.6 2.4 %collective-permute-start.5 = (bf16[256,2048]{1,0:T(8,128)(2,1)}, bf16[256,2048]{1,0:T(8,128)(2,1)S(1)}, u32[]{:S(2)}, u32[]{:S(2)}) collective-permute-start(bf16[256,2048]{1,0:T(8,128)(2,1)} %collective-permute-done.4.refs_10_), channel_id=1, source_target_pairs={{0,1},{1,0},{2,3},{3,2},{4,5},{5,4},{6,7},{7,6},{8,9},{9,8},{10,11... | collective-permute-start | bytes 3145736 | tf_op jit(solution)/shard_map/ppermute | solution.py:411
  123.7 1.2 all-to-all-done.4.in_ref
  124.9 6.2 %shard_map.178 = bf16[16,160,128]{2,1,0:T(8,128)(2,1)S(1)} custom-call(bf16[16,160,128]{2,1,0:T(8,128)(2,1)S(1)} %all-to-all-done.4.in_ref, f32[16,8,128]{2,1,0:T(8,128)S(1)} %get-tuple-element.15.gain_ref, bf16[256,2048]{1,0:T(8,128)(2,1)S(1)} %collective-permute-done.5.late_ref, bf16[2048,256]{1,0:T(8,128)(2,1)} %bitcast.13.refs_0_, ...), custom_call_target="tpu_custom_call" | custom-call | tf_op jit(solution)/shard_map/pallas_call | solution.py:392
  131.1 24.4 %all_to_all.36.in_ref = bf16[16,160,128]{2,1,0:T(8,128)(2,1)S(1)} all-to-all(bf16[16,160,128]{2,1,0:T(8,128)(2,1)S(1)} %shard_map.178), channel_id=1, replica_groups=mesh['z'=8,'x'=4,'y'=8,'c'=2] {'y','c'}, dimensions={0} | all-to-all | bytes 1310720 | tf_op jit(solution)/shard_map/all_to_all | solution.py:403
  156.4 5.7 %all-to-all-start.6 = ((bf16[32,24,128]{2,1,0:T(8,128)(2,1)}), bf16[32,24,128]{2,1,0:T(8,128)(2,1)S(1)}, u32[]{:S(2)}, u32[]{:S(2)}) async-start(bf16[32,24,128]{2,1,0:T(8,128)(2,1)} %bitcast.15), calls=%async_computation.6 | async-start | bytes 393216 | tf_op jit(solution)/shard_map/all_to_all | solution.py:403
  163.1 9.8 %all-to-all-done.6 = bf16[32,24,128]{2,1,0:T(8,128)(2,1)S(1)} async-done(((bf16[32,24,128]{2,1,0:T(8,128)(2,1)}), bf16[32,24,128]{2,1,0:T(8,128)(2,1)S(1)}, u32[]{:S(2)}, u32[]{:S(2)}) %all-to-all-start.6) | async-done | bytes 196640 | tf_op jit(solution)/shard_map/all_to_all | solution.py:403
  (40 shorter events, 6.3 us)
Async XLA Ops:
  2.4 11.0 %copy-start = (bf16[128,2048]{1,0:T(8,128)(2,1)S(1)}, bf16[128,2048]{1,0:T(8,128)(2,1)}, u32[]{:S(2)}) copy-start(bf16[128,2048]{1,0:T(8,128)(2,1)} %w_own_ref.1) | copy-start | bytes 1572868
  2.5 29.7 %all-to-all-start = ((bf16[8,272,128]{2,1,0:T(8,128)(2,1)}), bf16[8,272,128]{2,1,0:T(8,128)(2,1)S(1)}, u32[]{:S(2)}, u32[]{:S(2)}) async-start(bf16[8,272,128]{2,1,0:T(8,128)(2,1)} %get-tuple-element.12), calls=%async_computation | async-start | bytes 1114112 | tf_op jit(solution)/shard_map/all_to_all | solution.py:403
  13.5 29.3 %collective-permute-start.3 = (bf16[128,2048]{1,0:T(8,128)(2,1)S(1)}, bf16[128,2048]{1,0:T(8,128)(2,1)S(1)}, u32[]{:S(2)}, u32[]{:S(2)}) collective-permute-start(bf16[128,2048]{1,0:T(8,128)(2,1)S(1)} %copy-done), channel_id=1, source_target_pairs={{0,1},{1,0},{2,3},{3,2},{4,5},{5,4},{6,7},{7,6},{8,9},{9,8},{10,11... | collective-permute-start | bytes 1572872 | tf_op jit(solution)/shard_map/ppermute | solution.py:411
  16.3 10.6 %collective-permute-start = (bf16[272,128]{1,0:T(8,128)(2,1)S(1)}, bf16[272,128]{1,0:T(8,128)(2,1)S(1)}, u32[]{:S(2)}, u32[]{:S(2)}) collective-permute-start(bf16[272,128]{1,0:T(8,128)(2,1)S(1)} %get-tuple-element.11.refs_0_), channel_id=1, source_target_pairs={{0,16},{16,32},{32,48},{48,0},{1,17},{17,33},{33,49},{49,1},{2,18}... | collective-permute-start | bytes 208904 | tf_op jit(solution)/shard_map/ppermute | solution.py:407
  19.5 7.4 %collective-permute-start.1 = (bf16[272,128]{1,0:T(8,128)(2,1)S(1)}, bf16[272,128]{1,0:T(8,128)(2,1)S(1)}, u32[]{:S(2)}, u32[]{:S(2)}) collective-permute-start(bf16[272,128]{1,0:T(8,128)(2,1)S(1)} %get-tuple-element.11.refs_0_), channel_id=1, source_target_pairs={{0,32},{16,48},{32,0},{48,16},{1,33},{17,49},{33,1},{49,17},{2,34}... | collective-permute-start | bytes 208904 | tf_op jit(solution)/shard_map/ppermute | solution.py:407
  23.8 5.1 %collective-permute-start.2 = (bf16[272,128]{1,0:T(8,128)(2,1)S(1)}, bf16[272,128]{1,0:T(8,128)(2,1)S(1)}, u32[]{:S(2)}, u32[]{:S(2)}) collective-permute-start(bf16[272,128]{1,0:T(8,128)(2,1)S(1)} %get-tuple-element.11.refs_0_), channel_id=1, source_target_pairs={{0,48},{16,0},{32,16},{48,32},{1,49},{17,1},{33,17},{49,33},{2,50}... | collective-permute-start | bytes 208904 | tf_op jit(solution)/shard_map/ppermute | solution.py:407
  38.0 11.6 %all-to-all-start.1 = ((bf16[8,144,128]{2,1,0:T(8,128)(2,1)}), bf16[8,144,128]{2,1,0:T(8,128)(2,1)S(1)}, u32[]{:S(2)}, u32[]{:S(2)}) async-start(bf16[8,144,128]{2,1,0:T(8,128)(2,1)} %shard_map.173), calls=%async_computation.1 | async-start | bytes 589824 | tf_op jit(solution)/shard_map/all_to_all | solution.py:403
  51.1 14.8 %copy-start.6 = (bf16[1,256,2048]{2,1,0:T(8,128)(2,1)S(1)}, bf16[1,256,2048]{2,1,0:T(8,128)(2,1)}, u32[]{:S(2)}) copy-start(bf16[1,256,2048]{2,1,0:T(8,128)(2,1)} %param.31) | copy-start | bytes 3145732
  51.1 26.9 %all-to-all-start.2 = ((bf16[16,144,128]{2,1,0:T(8,128)(2,1)}), bf16[16,144,128]{2,1,0:T(8,128)(2,1)S(1)}, u32[]{:S(2)}, u32[]{:S(2)}) async-start(bf16[16,144,128]{2,1,0:T(8,128)(2,1)} %shard_map.174), calls=%async_computation.2 | async-start | bytes 1179648 | tf_op jit(solution)/shard_map/all_to_all | solution.py:403
  59.4 42.7 %collective-permute-start.8 = (bf16[2048,256]{1,0:T(8,128)(2,1)}, bf16[2048,256]{1,0:T(8,128)(2,1)}, u32[]{:S(2)}, u32[]{:S(2)}) collective-permute-start(bf16[2048,256]{1,0:T(8,128)(2,1)} %bitcast.13.refs_0_), channel_id=1, source_target_pairs={{0,2},{1,15},{2,0},{3,5},{4,6},{5,3},{6,4},{7,9},{8,10},{9,7},{10,... | collective-permute-start | bytes 3145736 | tf_op jit(solution)/shard_map/ppermute | solution.py:419
  63.9 8.5 %copy-start.4 = (s32[256,2]{0,1:T(2,128)S(1)}, s32[256,2]{0,1:T(2,128)}, u32[]{:S(2)}) copy-start(s32[256,2]{0,1:T(2,128)} %param.27) | copy-start | bytes 6148
  63.9 40.5 %collective-permute-start.9 = (bf16[2048,256]{1,0:T(8,128)(2,1)}, bf16[2048,256]{1,0:T(8,128)(2,1)}, u32[]{:S(2)}, u32[]{:S(2)}) collective-permute-start(bf16[2048,256]{1,0:T(8,128)(2,1)} %bitcast.14.refs_1_), channel_id=1, source_target_pairs={{0,2},{1,15},{2,0},{3,5},{4,6},{5,3},{6,4},{7,9},{8,10},{9,7},{10,... | collective-permute-start | bytes 3145736 | tf_op jit(solution)/shard_map/ppermute | solution.py:419
  66.0 50.7 %collective-permute-start.4 = (bf16[256,2048]{1,0:T(8,128)(2,1)S(1)}, bf16[256,2048]{1,0:T(8,128)(2,1)}, u32[]{:S(2)}, u32[]{:S(2)}) collective-permute-start(bf16[256,2048]{1,0:T(8,128)(2,1)S(1)} %bitcast.29), channel_id=1, source_target_pairs={{0,2},{1,15},{2,0},{3,5},{4,6},{5,3},{6,4},{7,9},{8,10},{9,7},{10,... | collective-permute-start | bytes 3145736 | tf_op jit(solution)/shard_map/ppermute | solution.py:419
  70.5 48.1 %collective-permute-start.12 = (bf16[256,2048]{1,0:T(8,128)(2,1)S(1)}, bf16[256,2048]{1,0:T(8,128)(2,1)}, u32[]{:S(2)}, u32[]{:S(2)}) collective-permute-start(bf16[256,2048]{1,0:T(8,128)(2,1)S(1)} %bitcast.30), channel_id=1, source_target_pairs={{0,1},{1,0},{2,3},{3,2},{4,5},{5,4},{6,7},{7,6},{8,9},{9,8},{10,11... | collective-permute-start | bytes 3145736 | tf_op jit(solution)/shard_map/ppermute | solution.py:411
  72.4 5.6 %copy-start.3 = (bf16[256,128]{1,0:T(8,128)(2,1)S(1)}, bf16[256,128]{1,0:T(8,128)(2,1)}, u32[]{:S(2)}) copy-start(bf16[256,128]{1,0:T(8,128)(2,1)} %residual_ref.1) | copy-start | bytes 196612
  78.3 16.9 %copy-start.2 = (bf16[160,192]{1,0:T(8,128)(2,1)S(1)}, bf16[160,192]{1,0:T(8,128)(2,1)}, u32[]{:S(2)}) copy-start(bf16[160,192]{1,0:T(8,128)(2,1)} %constant.28.clone.drop_ref) | copy-start | bytes 184324
  96.4 28.5 %all-to-all-start.4 = ((bf16[16,160,128]{2,1,0:T(8,128)(2,1)}), bf16[16,160,128]{2,1,0:T(8,128)(2,1)S(1)}, u32[]{:S(2)}, u32[]{:S(2)}) async-start(bf16[16,160,128]{2,1,0:T(8,128)(2,1)} %shard_map.177), calls=%async_computation.4 | async-start | bytes 1310720 | tf_op jit(solution)/shard_map/all_to_all | solution.py:403
  100.1 20.9 %collective-permute-start.6 = (bf16[2048,256]{1,0:T(8,128)(2,1)}, bf16[2048,256]{1,0:T(8,128)(2,1)S(1)}, u32[]{:S(2)}, u32[]{:S(2)}) collective-permute-start(bf16[2048,256]{1,0:T(8,128)(2,1)} %bitcast.13.refs_0_), channel_id=1, source_target_pairs={{0,1},{1,0},{2,3},{3,2},{4,5},{5,4},{6,7},{7,6},{8,9},{9,8},{10,11... | collective-permute-start | bytes 3145736 | tf_op jit(solution)/shard_map/ppermute | solution.py:411
  102.2 18.8 %collective-permute-start.7 = (bf16[2048,256]{1,0:T(8,128)(2,1)}, bf16[2048,256]{1,0:T(8,128)(2,1)S(1)}, u32[]{:S(2)}, u32[]{:S(2)}) collective-permute-start(bf16[2048,256]{1,0:T(8,128)(2,1)} %bitcast.14.refs_1_), channel_id=1, source_target_pairs={{0,1},{1,0},{2,3},{3,2},{4,5},{5,4},{6,7},{7,6},{8,9},{9,8},{10,11... | collective-permute-start | bytes 3145736 | tf_op jit(solution)/shard_map/ppermute | solution.py:411
  104.5 16.5 %collective-permute-start.10 = (bf16[2048,256]{1,0:T(8,128)(2,1)}, bf16[2048,256]{1,0:T(8,128)(2,1)S(1)}, u32[]{:S(2)}, u32[]{:S(2)}) collective-permute-start(bf16[2048,256]{1,0:T(8,128)(2,1)} %collective-permute-done.8.refs_4_), channel_id=1, source_target_pairs={{0,1},{1,0},{2,3},{3,2},{4,5},{5,4},{6,7},{7,6},{8,9},{9,8},{10,11... | collective-permute-start | bytes 3145736 | tf_op jit(solution)/shard_map/ppermute | solution.py:411
  116.6 4.8 %collective-permute-start.11 = (bf16[2048,256]{1,0:T(8,128)(2,1)}, bf16[2048,256]{1,0:T(8,128)(2,1)S(1)}, u32[]{:S(2)}, u32[]{:S(2)}) collective-permute-start(bf16[2048,256]{1,0:T(8,128)(2,1)} %collective-permute-done.9.refs_5_), channel_id=1, source_target_pairs={{0,1},{1,0},{2,3},{3,2},{4,5},{5,4},{6,7},{7,6},{8,9},{9,8},{10,11... | collective-permute-start | bytes 3145736 | tf_op jit(solution)/shard_map/ppermute | solution.py:411
  118.6 5.2 %collective-permute-start.5 = (bf16[256,2048]{1,0:T(8,128)(2,1)}, bf16[256,2048]{1,0:T(8,128)(2,1)S(1)}, u32[]{:S(2)}, u32[]{:S(2)}) collective-permute-start(bf16[256,2048]{1,0:T(8,128)(2,1)} %collective-permute-done.4.refs_10_), channel_id=1, source_target_pairs={{0,1},{1,0},{2,3},{3,2},{4,5},{5,4},{6,7},{7,6},{8,9},{9,8},{10,11... | collective-permute-start | bytes 3145736 | tf_op jit(solution)/shard_map/ppermute | solution.py:411
  121.0 1.0 copy-start.7
  121.0 1.4 copy-start.8
  121.0 1.6 copy-start.9
  122.7 1.1 copy-start.10
  131.1 24.4 %copy-start.1 = (bf16[192,160]{1,0:T(8,128)(2,1)S(1)}, bf16[192,160]{1,0:T(8,128)(2,1)}, u32[]{:S(2)}) copy-start(bf16[192,160]{1,0:T(8,128)(2,1)} %constant.29.clone.widen_ref) | copy-start | bytes 184324
  156.4 5.7 %copy-start.5 = (f32[256,2]{0,1:T(2,128)S(1)}, f32[256,2]{0,1:T(2,128)}, u32[]{:S(2)}) copy-start(f32[256,2]{0,1:T(2,128)} %param.28) | copy-start | bytes 6148
  156.4 16.4 %all-to-all-start.6 = ((bf16[32,24,128]{2,1,0:T(8,128)(2,1)}), bf16[32,24,128]{2,1,0:T(8,128)(2,1)S(1)}, u32[]{:S(2)}, u32[]{:S(2)}) async-start(bf16[32,24,128]{2,1,0:T(8,128)(2,1)} %bitcast.15), calls=%async_computation.6 | async-start | bytes 393216 | tf_op jit(solution)/shard_map/all_to_all | solution.py:403

commit v8 on v7

--- a/solution.py
+++ b/solution.py
@@ -27,7 +27,8 @@
 GROUPS = 4
 ROWS = N_SP * CAP // GROUPS
 BLOCKS = N_SP // GROUPS
-NOTE = 16
+NOTE = 8
+SUMS = 16
 MASK_BIG = 16384.0
 WINDOWS = (5, 6, N_Z)
 
@@ -151,7 +152,7 @@
         kp_ref[j * TOK : (j + 1) * TOK, :] = jnp.where(low, kf, mark).astype(BF16)
         vt_ref[j, :HD, :HALF] = kv_ref[j, HALF : HALF + HD, :]
         vt_ref[j, :HD, HALF:] = kv_ref[j, HALF + HD : TOK, :]
-        vt_ref[j, HD:, :] = jnp.ones((NOTE, TOK), BF16)
+        vt_ref[j, HD:, :] = jnp.ones((SUMS, TOK), BF16)
 
     def documents(note):
         n0, n1 = note[0:1, :].astype(F32), note[1:2, :].astype(F32)
@@ -179,7 +180,7 @@
         other = jnp.where((doc == lane) | (lane > HD + 2), 0.0, -MASK_BIG)
         heads = [jnp.where(low, qh, other).astype(BF16) for qh in (qf, pltpu.roll(qf, HD, 1))]
         peaks = [jnp.full((8, TOK), -jnp.inf, F32) for _ in heads]
-        accs = [jnp.zeros((HD + NOTE, TOK), F32) for _ in heads]
+        accs = [jnp.zeros((HD + SUMS, TOK), F32) for _ in heads]
         tops = [None, None]
 
         def score(h, j):
@@ -320,8 +321,8 @@
             out_ref[g] = kept
 
 
-def expert_body(in_ref, gain_ref, late_ref, *refs):
-    many = 3 * GROUPS - 1
+def expert_body(in_ref, gain_ref, late0_ref, late1_ref, *refs):
+    many = 3 * GROUPS - 2
     far, (out_ref, x_ref), weights, sems = refs[:many], refs[many : many + 2], refs[many + 2 : -1], refs[-1]
     copies = [pltpu.make_async_copy(far[i], weights[i], sems.at[i]) for i in range(many)]
     for copy in copies[:4]:
@@ -346,7 +347,8 @@
         hidden.append(unit.astype(BF16))
     for copy in copies[2 * GROUPS :]:
         copy.wait()
-    downs = weights[2 * GROUPS :] + (late_ref,)
+    own_down, far_down = weights[2 * GROUPS :]
+    downs = (own_down, late0_ref, far_down, late1_ref)
     for g in range(0, N_TP, 2):
         cols = slice(g * LANES, (g + 2) * LANES)
         part = dot(hidden[0], downs[0][:, cols])
@@ -523,7 +525,7 @@
         scratch=[
             pltpu.VMEM((N_X, TOK + NOTE, LANES), BF16),
             pltpu.VMEM((N_Z * TOK, LANES), BF16),
-            pltpu.VMEM((N_Z, HD + NOTE, TOK), BF16),
+            pltpu.VMEM((N_Z, HD + SUMS, TOK), BF16),
             pltpu.VMEM((2, N_Z, TOK, TOK), F32),
             pltpu.SMEM((N_X,), jnp.int32),
         ],
@@ -559,12 +561,13 @@
         jnp.asarray(drop, BF16),
     )
     columns = exchange(spread, ("y", "c"))
-    weights = (gate, up, gate_o, up_o, gate_y, up_y, gate_yo, up_yo, down, down_o, down_y)
+    weights = (gate, up, gate_o, up_o, gate_y, up_y, gate_yo, up_yo, down, down_y)
     parts = call(
         expert_body,
         shaped((N_TP, ROWS, LANES)),
         columns,
         gain_all,
+        down_o,
         down_yo,
         *weights,
         scratch=[pltpu.VMEM((ROWS, D), BF16)]

time: 175 us -> 174 us (level)
  no operation moved by 1% of the time
where the time goes in v8:
time: 174 us; the launch traced here: 173 us
  starting transfers between devices  70.5 us (41%)
  blocking collectives  41.6 us (24%)
  waiting for transfers between devices  37.4 us (21%)
  Pallas kernels  20.5 us (12%)
  local copies, waits for them, and re-layouts  2.28 us (1%)
    all_to_all x2, blocking collectives, exchange(): return lax.all_to_all(x, axes, 0, 0, tiled=True)  41.6 us
    all_to_all x5, starting transfers between devices, exchange(): return lax.all_to_all(x, axes, 0, 0, tiled=True)  33.6 us
    all_to_all x5, waiting for transfers between devices, exchange(): return lax.all_to_all(x, axes, 0, 0, tiled=True)  25.1 us
    pallas_call x12, Pallas kernels, call(): pl.pallas_call(body, out_shape=outs, in_specs=specs, out_specs=[VMEM] * l...  20.5 us
    ppermute x7, starting transfers between devices, partner(): return lax.ppermute(x, 'c', [(0, 1), (1, 0)])  15.4 us
    ppermute x3, starting transfers between devices, neighbour(): return lax.ppermute(x, ('y', 'c'), pairs)  11 us
    ppermute x3, starting transfers between devices, shifted(): return lax.ppermute(x, axis, [(i, (i + by) % size) for i in range(size)])  10.5 us
    ppermute x3, waiting for transfers between devices, neighbour(): return lax.ppermute(x, ('y', 'c'), pairs)  9.98 us
  transfers between devices with their start and end apart: 18, of which 8 were waited for; matrix products, arithmetic and copies ran while one was open for 0% of the time, Pallas kernels for 5%

profile of v8, /device:TPU:1, one launch (start us, length us, event | category | flops | bytes accessed | tf_op | source)
XLA Modules:
  0.0 172.6 jit_solution(11013704767128253188)
XLA Ops:
  0.0 2.4 %shard_map.172 = (bf16[264,128]{1,0:T(8,128)(2,1)S(1)}, bf16[8,264,128]{2,1,0:T(8,128)(2,1)}, f32[1,128]{1,0:T(1,128)S(1)}) custom-call(s32[1]{0:T(128)} %bitcast.2.blk, bf16[256,128]{1,0:T(8,128)(2,1)} %refs_0_.1, bf16[64,256]{1,0:T(8,128)(2,1)} %bitcast.28, bf16[64,256]{1,0:T(8,128)(2,1)} %bitcast.29, s32[2,128]{1,0:T(2,128)} %bitcast.30, ...), custom_call_target="tpu_custom_call" | custom-call | tf_op jit(solution)/shard_map/pallas_call | solution.py:394
  2.5 11.0 %all-to-all-start = ((bf16[8,264,128]{2,1,0:T(8,128)(2,1)}), bf16[8,264,128]{2,1,0:T(8,128)(2,1)S(1)}, u32[]{:S(2)}, u32[]{:S(2)}) async-start(bf16[8,264,128]{2,1,0:T(8,128)(2,1)} %get-tuple-element.12), calls=%async_computation | async-start | bytes 1081344 | tf_op jit(solution)/shard_map/all_to_all | solution.py:405
  13.5 2.9 %collective-permute-start.3 = (bf16[128,2048]{1,0:T(8,128)(2,1)S(1)}, bf16[128,2048]{1,0:T(8,128)(2,1)S(1)}, u32[]{:S(2)}, u32[]{:S(2)}) collective-permute-start(bf16[128,2048]{1,0:T(8,128)(2,1)S(1)} %copy-done), channel_id=1, source_target_pairs={{0,1},{1,0},{2,3},{3,2},{4,5},{5,4},{6,7},{7,6},{8,9},{9,8},{10,11... | collective-permute-start | bytes 1572872 | tf_op jit(solution)/shard_map/ppermute | solution.py:413
  16.3 3.1 %collective-permute-start = (bf16[264,128]{1,0:T(8,128)(2,1)S(1)}, bf16[264,128]{1,0:T(8,128)(2,1)S(1)}, u32[]{:S(2)}, u32[]{:S(2)}) collective-permute-start(bf16[264,128]{1,0:T(8,128)(2,1)S(1)} %get-tuple-element.11.refs_0_), channel_id=1, source_target_pairs={{0,16},{16,32},{32,48},{48,0},{1,17},{17,33},{33,49},{49,1},{2,18}... | collective-permute-start | bytes 202760 | tf_op jit(solution)/shard_map/ppermute | solution.py:409
  19.5 4.4 %collective-permute-start.1 = (bf16[264,128]{1,0:T(8,128)(2,1)S(1)}, bf16[264,128]{1,0:T(8,128)(2,1)S(1)}, u32[]{:S(2)}, u32[]{:S(2)}) collective-permute-start(bf16[264,128]{1,0:T(8,128)(2,1)S(1)} %get-tuple-element.11.refs_0_), channel_id=1, source_target_pairs={{0,32},{16,48},{32,0},{48,16},{1,33},{17,49},{33,1},{49,17},{2,34}... | collective-permute-start | bytes 202760 | tf_op jit(solution)/shard_map/ppermute | solution.py:409
  23.8 3.1 %collective-permute-start.2 = (bf16[264,128]{1,0:T(8,128)(2,1)S(1)}, bf16[264,128]{1,0:T(8,128)(2,1)S(1)}, u32[]{:S(2)}, u32[]{:S(2)}) collective-permute-start(bf16[264,128]{1,0:T(8,128)(2,1)S(1)} %get-tuple-element.11.refs_0_), channel_id=1, source_target_pairs={{0,48},{16,0},{32,16},{48,32},{1,49},{17,1},{33,17},{49,33},{2,50}... | collective-permute-start | bytes 202760 | tf_op jit(solution)/shard_map/ppermute | solution.py:409
  26.9 1.9 %collective-permute-done.2.refs_3_ = bf16[264,128]{1,0:T(8,128)(2,1)S(1)} collective-permute-done((bf16[264,128]{1,0:T(8,128)(2,1)S(1)}, bf16[264,128]{1,0:T(8,128)(2,1)S(1)}, u32[]{:S(2)}, u32[]{:S(2)}) %collective-permute-start.2) | collective-permute-done | bytes 67616 | tf_op jit(solution)/shard_map/ppermute | solution.py:409
  28.9 2.9 %all-to-all-done.refs_4_ = bf16[8,264,128]{2,1,0:T(8,128)(2,1)S(1)} async-done(((bf16[8,264,128]{2,1,0:T(8,128)(2,1)}), bf16[8,264,128]{2,1,0:T(8,128)(2,1)S(1)}, u32[]{:S(2)}, u32[]{:S(2)}) %all-to-all-start) | async-done | bytes 540704 | tf_op jit(solution)/shard_map/all_to_all | solution.py:405
  31.8 5.9 %shard_map.173 = bf16[8,136,128]{2,1,0:T(8,128)(2,1)} custom-call(s32[1]{0:T(128)} %bitcast.1.spot, bf16[264,128]{1,0:T(8,128)(2,1)S(1)} %get-tuple-element.11.refs_0_, bf16[264,128]{1,0:T(8,128)(2,1)S(1)} %collective-permute-done.refs_1_, bf16[264,128]{1,0:T(8,128)(2,1)S(1)} %collective-permute-done.1.refs_2_, ...), custom_call_target="tpu_custom_call" | custom-call | tf_op jit(solution)/shard_map/pallas_call | solution.py:394
  37.7 4.8 %all-to-all-start.1 = ((bf16[8,136,128]{2,1,0:T(8,128)(2,1)}), bf16[8,136,128]{2,1,0:T(8,128)(2,1)S(1)}, u32[]{:S(2)}, u32[]{:S(2)}) async-start(bf16[8,136,128]{2,1,0:T(8,128)(2,1)} %shard_map.173), calls=%async_computation.1 | async-start | bytes 557056 | tf_op jit(solution)/shard_map/all_to_all | solution.py:405
  42.4 6.6 %all-to-all-done.1.in_ref = bf16[8,136,128]{2,1,0:T(8,128)(2,1)S(1)} async-done(((bf16[8,136,128]{2,1,0:T(8,128)(2,1)}), bf16[8,136,128]{2,1,0:T(8,128)(2,1)S(1)}, u32[]{:S(2)}, u32[]{:S(2)}) %all-to-all-start.1) | async-done | bytes 278560 | tf_op jit(solution)/shard_map/all_to_all | solution.py:405
  49.1 1.6 shard_map.174
  50.6 8.2 %all-to-all-start.2 = ((bf16[16,136,128]{2,1,0:T(8,128)(2,1)}), bf16[16,136,128]{2,1,0:T(8,128)(2,1)S(1)}, u32[]{:S(2)}, u32[]{:S(2)}) async-start(bf16[16,136,128]{2,1,0:T(8,128)(2,1)} %shard_map.174), calls=%async_computation.2 | async-start | bytes 1114112 | tf_op jit(solution)/shard_map/all_to_all | solution.py:405
  58.8 4.5 %collective-permute-start.9 = (bf16[2048,256]{1,0:T(8,128)(2,1)}, bf16[2048,256]{1,0:T(8,128)(2,1)}, u32[]{:S(2)}, u32[]{:S(2)}) collective-permute-start(bf16[2048,256]{1,0:T(8,128)(2,1)} %bitcast.13.refs_0_), channel_id=1, source_target_pairs={{0,2},{1,15},{2,0},{3,5},{4,6},{5,3},{6,4},{7,9},{8,10},{9,7},{10,... | collective-permute-start | bytes 3145736 | tf_op jit(solution)/shard_map/ppermute | solution.py:421
  63.3 2.0 %collective-permute-start.10 = (bf16[2048,256]{1,0:T(8,128)(2,1)}, bf16[2048,256]{1,0:T(8,128)(2,1)}, u32[]{:S(2)}, u32[]{:S(2)}) collective-permute-start(bf16[2048,256]{1,0:T(8,128)(2,1)} %bitcast.14.refs_1_), channel_id=1, source_target_pairs={{0,2},{1,15},{2,0},{3,5},{4,6},{5,3},{6,4},{7,9},{8,10},{9,7},{10,... | collective-permute-start | bytes 3145736 | tf_op jit(solution)/shard_map/ppermute | solution.py:421
  65.3 4.5 %collective-permute-start.5 = (bf16[256,2048]{1,0:T(8,128)(2,1)}, bf16[256,2048]{1,0:T(8,128)(2,1)}, u32[]{:S(2)}, u32[]{:S(2)}) collective-permute-start(bf16[256,2048]{1,0:T(8,128)(2,1)} %bitcast.12.refs_8_), channel_id=1, source_target_pairs={{0,2},{1,15},{2,0},{3,5},{4,6},{5,3},{6,4},{7,9},{8,10},{9,7},{10,... | collective-permute-start | bytes 3145736 | tf_op jit(solution)/shard_map/ppermute | solution.py:421
  69.8 1.9 %collective-permute-start.4 = (bf16[256,2048]{1,0:T(8,128)(2,1)}, bf16[256,2048]{1,0:T(8,128)(2,1)S(1)}, u32[]{:S(2)}, u32[]{:S(2)}) collective-permute-start(bf16[256,2048]{1,0:T(8,128)(2,1)} %bitcast.12.refs_8_), channel_id=1, source_target_pairs={{0,1},{1,0},{2,3},{3,2},{4,5},{5,4},{6,7},{7,6},{8,9},{9,8},{10,11... | collective-permute-start | bytes 3145736 | tf_op jit(solution)/shard_map/ppermute | solution.py:413
  72.0 4.7 %all-to-all-done.2.in_ref = bf16[16,136,128]{2,1,0:T(8,128)(2,1)S(1)} async-done(((bf16[16,136,128]{2,1,0:T(8,128)(2,1)}), bf16[16,136,128]{2,1,0:T(8,128)(2,1)S(1)}, u32[]{:S(2)}, u32[]{:S(2)}) %all-to-all-start.2) | async-done | bytes 557088 | tf_op jit(solution)/shard_map/all_to_all | solution.py:405
  77.0 17.3 %all_to_all.35 = bf16[32,24,128]{2,1,0:T(8,128)(2,1)S(1)} all-to-all(bf16[32,24,128]{2,1,0:T(8,128)(2,1)S(1)} %bitcast.20), channel_id=1, replica_groups=mesh['z'=8,'x'=4,'y'=8,'c'=2] {'z','x'}, dimensions={0} | all-to-all | bytes 393216 | tf_op jit(solution)/shard_map/all_to_all | solution.py:405
  94.4 1.1 shard_map.177
  95.5 3.6 %all-to-all-start.4 = ((bf16[16,160,128]{2,1,0:T(8,128)(2,1)}), bf16[16,160,128]{2,1,0:T(8,128)(2,1)S(1)}, u32[]{:S(2)}, u32[]{:S(2)}) async-start(bf16[16,160,128]{2,1,0:T(8,128)(2,1)} %shard_map.177), calls=%async_computation.4 | async-start | bytes 1310720 | tf_op jit(solution)/shard_map/all_to_all | solution.py:405
  99.1 2.0 %collective-permute-start.7 = (bf16[2048,256]{1,0:T(8,128)(2,1)}, bf16[2048,256]{1,0:T(8,128)(2,1)S(1)}, u32[]{:S(2)}, u32[]{:S(2)}) collective-permute-start(bf16[2048,256]{1,0:T(8,128)(2,1)} %bitcast.13.refs_0_), channel_id=1, source_target_pairs={{0,1},{1,0},{2,3},{3,2},{4,5},{5,4},{6,7},{7,6},{8,9},{9,8},{10,11... | collective-permute-start | bytes 3145736 | tf_op jit(solution)/shard_map/ppermute | solution.py:413
  101.2 2.3 %collective-permute-start.8 = (bf16[2048,256]{1,0:T(8,128)(2,1)}, bf16[2048,256]{1,0:T(8,128)(2,1)S(1)}, u32[]{:S(2)}, u32[]{:S(2)}) collective-permute-start(bf16[2048,256]{1,0:T(8,128)(2,1)} %bitcast.14.refs_1_), channel_id=1, source_target_pairs={{0,1},{1,0},{2,3},{3,2},{4,5},{5,4},{6,7},{7,6},{8,9},{9,8},{10,11... | collective-permute-start | bytes 3145736 | tf_op jit(solution)/shard_map/ppermute | solution.py:413
  103.5 2.0 %collective-permute-start.11 = (bf16[2048,256]{1,0:T(8,128)(2,1)}, bf16[2048,256]{1,0:T(8,128)(2,1)S(1)}, u32[]{:S(2)}, u32[]{:S(2)}) collective-permute-start(bf16[2048,256]{1,0:T(8,128)(2,1)} %collective-permute-done.9.refs_4_), channel_id=1, source_target_pairs={{0,1},{1,0},{2,3},{3,2},{4,5},{5,4},{6,7},{7,6},{8,9},{9,8},{10,11... | collective-permute-start | bytes 3145736 | tf_op jit(solution)/shard_map/ppermute | solution.py:413
  105.5 10.0 %collective-permute-done.5.refs_9_ = bf16[256,2048]{1,0:T(8,128)(2,1)} collective-permute-done((bf16[256,2048]{1,0:T(8,128)(2,1)}, bf16[256,2048]{1,0:T(8,128)(2,1)}, u32[]{:S(2)}, u32[]{:S(2)}) %collective-permute-start.5) | collective-permute-done | bytes 1048608 | tf_op jit(solution)/shard_map/ppermute | solution.py:421
  115.5 1.9 %collective-permute-start.12 = (bf16[2048,256]{1,0:T(8,128)(2,1)}, bf16[2048,256]{1,0:T(8,128)(2,1)S(1)}, u32[]{:S(2)}, u32[]{:S(2)}) collective-permute-start(bf16[2048,256]{1,0:T(8,128)(2,1)} %collective-permute-done.10.refs_5_), channel_id=1, source_target_pairs={{0,1},{1,0},{2,3},{3,2},{4,5},{5,4},{6,7},{7,6},{8,9},{9,8},{10,11... | collective-permute-start | bytes 3145736 | tf_op jit(solution)/shard_map/ppermute | solution.py:413
  117.4 2.4 %collective-permute-start.6 = (bf16[256,2048]{1,0:T(8,128)(2,1)}, bf16[256,2048]{1,0:T(8,128)(2,1)S(1)}, u32[]{:S(2)}, u32[]{:S(2)}) collective-permute-start(bf16[256,2048]{1,0:T(8,128)(2,1)} %collective-permute-done.5.refs_9_), channel_id=1, source_target_pairs={{0,1},{1,0},{2,3},{3,2},{4,5},{5,4},{6,7},{7,6},{8,9},{9,8},{10,11... | collective-permute-start | bytes 3145736 | tf_op jit(solution)/shard_map/ppermute | solution.py:413
  122.5 1.1 all-to-all-done.4.in_ref
  123.6 5.9 %shard_map.178 = bf16[16,160,128]{2,1,0:T(8,128)(2,1)S(1)} custom-call(bf16[16,160,128]{2,1,0:T(8,128)(2,1)S(1)} %all-to-all-done.4.in_ref, f32[16,8,128]{2,1,0:T(8,128)S(1)} %get-tuple-element.15.gain_ref, bf16[256,2048]{1,0:T(8,128)(2,1)S(1)} %collective-permute-done.4.late0_ref, bf16[256,2048]{1,0:T(8,128)(2,1)S(1)} %collective-permute-done.6.late1_ref, ...), custom_call_target="tpu_custom_call" | custom-call | tf_op jit(solution)/shard_map/pallas_call | solution.py:394
  129.5 24.3 %all_to_all.36.in_ref = bf16[16,160,128]{2,1,0:T(8,128)(2,1)S(1)} all-to-all(bf16[16,160,128]{2,1,0:T(8,128)(2,1)S(1)} %shard_map.178), channel_id=1, replica_groups=mesh['z'=8,'x'=4,'y'=8,'c'=2] {'y','c'}, dimensions={0} | all-to-all | bytes 1310720 | tf_op jit(solution)/shard_map/all_to_all | solution.py:405
  154.7 6.0 %all-to-all-start.6 = ((bf16[32,24,128]{2,1,0:T(8,128)(2,1)}), bf16[32,24,128]{2,1,0:T(8,128)(2,1)S(1)}, u32[]{:S(2)}, u32[]{:S(2)}) async-start(bf16[32,24,128]{2,1,0:T(8,128)(2,1)} %bitcast.15), calls=%async_computation.6 | async-start | bytes 393216 | tf_op jit(solution)/shard_map/all_to_all | solution.py:405
  161.7 9.7 %all-to-all-done.6 = bf16[32,24,128]{2,1,0:T(8,128)(2,1)S(1)} async-done(((bf16[32,24,128]{2,1,0:T(8,128)(2,1)}), bf16[32,24,128]{2,1,0:T(8,128)(2,1)S(1)}, u32[]{:S(2)}, u32[]{:S(2)}) %all-to-all-start.6) | async-done | bytes 196640 | tf_op jit(solution)/shard_map/all_to_all | solution.py:405
  (38 shorter events, 6.2 us)
Async XLA Ops:
  2.4 11.0 %copy-start = (bf16[128,2048]{1,0:T(8,128)(2,1)S(1)}, bf16[128,2048]{1,0:T(8,128)(2,1)}, u32[]{:S(2)}) copy-start(bf16[128,2048]{1,0:T(8,128)(2,1)} %w_own_ref.1) | copy-start | bytes 1572868
  2.5 29.3 %all-to-all-start = ((bf16[8,264,128]{2,1,0:T(8,128)(2,1)}), bf16[8,264,128]{2,1,0:T(8,128)(2,1)S(1)}, u32[]{:S(2)}, u32[]{:S(2)}) async-start(bf16[8,264,128]{2,1,0:T(8,128)(2,1)} %get-tuple-element.12), calls=%async_computation | async-start | bytes 1081344 | tf_op jit(solution)/shard_map/all_to_all | solution.py:405
  13.5 29.0 %collective-permute-start.3 = (bf16[128,2048]{1,0:T(8,128)(2,1)S(1)}, bf16[128,2048]{1,0:T(8,128)(2,1)S(1)}, u32[]{:S(2)}, u32[]{:S(2)}) collective-permute-start(bf16[128,2048]{1,0:T(8,128)(2,1)S(1)} %copy-done), channel_id=1, source_target_pairs={{0,1},{1,0},{2,3},{3,2},{4,5},{5,4},{6,7},{7,6},{8,9},{9,8},{10,11... | collective-permute-start | bytes 1572872 | tf_op jit(solution)/shard_map/ppermute | solution.py:413
  16.3 10.6 %collective-permute-start = (bf16[264,128]{1,0:T(8,128)(2,1)S(1)}, bf16[264,128]{1,0:T(8,128)(2,1)S(1)}, u32[]{:S(2)}, u32[]{:S(2)}) collective-permute-start(bf16[264,128]{1,0:T(8,128)(2,1)S(1)} %get-tuple-element.11.refs_0_), channel_id=1, source_target_pairs={{0,16},{16,32},{32,48},{48,0},{1,17},{17,33},{33,49},{49,1},{2,18}... | collective-permute-start | bytes 202760 | tf_op jit(solution)/shard_map/ppermute | solution.py:409
  19.5 7.4 %collective-permute-start.1 = (bf16[264,128]{1,0:T(8,128)(2,1)S(1)}, bf16[264,128]{1,0:T(8,128)(2,1)S(1)}, u32[]{:S(2)}, u32[]{:S(2)}) collective-permute-start(bf16[264,128]{1,0:T(8,128)(2,1)S(1)} %get-tuple-element.11.refs_0_), channel_id=1, source_target_pairs={{0,32},{16,48},{32,0},{48,16},{1,33},{17,49},{33,1},{49,17},{2,34}... | collective-permute-start | bytes 202760 | tf_op jit(solution)/shard_map/ppermute | solution.py:409
  23.8 5.0 %collective-permute-start.2 = (bf16[264,128]{1,0:T(8,128)(2,1)S(1)}, bf16[264,128]{1,0:T(8,128)(2,1)S(1)}, u32[]{:S(2)}, u32[]{:S(2)}) collective-permute-start(bf16[264,128]{1,0:T(8,128)(2,1)S(1)} %get-tuple-element.11.refs_0_), channel_id=1, source_target_pairs={{0,48},{16,0},{32,16},{48,32},{1,49},{17,1},{33,17},{49,33},{2,50}... | collective-permute-start | bytes 202760 | tf_op jit(solution)/shard_map/ppermute | solution.py:409
  37.7 11.4 %all-to-all-start.1 = ((bf16[8,136,128]{2,1,0:T(8,128)(2,1)}), bf16[8,136,128]{2,1,0:T(8,128)(2,1)S(1)}, u32[]{:S(2)}, u32[]{:S(2)}) async-start(bf16[8,136,128]{2,1,0:T(8,128)(2,1)} %shard_map.173), calls=%async_computation.1 | async-start | bytes 557056 | tf_op jit(solution)/shard_map/all_to_all | solution.py:405
  50.6 26.0 %all-to-all-start.2 = ((bf16[16,136,128]{2,1,0:T(8,128)(2,1)}), bf16[16,136,128]{2,1,0:T(8,128)(2,1)S(1)}, u32[]{:S(2)}, u32[]{:S(2)}) async-start(bf16[16,136,128]{2,1,0:T(8,128)(2,1)} %shard_map.174), calls=%async_computation.2 | async-start | bytes 1114112 | tf_op jit(solution)/shard_map/all_to_all | solution.py:405
  58.8 42.3 %collective-permute-start.9 = (bf16[2048,256]{1,0:T(8,128)(2,1)}, bf16[2048,256]{1,0:T(8,128)(2,1)}, u32[]{:S(2)}, u32[]{:S(2)}) collective-permute-start(bf16[2048,256]{1,0:T(8,128)(2,1)} %bitcast.13.refs_0_), channel_id=1, source_target_pairs={{0,2},{1,15},{2,0},{3,5},{4,6},{5,3},{6,4},{7,9},{8,10},{9,7},{10,... | collective-permute-start | bytes 3145736 | tf_op jit(solution)/shard_map/ppermute | solution.py:421
  63.3 8.5 %copy-start.4 = (s32[256,2]{0,1:T(2,128)S(1)}, s32[256,2]{0,1:T(2,128)}, u32[]{:S(2)}) copy-start(s32[256,2]{0,1:T(2,128)} %param.27) | copy-start | bytes 6148
  63.3 40.2 %collective-permute-start.10 = (bf16[2048,256]{1,0:T(8,128)(2,1)}, bf16[2048,256]{1,0:T(8,128)(2,1)}, u32[]{:S(2)}, u32[]{:S(2)}) collective-permute-start(bf16[2048,256]{1,0:T(8,128)(2,1)} %bitcast.14.refs_1_), channel_id=1, source_target_pairs={{0,2},{1,15},{2,0},{3,5},{4,6},{5,3},{6,4},{7,9},{8,10},{9,7},{10,... | collective-permute-start | bytes 3145736 | tf_op jit(solution)/shard_map/ppermute | solution.py:421
  65.3 50.2 %collective-permute-start.5 = (bf16[256,2048]{1,0:T(8,128)(2,1)}, bf16[256,2048]{1,0:T(8,128)(2,1)}, u32[]{:S(2)}, u32[]{:S(2)}) collective-permute-start(bf16[256,2048]{1,0:T(8,128)(2,1)} %bitcast.12.refs_8_), channel_id=1, source_target_pairs={{0,2},{1,15},{2,0},{3,5},{4,6},{5,3},{6,4},{7,9},{8,10},{9,7},{10,... | collective-permute-start | bytes 3145736 | tf_op jit(solution)/shard_map/ppermute | solution.py:421
  69.8 47.6 %collective-permute-start.4 = (bf16[256,2048]{1,0:T(8,128)(2,1)}, bf16[256,2048]{1,0:T(8,128)(2,1)S(1)}, u32[]{:S(2)}, u32[]{:S(2)}) collective-permute-start(bf16[256,2048]{1,0:T(8,128)(2,1)} %bitcast.12.refs_8_), channel_id=1, source_target_pairs={{0,1},{1,0},{2,3},{3,2},{4,5},{5,4},{6,7},{7,6},{8,9},{9,8},{10,11... | collective-permute-start | bytes 3145736 | tf_op jit(solution)/shard_map/ppermute | solution.py:413
  71.8 4.9 %copy-start.3 = (bf16[256,128]{1,0:T(8,128)(2,1)S(1)}, bf16[256,128]{1,0:T(8,128)(2,1)}, u32[]{:S(2)}) copy-start(bf16[256,128]{1,0:T(8,128)(2,1)} %residual_ref.1) | copy-start | bytes 196612
  77.0 17.4 %copy-start.2 = (bf16[160,192]{1,0:T(8,128)(2,1)S(1)}, bf16[160,192]{1,0:T(8,128)(2,1)}, u32[]{:S(2)}) copy-start(bf16[160,192]{1,0:T(8,128)(2,1)} %constant.28.clone.drop_ref) | copy-start | bytes 184324
  95.5 28.1 %all-to-all-start.4 = ((bf16[16,160,128]{2,1,0:T(8,128)(2,1)}), bf16[16,160,128]{2,1,0:T(8,128)(2,1)S(1)}, u32[]{:S(2)}, u32[]{:S(2)}) async-start(bf16[16,160,128]{2,1,0:T(8,128)(2,1)} %shard_map.177), calls=%async_computation.4 | async-start | bytes 1310720 | tf_op jit(solution)/shard_map/all_to_all | solution.py:405
  99.1 20.7 %collective-permute-start.7 = (bf16[2048,256]{1,0:T(8,128)(2,1)}, bf16[2048,256]{1,0:T(8,128)(2,1)S(1)}, u32[]{:S(2)}, u32[]{:S(2)}) collective-permute-start(bf16[2048,256]{1,0:T(8,128)(2,1)} %bitcast.13.refs_0_), channel_id=1, source_target_pairs={{0,1},{1,0},{2,3},{3,2},{4,5},{5,4},{6,7},{7,6},{8,9},{9,8},{10,11... | collective-permute-start | bytes 3145736 | tf_op jit(solution)/shard_map/ppermute | solution.py:413
  101.2 18.7 %collective-permute-start.8 = (bf16[2048,256]{1,0:T(8,128)(2,1)}, bf16[2048,256]{1,0:T(8,128)(2,1)S(1)}, u32[]{:S(2)}, u32[]{:S(2)}) collective-permute-start(bf16[2048,256]{1,0:T(8,128)(2,1)} %bitcast.14.refs_1_), channel_id=1, source_target_pairs={{0,1},{1,0},{2,3},{3,2},{4,5},{5,4},{6,7},{7,6},{8,9},{9,8},{10,11... | collective-permute-start | bytes 3145736 | tf_op jit(solution)/shard_map/ppermute | solution.py:413
  103.5 16.4 %collective-permute-start.11 = (bf16[2048,256]{1,0:T(8,128)(2,1)}, bf16[2048,256]{1,0:T(8,128)(2,1)S(1)}, u32[]{:S(2)}, u32[]{:S(2)}) collective-permute-start(bf16[2048,256]{1,0:T(8,128)(2,1)} %collective-permute-done.9.refs_4_), channel_id=1, source_target_pairs={{0,1},{1,0},{2,3},{3,2},{4,5},{5,4},{6,7},{7,6},{8,9},{9,8},{10,11... | collective-permute-start | bytes 3145736 | tf_op jit(solution)/shard_map/ppermute | solution.py:413
  115.5 4.8 %collective-permute-start.12 = (bf16[2048,256]{1,0:T(8,128)(2,1)}, bf16[2048,256]{1,0:T(8,128)(2,1)S(1)}, u32[]{:S(2)}, u32[]{:S(2)}) collective-permute-start(bf16[2048,256]{1,0:T(8,128)(2,1)} %collective-permute-done.10.refs_5_), channel_id=1, source_target_pairs={{0,1},{1,0},{2,3},{3,2},{4,5},{5,4},{6,7},{7,6},{8,9},{9,8},{10,11... | collective-permute-start | bytes 3145736 | tf_op jit(solution)/shard_map/ppermute | solution.py:413
  117.4 5.1 %collective-permute-start.6 = (bf16[256,2048]{1,0:T(8,128)(2,1)}, bf16[256,2048]{1,0:T(8,128)(2,1)S(1)}, u32[]{:S(2)}, u32[]{:S(2)}) collective-permute-start(bf16[256,2048]{1,0:T(8,128)(2,1)} %collective-permute-done.5.refs_9_), channel_id=1, source_target_pairs={{0,1},{1,0},{2,3},{3,2},{4,5},{5,4},{6,7},{7,6},{8,9},{9,8},{10,11... | collective-permute-start | bytes 3145736 | tf_op jit(solution)/shard_map/ppermute | solution.py:413
  119.8 1.0 copy-start.6
  119.9 1.3 copy-start.7
  119.9 1.6 copy-start.8
  121.5 1.0 copy-start.9
  129.5 24.3 %copy-start.1 = (bf16[192,160]{1,0:T(8,128)(2,1)S(1)}, bf16[192,160]{1,0:T(8,128)(2,1)}, u32[]{:S(2)}) copy-start(bf16[192,160]{1,0:T(8,128)(2,1)} %constant.29.clone.widen_ref) | copy-start | bytes 184324
  154.7 6.0 %copy-start.5 = (f32[256,2]{0,1:T(2,128)S(1)}, f32[256,2]{0,1:T(2,128)}, u32[]{:S(2)}) copy-start(f32[256,2]{0,1:T(2,128)} %param.28) | copy-start | bytes 6148
  154.7 16.7 %all-to-all-start.6 = ((bf16[32,24,128]{2,1,0:T(8,128)(2,1)}), bf16[32,24,128]{2,1,0:T(8,128)(2,1)S(1)}, u32[]{:S(2)}, u32[]{:S(2)}) async-start(bf16[32,24,128]{2,1,0:T(8,128)(2,1)} %bitcast.15), calls=%async_computation.6 | async-start | bytes 393216 | tf_op jit(solution)/shard_map/all_to_all | solution.py:405
